TPU v7x, 256 devices: a 4x2x16 block of a 4x16x16 slice. The times are simulated.
256 devices in a mesh: grp: 2 (over y), sp: 32 (over z, core), tp: 4 (over x).
Axes of the slice: x: 4, y: 2, z: 16, core: 2. Of those that a mesh axis runs over, the one named last changes fastest.
The devices are a block of a 4x16x16 slice.
Arguments:
- tokens: bfloat16 [196608, 2048], P(('grp', 'sp', 'tp')), parts along dimension 0, may hold values from -6 to 6
- gain_pre: float32 [2, 2048], replicated, may hold values from 0.1 to 1.9
- gain_post: float32 [2, 2048], replicated, may hold values from 0.1 to 1.9
- w_b: bfloat16 [2, 2048, 512], P(None, 'sp', 'tp'), may hold values from -0.125 to 0.125
- w_c: bfloat16 [2, 2048, 512], P(None, 'sp', 'tp'), may hold values from -0.125 to 0.125
- w_x: bfloat16 [2, 2048, 512], P(None, 'sp', 'tp'), may hold values from -0.125 to 0.125
- taps: float32 [2, 3, 512], replicated, may hold values from -3.5 to 3.5
- w_out: bfloat16 [2, 512, 2048], P(None, 'tp', 'sp'), may hold values from -0.25 to 0.25
Outputs:
- result: bfloat16 [196608, 2048], P(('grp', 'sp', 'tp')), parts along dimension 0
There are 2 independent parts, one for each index of `grp`. A program takes and returns all parts, laid end to end along the dimension named above; an argument that names none is the same for every part. Nothing has to cross between parts.
All inputs are finite; a program needn't handle non-finite values.
Results may differ from a plain program's by a relative error of at most 0.024.
Values may be sent and summed in bfloat16 or wider, within the bound.
No kernel may reach another device: no remote copies, remote signals or barrier semaphores. Data moves between devices by JAX's collectives and lax.ppermute only.
A program may use at most 128 MiB of HBM per device.

v0:
```python
import jax
import jax.numpy as jnp
from jax import lax
from jax.sharding import PartitionSpec as P

epsilon = 1e-06


def turned_gather(arrays, axis, dims):
    turned = [jnp.moveaxis(a, dim, 0) for a, dim in zip(arrays, dims)]
    widths = [t[0].size for t in turned]
    both = jnp.concatenate([t.reshape(-1, w) for t, w in zip(turned, widths)], axis=1)
    result = lax.all_gather(both, axis, axis=0, tiled=True)
    blocks = jnp.split(result, [sum(widths[:k]) for k in range(1, len(widths))], axis=1)
    return tuple(
        (
            jnp.moveaxis(b.reshape(-1, *t.shape[1:]), 0, dim)
            for b, t, dim in zip(blocks, turned, dims)
        )
    )


def for_sending(value):
    return jax.tree.map(lambda a: a.astype(jnp.bfloat16) if a.dtype == jnp.float32 else a, value)


def joined_along(blocks, dim):
    dims = list(blocks.shape[1:])
    dims[dim] *= blocks.shape[0]
    return jnp.moveaxis(blocks, 0, dim).reshape(dims)


def sent_to_all(value, axis):
    copies = jnp.broadcast_to(value, (lax.axis_size(axis), *value.shape))
    return lax.all_to_all(copies, axis, split_axis=0, concat_axis=0, tiled=True)


def collect(value, axis, dim):
    return joined_along(sent_to_all(value, axis), dim)


def from_behind(block, axis, distance):
    devices = range(lax.axis_size(axis))
    route = [(i - distance, i) for i in devices if i - distance in devices]
    return lax.ppermute(block, axis, route)


def normed(activations, gain_row):
    values_f = activations.astype(jnp.float32)
    scale = lax.rsqrt(jnp.mean(values_f * values_f, axis=-1, keepdims=True) + epsilon)
    return values_f * scale * gain_row


def fold_into(hidden, pieces):
    return tuple(
        (
            jnp.dot(hidden, weight_piece, preferred_element_type=jnp.float32)
            for weight_piece in pieces
        )
    )


def convolve(extended, tap_rows):
    kernel_size = tap_rows.shape[0]
    row_total = extended.shape[0] - kernel_size + 1
    extended_f = extended.astype(jnp.float32)
    convolved = jnp.zeros((row_total, extended.shape[1]), jnp.float32)
    for offset in range(kernel_size):
        convolved = convolved + tap_rows[offset][None, :] * extended_f[offset : offset + row_total]
    return convolved


def layer_blocks(w_b, w_c, w_x, w_out, layer_index):
    return turned_gather(
        (w_b[layer_index], w_c[layer_index], w_x[layer_index], w_out[layer_index]),
        "tp",
        (1, 1, 1, 0),
    )


def gated_inputs(stream, gain_row, weights):
    hidden = normed(stream, gain_row).astype(jnp.bfloat16)
    sums = fold_into(
        hidden,
        jax.tree.map(
            lambda part: lax.all_gather(part, "sp", axis=0, tiled=True), for_sending(weights)
        ),
    )
    gate_b, gate_c, values = (item.astype(jnp.bfloat16) for item in sums)
    product = (gate_c.astype(jnp.float32) * values.astype(jnp.float32)).astype(jnp.bfloat16)
    return (gate_b, product)


def mixed_output(residual, gate_b, extended, tap_rows, out_weight, gain_row):
    convolved = convolve(extended, tap_rows)
    weighted = (gate_b.astype(jnp.float32) * convolved).astype(jnp.bfloat16)
    branch = jnp.dot(weighted, collect(out_weight, "sp", 1), preferred_element_type=jnp.float32)
    return (residual.astype(jnp.float32) + normed(branch, gain_row)).astype(jnp.bfloat16)


def on_device(tokens, gain_pre, gain_post, w_b, w_c, w_x, taps, w_out):
    layer_total = gain_pre.shape[0]
    kernel_size = taps.shape[1]
    reach = kernel_size - 1
    stream = tokens
    for layer_index in range(layer_total):
        blocks = layer_blocks(w_b, w_c, w_x, w_out, layer_index)
        gate_b, product = gated_inputs(stream, gain_pre[layer_index], blocks[:3])
        before = from_behind(product[-reach:], ("sp", "tp"), 1)
        extended = jnp.concatenate([before, product], axis=0)
        stream = mixed_output(
            stream, gate_b, extended, taps[layer_index], blocks[3], gain_post[layer_index]
        )
    return stream


def solution(mesh):
    placed = (
        P(("grp", "sp", "tp"), None),
        P(),
        P(),
        P(None, "sp", "tp"),
        P(None, "sp", "tp"),
        P(None, "sp", "tp"),
        P(),
        P(None, "tp", "sp"),
    )
    return jax.shard_map(
        on_device,
        mesh=mesh,
        in_specs=placed,
        out_specs=P(("grp", "sp", "tp"), None),
        check_vma=False,
    )
```

profile of v0, /device:TPU:33, one launch (start us, length us, event | category | flops | bytes accessed | tf_op | source)
XLA Modules:
  0.0 546.8 jit_solution(12233096743608469934)
XLA Ops:
  6.5 0.0 all-gather.11.cloned.1.call-start
  6.6 0.7 slice_bitcast_fusion.9
  7.3 0.7 slice_bitcast_fusion.6
  8.0 0.8 slice_bitcast_fusion.7
  8.8 10.6 %all_gather.24 = bf16[512,256]{0,1:T(8,128)(2,1)S(1)} all-gather(bf16[128,256]{0,1:T(8,128)(2,1)S(1)} %pad_maximum_fusion), channel_id=1, replica_groups=mesh['grp'=2,'sp'=32,'tp'=4] {'tp'}, dimensions={0}, use_global_device_ids=true | all-gather | bytes 327680 | tf_op jit(solution)/shard_map/all_gather | solution.py:13
  19.5 0.7 slice_bitcast_fusion.5
  20.1 0.1 all-gather.11.cloned.1.call-update
  20.2 0.1 all-gather.9.cloned.1.call-start
  20.3 0.7 all-gather.9.cloned.1.call-update
  21.0 0.1 all-gather.7.cloned.1.call-start
  21.1 0.7 all-gather.7.cloned.1.call-update
  21.8 1.6 broadcast_in_dim.4
  23.4 27.1 %all-to-all-start = ((bf16[32,512,64]{1,2,0:T(8,128)(2,1)}), bf16[32,512,64]{1,2,0:T(8,128)(2,1)S(1)}, u32[]{:S(2)}, u32[]{:S(2)}) async-start(bf16[32,512,64]{1,2,0:T(8,128)(2,1)} %broadcast_in_dim.4), calls=%async_computation | async-start | bytes 4194304 | tf_op jit(solution)/shard_map/all_to_all | solution.py:35
  50.4 0.1 all-gather.17.cloned.1.call-start
  50.5 10.3 %all_gather.28 = bf16[512,256]{0,1:T(8,128)(2,1)S(1)} all-gather(bf16[128,256]{0,1:T(8,128)(2,1)S(1)} %pad_maximum_fusion.1), channel_id=1, replica_groups=mesh['grp'=2,'sp'=32,'tp'=4] {'tp'}, dimensions={0}, use_global_device_ids=true | all-gather | bytes 327680 | tf_op jit(solution)/shard_map/all_gather | solution.py:13
  60.9 0.7 slice_bitcast_fusion.2
  61.5 0.1 all-gather.17.cloned.1.call-update
  61.6 0.1 all-gather.15.cloned.1.call-start
  61.7 0.6 all-gather.15.cloned.1.call-update
  62.3 95.9 %all-to-all-done = bf16[32,512,64]{1,2,0:T(8,128)(2,1)S(1)} async-done(((bf16[32,512,64]{1,2,0:T(8,128)(2,1)}), bf16[32,512,64]{1,2,0:T(8,128)(2,1)S(1)}, u32[]{:S(2)}, u32[]{:S(2)}) %all-to-all-start) | async-done | bytes 2097184 | tf_op jit(solution)/shard_map/all_to_all | solution.py:35
  158.1 0.0 copy-start.2
  158.1 1.3 copy-done.2
  159.5 0.0 copy-start
  159.5 1.6 broadcast_in_dim.5
  161.0 0.0 copy-start.3
  161.0 0.0 copy-start.4
  161.1 7.6 %all-to-all-start.1 = ((bf16[32,512,64]{1,2,0:T(8,128)(2,1)}), bf16[32,512,64]{1,2,0:T(8,128)(2,1)}, u32[]{:S(2)}, u32[]{:S(2)}) async-start(bf16[32,512,64]{1,2,0:T(8,128)(2,1)} %broadcast_in_dim.5), calls=%async_computation.1 | async-start | bytes 4194304 | tf_op jit(solution)/shard_map/all_to_all | solution.py:35
  168.6 0.1 all-gather.13.cloned.1.call-start
  168.7 0.6 all-gather.13.cloned.1.call-update
  169.3 0.0 copy-done
  169.3 0.7 fusion
  170.0 0.0 copy-done.3
  170.0 0.0 copy-done.4
  170.0 0.0 all-gather.11.cloned.1.call-done
  170.1 4.3 convolution_convert_fusion.3
  174.4 0.0 copy-start.5
  174.4 73.0 %all-gather.9.cloned.1.call-done = bf16[2048,512]{1,0:T(8,128)(2,1)} async-done(((bf16[64,512]{1,0:T(8,128)(2,1)}), bf16[2048,512]{1,0:T(8,128)(2,1)}) %all-gather.9.cloned.1.call-update) | async-done | bytes 2097168 | tf_op jit(solution)/shard_map/all_gather | solution.py:86
  247.4 3.6 multiply_convert_fusion.1
  251.0 2.1 collective-permute-start
  253.1 0.0 copy-done.5
  253.2 4.4 collective-permute-done
  257.5 1.4 maximum_convert_fusion
  258.9 60.5 %all-gather.7.cloned.1.call-done = bf16[2048,512]{1,0:T(8,128)(2,1)} async-done(((bf16[64,512]{1,0:T(8,128)(2,1)}), bf16[2048,512]{1,0:T(8,128)(2,1)}) %all-gather.7.cloned.1.call-update) | async-done | bytes 2097168 | tf_op jit(solution)/shard_map/all_gather | solution.py:86
  319.4 9.9 %multiply_reduce_fusion.1 = (f32[768]{0:T(1024)S(1)}, f32[768,2048]{1,0:T(8,128)}) fusion(bf16[512,2048]{0,1:T(8,128)(2,1)} %bitcast.64, f32[770,512]{1,0:T(8,128)} %maximum_convert_fusion, bf16[2048,512]{1,0:T(8,128)(2,1)} %all-gather.7.cloned.1.call-done, f32[512]{0:T(512)S(1)} %bitcast.76, f32[512]{0:T(512)S(1)} %bitcast.77, f32[512]{0:T(512)S(1)} %bitcast.78, ...), kind=kOutput, calls=%fused_computation.15 | convolution fusion | flops 3234200832 | bytes 18370560 | tf_op jit(solution)/shard_map/dot_general | solution.py:97
  329.3 4.8 fusion.4
  334.2 52.8 %all-gather.17.cloned.1.call-done = bf16[2048,512]{1,0:T(8,128)(2,1)} async-done(((bf16[64,512]{1,0:T(8,128)(2,1)}), bf16[2048,512]{1,0:T(8,128)(2,1)}) %all-gather.17.cloned.1.call-update) | async-done | bytes 2097168 | tf_op jit(solution)/shard_map/all_gather | solution.py:86
  386.9 0.0 copy-start.1
  386.9 5.4 convolution_convert_fusion
  392.4 63.4 %all-gather.15.cloned.1.call-done = bf16[2048,512]{1,0:T(8,128)(2,1)} async-done(((bf16[64,512]{1,0:T(8,128)(2,1)}), bf16[2048,512]{1,0:T(8,128)(2,1)}) %all-gather.15.cloned.1.call-update) | async-done | bytes 2097168 | tf_op jit(solution)/shard_map/all_gather | solution.py:86
  455.7 0.0 copy-done.1
  455.7 3.6 multiply_convert_fusion
  459.4 3.1 collective-permute-start.1
  462.5 3.0 collective-permute-done.1
  465.5 1.4 maximum_convert_fusion.1
  466.9 57.7 %all-gather.13.cloned.1.call-done = bf16[2048,512]{1,0:T(8,128)(2,1)} async-done(((bf16[64,512]{1,0:T(8,128)(2,1)}), bf16[2048,512]{1,0:T(8,128)(2,1)}) %all-gather.13.cloned.1.call-update) | async-done | bytes 2097168 | tf_op jit(solution)/shard_map/all_gather | solution.py:86
  524.5 0.0 all-to-all-done.1
  524.5 10.0 %multiply_reduce_fusion = (f32[768]{0:T(1024)S(1)}, f32[768,2048]{1,0:T(8,128)}) fusion(bf16[512,2048]{0,1:T(8,128)(2,1)} %bitcast.32, f32[770,512]{1,0:T(8,128)} %maximum_convert_fusion.1, bf16[2048,512]{1,0:T(8,128)(2,1)} %all-gather.13.cloned.1.call-done, f32[512]{0:T(512)S(1)} %bitcast.74, f32[512]{0:T(512)S(1)} %bitcast.75, f32[512]{0:T(512)S(1)} %bitcast.73, ...), kind=kOutput, calls=%fused_computation.14 | convolution fusion | flops 3234200832 | bytes 18370560 | tf_op jit(solution)/shard_map/dot_general | solution.py:97
  534.5 5.4 fusion.7
  (11 shorter events, 0.1 us)
Async XLA Ops:
  6.5 163.5 %all-gather.11.cloned.1.call-start = ((), (), s32[]{:S(2)}) async-start(), calls=%async_computation.4 | async-start | bytes 2162688 | tf_op jit(solution)/shard_map/all_gather | solution.py:86
  20.2 227.2 %all-gather.9.cloned.1.call-start = ((), (), s32[]{:S(2)}) async-start(), calls=%async_computation.3 | async-start | bytes 2162688 | tf_op jit(solution)/shard_map/all_gather | solution.py:86
  21.0 298.4 %all-gather.7.cloned.1.call-start = ((), (), s32[]{:S(2)}) async-start(), calls=%async_computation.2 | async-start | bytes 2162688 | tf_op jit(solution)/shard_map/all_gather | solution.py:86
  23.4 134.8 %all-to-all-start = ((bf16[32,512,64]{1,2,0:T(8,128)(2,1)}), bf16[32,512,64]{1,2,0:T(8,128)(2,1)S(1)}, u32[]{:S(2)}, u32[]{:S(2)}) async-start(bf16[32,512,64]{1,2,0:T(8,128)(2,1)} %broadcast_in_dim.4), calls=%async_computation | async-start | bytes 4194304 | tf_op jit(solution)/shard_map/all_to_all | solution.py:35
  50.4 336.5 %all-gather.17.cloned.1.call-start = ((), (), s32[]{:S(2)}) async-start(), calls=%async_computation.7 | async-start | bytes 2162688 | tf_op jit(solution)/shard_map/all_gather | solution.py:86
  61.6 394.1 %all-gather.15.cloned.1.call-start = ((), (), s32[]{:S(2)}) async-start(), calls=%async_computation.6 | async-start | bytes 2162688 | tf_op jit(solution)/shard_map/all_gather | solution.py:86
  158.1 1.3 copy-start.2
  159.5 9.8 %copy-start = (bf16[768,2048]{1,0:T(8,128)(2,1)S(1)}, bf16[768,2048]{1,0:T(8,128)(2,1)}, u32[]{:S(2)}) copy-start(bf16[768,2048]{1,0:T(8,128)(2,1)} %param.8) | copy-start | bytes 9437188
  161.0 8.9 %copy-start.3 = (f32[2,2048]{1,0:T(2,128)S(1)}, f32[2,2048]{1,0:T(2,128)}, u32[]{:S(2)}) copy-start(f32[2,2048]{1,0:T(2,128)} %param.9) | copy-start | bytes 49156
  161.0 9.0 %copy-start.4 = (f32[2,2048]{1,0:T(2,128)S(1)}, f32[2,2048]{1,0:T(2,128)}, u32[]{:S(2)}) copy-start(f32[2,2048]{1,0:T(2,128)} %param.10) | copy-start | bytes 49156
  161.1 363.5 %all-to-all-start.1 = ((bf16[32,512,64]{1,2,0:T(8,128)(2,1)}), bf16[32,512,64]{1,2,0:T(8,128)(2,1)}, u32[]{:S(2)}, u32[]{:S(2)}) async-start(bf16[32,512,64]{1,2,0:T(8,128)(2,1)} %broadcast_in_dim.5), calls=%async_computation.1 | async-start | bytes 4194304 | tf_op jit(solution)/shard_map/all_to_all | solution.py:35
  168.6 355.9 %all-gather.13.cloned.1.call-start = ((), (), s32[]{:S(2)}) async-start(), calls=%async_computation.5 | async-start | bytes 2162688 | tf_op jit(solution)/shard_map/all_gather | solution.py:86
  174.4 78.7 %copy-start.5 = (f32[2,3,512]{2,0,1:T(2,128)S(1)}, f32[2,3,512]{2,0,1:T(2,128)}, u32[]{:S(2)}) copy-start(f32[2,3,512]{2,0,1:T(2,128)} %param.14) | copy-start | bytes 36868
  251.0 6.5 %collective-permute-start = (bf16[2,512]{1,0:T(2,128)(2,1)S(1)}, bf16[2,512]{1,0:T(2,128)(2,1)S(1)}, u32[]{:S(2)}, u32[]{:S(2)}) collective-permute-start(bf16[2,512]{1,0:T(2,128)(2,1)S(1)} %slice.118), channel_id=1, source_target_pairs={{0,1},{1,2},{2,3},{3,4},{4,5},{5,6},{6,7},{7,8},{8,9},{9,10},{10,1... | collective-permute-start | bytes 6152 | tf_op jit(solution)/shard_map/ppermute | solution.py:45
  386.9 68.8 %copy-start.1 = (bf16[768,2048]{1,0:T(8,128)(2,1)S(1)}, bf16[768,2048]{1,0:T(8,128)(2,1)}, u32[]{:S(2)}) copy-start(bf16[768,2048]{1,0:T(8,128)(2,1)} %get-tuple-element.6) | copy-start | bytes 9437188
  459.4 6.1 %collective-permute-start.1 = (bf16[2,512]{1,0:T(2,128)(2,1)S(1)}, bf16[2,512]{1,0:T(2,128)(2,1)S(1)}, u32[]{:S(2)}, u32[]{:S(2)}) collective-permute-start(bf16[2,512]{1,0:T(2,128)(2,1)S(1)} %slice.122), channel_id=1, source_target_pairs={{0,1},{1,2},{2,3},{3,4},{4,5},{5,6},{6,7},{7,8},{8,9},{9,10},{10,1... | collective-permute-start | bytes 6152 | tf_op jit(solution)/shard_map/ppermute | solution.py:45
Sparse Core Ops, SparseCore 0:
  20.3 114.5 all-gather.10
  136.8 110.5 all-gather.8
  249.2 70.1 all-gather.6
  321.1 65.7 all-gather.16
  388.6 67.0 all-gather.14
  457.4 67.0 all-gather.12
where the time goes:
time: 548 us; the launch traced here: 547 us
  waiting for transfers between devices  413 us (75%)
  starting transfers between devices  40.2 us (7%)
  matrix products  36.8 us (7%)
  blocking collectives  21 us (4%)
  other arithmetic  13.8 us (3%)
  between operations  13.6 us (2%)
  local copies, waits for them, and re-layouts  8.13 us (1%)
    all_gather x6, waiting for transfers between devices, gated_inputs(): lax.all_gather(part, 'sp', axis=0, tiled=True)  307 us
    all_to_all x2, waiting for transfers between devices, sent_to_all(): return lax.all_to_all(copies, axis, split_axis=0, concat_axis=0, tiled=True)  95.9 us
    all_to_all x2, starting transfers between devices, sent_to_all(): return lax.all_to_all(copies, axis, split_axis=0, concat_axis=0, tiled=True)  34.6 us
    all_gather x2, blocking collectives, turned_gather(): result = lax.all_gather(both, axis, axis=0, tiled=True)  21 us
    dot_general x2, matrix products, mixed_output(): jnp.dot(weighted, collect(out_weight, 'sp', 1), preferred_element_type=jn...  19.9 us
    dot_general x4, matrix products, fold_into(): jnp.dot(hidden, weight_piece, preferred_element_type=jnp.float32)  16.9 us
  transfers between devices with their start and end apart: 10, of which 8 were waited for; matrix products, arithmetic and copies ran while one was open for 7% of the time, Pallas kernels for 0%

commit v1 on v0

v1 whole, which is shorter than its diff:
```python
import jax
import jax.numpy as jnp
from jax import lax
from jax.experimental import pallas as pl
from jax.experimental.pallas import tpu as pltpu
from jax.sharding import PartitionSpec as P

epsilon = 1e-06
HALO = 32
TILES = 2
MATS = 4


def rms(values_f):
    return lax.rsqrt(jnp.mean(values_f * values_f, axis=-1, keepdims=True) + epsilon)


def nt_dot(a, b):
    return lax.dot_general(a, b, (((1,), (1,)), ((), ())), preferred_element_type=jnp.float32)


def layer_body(stream, weights, gain_pre, taps, gain_post, conv_ref, branch_ref):
    rows = stream.shape[0]
    kernel_size = taps.shape[0]
    values_f = stream.astype(jnp.float32)
    hidden = (values_f * rms(values_f) * gain_pre).astype(jnp.bfloat16)
    project = lambda m: jnp.dot(hidden, weights(m), preferred_element_type=jnp.float32).astype(jnp.bfloat16)
    gate_c = project(1)
    values = project(2)
    product = (gate_c.astype(jnp.float32) * values.astype(jnp.float32)).astype(jnp.bfloat16)
    conv_ref[pl.ds(8, rows), :] = product.astype(jnp.float32)
    convolved = taps[0:1] * conv_ref[pl.ds(8 - kernel_size + 1, rows), :]
    for k in range(1, kernel_size):
        convolved = convolved + taps[k : k + 1] * conv_ref[pl.ds(8 - kernel_size + 1 + k, rows), :]
    gate_b = project(0)
    weighted = (gate_b.astype(jnp.float32) * convolved).astype(jnp.bfloat16)
    conv_ref[0:8, :] = conv_ref[pl.ds(rows, 8), :]
    branch_ref[...] = nt_dot(weighted, weights(3))
    branch = branch_ref[...]
    return (stream.astype(jnp.float32) + branch * rms(branch) * gain_post).astype(jnp.bfloat16)


def mixer(copies, sources, gain_pre, taps, gain_post, stream_parts, dims, out_rows, name):
    d, dc, sp, block_rows = dims
    total = sum(p.shape[0] for p in stream_parts)
    tile = total // TILES
    skip = total - out_rows
    n_src, n_parts = len(sources), len(stream_parts)

    def kernel(*refs):
        src = refs[:n_src]
        parts = refs[n_src : n_src + n_parts]
        pre_ref, taps_ref, post_ref, out_ref = refs[n_src + n_parts : n_src + n_parts + 4]
        w_ref, x_ref, conv_ref, branch_ref, res_ref, w_sem, x_sem, o_sem = refs[n_src + n_parts + 4 :]

        def part_copies():
            start = 0
            for k, p in enumerate(parts):
                yield pltpu.make_async_copy(p, x_ref.at[pl.ds(start, p.shape[0])], x_sem.at[k])
                start += p.shape[0]

        for c in part_copies():
            c.start()
        for s, t in copies(src, w_ref):
            pltpu.make_async_copy(s, t, w_sem).start()
        conv_ref[0:8, :] = jnp.zeros((8, dc), jnp.float32)
        for c in part_copies():
            c.wait()
        for s, t in copies(src, w_ref):
            pltpu.make_async_copy(s, t, w_sem).wait()

        def out_copy(i):
            first = skip if i == 0 else 0
            n = tile - first
            return pltpu.make_async_copy(
                res_ref.at[i, pl.ds(first, n)], out_ref.at[pl.ds(i * tile - skip + first, n)], o_sem.at[i]
            )

        def step(i, carry):
            row = pl.multiple_of(i * tile, 16)
            res_ref[i] = layer_body(
                x_ref[pl.ds(row, tile), :],
                lambda m: w_ref[m].reshape(d, dc),
                pre_ref[...],
                taps_ref[...],
                post_ref[...],
                conv_ref,
                branch_ref,
            )
            return carry

        lax.fori_loop(0, TILES, step, 0)
        for i in range(TILES):
            out_copy(i).start()
        for i in range(TILES):
            out_copy(i).wait()

    hbm = pl.BlockSpec(memory_space=pltpu.MemorySpace.HBM)
    vmem = pl.BlockSpec(memory_space=pltpu.MemorySpace.VMEM)
    return pl.pallas_call(
        kernel,
        out_shape=jax.ShapeDtypeStruct((out_rows, d), jnp.bfloat16),
        in_specs=[hbm] * (n_src + n_parts) + [vmem] * 3,
        out_specs=hbm,
        scratch_shapes=[
            pltpu.VMEM((MATS, sp, block_rows, dc), jnp.bfloat16),
            pltpu.VMEM((total, d), jnp.bfloat16),
            pltpu.VMEM((tile + 8, dc), jnp.float32),
            pltpu.VMEM((tile, d), jnp.float32),
            pltpu.VMEM((TILES, tile, d), jnp.bfloat16),
            pltpu.SemaphoreType.DMA,
            pltpu.SemaphoreType.DMA((n_parts,)),
            pltpu.SemaphoreType.DMA((TILES,)),
        ],
        compiler_params=pltpu.CompilerParams(vmem_limit_bytes=56 * 2**20),
        name=name,
    )(*sources, *stream_parts, gain_pre, taps, gain_post)


def turned(axis, size, stride, distance):
    n = size // stride
    return [(((i // stride + distance) % n) * stride + i % stride, i) for i in range(size)]


def receive(value, axis, distance, stride=1):
    return lax.ppermute(value, axis, turned(axis, lax.axis_size(axis), stride, distance))


def other_core(value):
    return lax.ppermute(value, "sp", [(i ^ 1, i) for i in range(lax.axis_size("sp"))])


def early_halo(tokens):
    axes = ("sp", "tp")
    total = lax.axis_size(axes)
    return lax.ppermute(tokens[-HALO:], axes, [(i - 1, i) for i in range(1, total)])


def on_device(tokens, gain_pre, gain_post, w_b, w_c, w_x, taps, w_out):
    layer_total, block_rows, block_cols = w_b.shape
    sp, tp = lax.axis_size("sp"), lax.axis_size("tp")
    d, dc = sp * block_rows, tp * block_cols
    dims = (d, dc, sp, block_rows)
    chips = sp // 2
    own = [
        jnp.stack([w_b[l], w_c[l], w_x[l], w_out[l].T]) for l in range(layer_total)
    ]

    last = own[1]
    along = jnp.stack([last] + [receive(last, "tp", k) for k in range(1, tp)])
    gathered = lax.all_gather(along, "sp", axis=0)
    halo = early_halo(tokens)

    z = lambda value, distance: receive(value, "sp", distance, 2)
    quarter = chips // 4
    first = own[0]
    one = jnp.stack([first, z(first, quarter), z(first, 2 * quarter), z(first, -quarter)])
    wrap = jnp.stack([one[3], one[0]])
    two = jnp.concatenate([one, z(one, 1), z(one[:2], 2), z(wrap, -2), z(one, -1)])
    offsets = (
        [quarter * k for k in range(4)]
        + [1 + quarter * k for k in range(4)]
        + [2, 2 + quarter]
        + [-2 + 3 * quarter, -2]
        + [-1 + quarter * k for k in range(4)]
    )
    half = chips // 2
    ahead = receive(two, "tp", 1)
    behind = receive(two, "tp", -1)
    far_a = receive(ahead[:half], "tp", 1)
    far_b = receive(behind[half:], "tp", -1)
    mine = [two, ahead, behind, far_a, far_b]
    theirs = [other_core(value) for value in mine]
    places = [(0, 0), (1, 0), (-1, 0), (2, 0), (2, half)]

    def first_copies(src, w_ref):
        here_sp, here_tp = lax.axis_index("sp"), lax.axis_index("tp")
        chip, core = here_sp // 2, here_sp % 2
        for side in range(2):
            side_core = core if side == 0 else 1 - core
            for p, (column, begin) in enumerate(places):
                ref = src[side * len(places) + p]
                lanes = pl.multiple_of(((here_tp + column + tp) % tp) * block_cols, block_cols)
                for k in range(ref.shape[0]):
                    row = ((chip + offsets[begin + k] + chips) % chips) * 2 + side_core
                    yield ref.at[k], w_ref.at[:, row, :, pl.ds(lanes, block_cols)]

    def last_copies(src, w_ref):
        here_tp = lax.axis_index("tp")
        for k in range(tp):
            lanes = pl.multiple_of(((here_tp + k) % tp) * block_cols, block_cols)
            for m in range(MATS):
                yield src[0].at[:, k, m], w_ref.at[m, :, :, pl.ds(lanes, block_cols)]

    row_of = lambda a, l: a[l][None, :]
    rows = tokens.shape[0]
    stream = mixer(
        first_copies, mine + theirs, row_of(gain_pre, 0), taps[0], row_of(gain_post, 0),
        [halo, tokens], dims, rows + HALO, "mixer_first",
    )
    return mixer(
        last_copies, [gathered], row_of(gain_pre, 1), taps[1], row_of(gain_post, 1),
        [stream], dims, rows, "mixer_last",
    )


def solution(mesh):
    placed = (
        P(("grp", "sp", "tp"), None),
        P(),
        P(),
        P(None, "sp", "tp"),
        P(None, "sp", "tp"),
        P(None, "sp", "tp"),
        P(),
        P(None, "tp", "sp"),
    )
    return jax.shard_map(
        on_device,
        mesh=mesh,
        in_specs=placed,
        out_specs=P(("grp", "sp", "tp"), None),
        check_vma=False,
    )
```

time: 548 us -> 167 us (0.30)
  waiting for transfers between devices: 413 us -> 54.7 us
  matrix products: 36.8 us -> 0 us
  Pallas kernels: 0 us -> 31 us
  blocking collectives: 21 us -> 0 us
  starting transfers between devices: 40.2 us -> 59 us
  other arithmetic: 13.8 us -> 0.83 us
    all_gather x6 -> x1, waiting for transfers between devices: 307 us -> 0.02 us  [on_device(): gathered = lax.all_gather(along, 'sp', axis=0)]
    all_to_all x2 -> x0, waiting for transfers between devices: 95.9 us -> none  [sent_to_all(): return lax.all_to_all(copies, axis, split_axis=0, concat_axis=0, tiled=True)]
    ppermute x2 -> x20, starting transfers between devices: 5.26 us -> 59 us  [the longest x14 46.3 us: receive(): lax.ppermute(value, axis, turned(axis, lax.axis_size(axis), stride, dista...]
    ppermute x2 -> x20, waiting for transfers between devices: 7.38 us -> 54.6 us  [the longest x14 46.1 us: receive(): lax.ppermute(value, axis, turned(axis, lax.axis_size(axis), stride, dista...]
    dot_general x6 -> x0, matrix products: 36.8 us -> none  [the longest x2 19.9 us: mixed_output(): jnp.dot(weighted, collect(out_weight, 'sp', 1), preferred_element_type=jn...]
    all_to_all x2 -> x0, starting transfers between devices: 34.6 us -> none  [sent_to_all(): return lax.all_to_all(copies, axis, split_axis=0, concat_axis=0, tiled=True)]
    pallas_call x0 -> x2, Pallas kernels: none -> 31 us  [mixer(): pl.pallas_call(kernel, out_shape=jax.ShapeDtypeStruct((out_rows, d), jnp....]
    all_gather x2 -> x0, blocking collectives: 21 us -> none  [turned_gather(): result = lax.all_gather(both, axis, axis=0, tiled=True)]
  transfers between devices with their start and end apart: 10 -> 21, of which waited for: 8 -> 12; matrix products, arithmetic and copies ran while one was open for 7% -> 2% of each run, Pallas kernels for 0% -> 9%
where the time goes in v1:
time: 167 us; the launch traced here: 165 us
  starting transfers between devices  59 us (35%)
  waiting for transfers between devices  54.7 us (33%)
  Pallas kernels  31 us (19%)
  between operations  13.7 us (8%)
  local copies, waits for them, and re-layouts  5.55 us (3%)
    ppermute x14, starting transfers between devices, receive(): lax.ppermute(value, axis, turned(axis, lax.axis_size(axis), stride, dista...  46.3 us
    ppermute x14, waiting for transfers between devices, receive(): lax.ppermute(value, axis, turned(axis, lax.axis_size(axis), stride, dista...  46.1 us
    pallas_call x2, Pallas kernels, mixer(): pl.pallas_call(kernel, out_shape=jax.ShapeDtypeStruct((out_rows, d), jnp....  31 us
    ppermute x5, starting transfers between devices, other_core(): lax.ppermute(value, 'sp', [(i ^ 1, i) for i in range(lax.axis_size('sp'))])  9.81 us
    ppermute x1, waiting for transfers between devices, early_halo(): lax.ppermute(tokens[-HALO:], axes, [(i - 1, i) for i in range(1, total)])  6.47 us
  transfers between devices with their start and end apart: 21, of which 12 were waited for; matrix products, arithmetic and copies ran while one was open for 2% of the time, Pallas kernels for 9%

profile of v1, /device:TPU:33, one launch (start us, length us, event | category | flops | bytes accessed | tf_op | source)
XLA Modules:
  0.0 164.8 jit_solution(10587350070008046298)
XLA Ops:
  6.5 0.0 all-gather.3.cloned.1.call-start
  6.6 0.7 fusion.4
  7.3 0.7 slice_bitcast_fusion
  8.0 0.8 fusion.2
  8.8 0.0 copy-start.13
  8.8 0.0 copy-start.11
  8.8 0.0 copy-start.12
  8.9 3.8 %collective-permute-start = (bf16[4,64,128]{2,1,0:T(8,128)(2,1)S(1)}, bf16[4,64,128]{2,1,0:T(8,128)(2,1)S(1)}, u32[]{:S(2)}, u32[]{:S(2)}) collective-permute-start(bf16[4,64,128]{2,1,0:T(8,128)(2,1)S(1)} %get-tuple-element.10), channel_id=1, source_target_pairs={{1,0},{2,1},{3,2},{0,3},{5,4},{6,5},{7,6},{4,7},{9,8},{10,9},{11,1... | collective-permute-start | bytes 196616 | tf_op jit(solution)/shard_map/ppermute | solution.py:126
  12.7 0.3 collective-permute-start.1
  12.9 0.7 collective-permute-start.2
  13.7 0.3 collective-permute-done
  14.0 3.4 %collective-permute-done.1 = bf16[4,64,128]{2,1,0:T(8,128)(2,1)S(1)} collective-permute-done((bf16[4,64,128]{2,1,0:T(8,128)(2,1)S(1)}, bf16[4,64,128]{2,1,0:T(8,128)(2,1)S(1)}, u32[]{:S(2)}, u32[]{:S(2)}) %collective-permute-start.1) | collective-permute-done | bytes 65568 | tf_op jit(solution)/shard_map/ppermute | solution.py:126
  17.4 0.6 collective-permute-done.2
  18.0 0.7 pad_maximum_fusion
  18.7 0.1 all-gather.3.cloned.1.call-update
  18.8 21.3 %collective-permute-start.3 = (bf16[4,64,128]{2,1,0:T(8,128)(2,1)S(1)}, bf16[4,64,128]{2,1,0:T(8,128)(2,1)S(1)}, u32[]{:S(2)}, u32[]{:S(2)}) collective-permute-start(bf16[4,64,128]{2,1,0:T(8,128)(2,1)S(1)} %get-tuple-element.8), channel_id=1, source_target_pairs={{32,0},{36,4},{40,8},{44,12},{48,16},{52,20},{56,24},{60,28},{64,3... | collective-permute-start | bytes 196616 | tf_op jit(solution)/shard_map/ppermute | solution.py:126
  40.1 0.0 collective-permute-start.5
  40.1 5.2 %collective-permute-start.4 = (bf16[4,64,128]{2,1,0:T(8,128)(2,1)S(1)}, bf16[4,64,128]{2,1,0:T(8,128)(2,1)S(1)}, u32[]{:S(2)}, u32[]{:S(2)}) collective-permute-start(bf16[4,64,128]{2,1,0:T(8,128)(2,1)S(1)} %get-tuple-element.8), channel_id=1, source_target_pairs={{64,0},{68,4},{72,8},{76,12},{80,16},{84,20},{88,24},{92,28},{96,3... | collective-permute-start | bytes 196616 | tf_op jit(solution)/shard_map/ppermute | solution.py:126
  45.3 0.0 collective-permute-done.3
  45.3 6.3 %collective-permute-done.5 = bf16[4,64,128]{2,1,0:T(8,128)(2,1)S(1)} collective-permute-done((bf16[4,64,128]{2,1,0:T(8,128)(2,1)S(1)}, bf16[4,64,128]{2,1,0:T(8,128)(2,1)S(1)}, u32[]{:S(2)}, u32[]{:S(2)}) %collective-permute-start.5) | collective-permute-done | bytes 65568 | tf_op jit(solution)/shard_map/ppermute | solution.py:126
  51.7 1.1 collective-permute-done.4
  52.8 9.2 %collective-permute-start.6 = (bf16[4,4,64,128]{3,2,1,0:T(8,128)(2,1)S(1)}, bf16[4,4,64,128]{3,2,1,0:T(8,128)(2,1)S(1)}, u32[]{:S(2)}, u32[]{:S(2)}) collective-permute-start(bf16[4,4,64,128]{3,2,1,0:T(8,128)(2,1)S(1)} %pad_maximum_fusion.1), channel_id=1, source_target_pairs={{8,0},{12,4},{16,8},{20,12},{24,16},{28,20},{32,24},{36,28},{40,32... | collective-permute-start | bytes 786440 | tf_op jit(solution)/shard_map/ppermute | solution.py:126
  62.0 0.0 collective-permute-start.9
  62.0 2.2 %collective-permute-start.7 = (bf16[2,4,64,128]{3,2,1,0:T(8,128)(2,1)S(1)}, bf16[2,4,64,128]{3,2,1,0:T(8,128)(2,1)S(1)}, u32[]{:S(2)}, u32[]{:S(2)}) collective-permute-start(bf16[2,4,64,128]{3,2,1,0:T(8,128)(2,1)S(1)} %get-tuple-element.6), channel_id=1, source_target_pairs={{16,0},{20,4},{24,8},{28,12},{32,16},{36,20},{40,24},{44,28},{48,3... | collective-permute-start | bytes 393224 | tf_op jit(solution)/shard_map/ppermute | solution.py:126
  64.3 0.2 collective-permute-start.8
  64.5 9.5 %collective-permute-done.6 = bf16[4,4,64,128]{3,2,1,0:T(8,128)(2,1)S(1)} collective-permute-done((bf16[4,4,64,128]{3,2,1,0:T(8,128)(2,1)S(1)}, bf16[4,4,64,128]{3,2,1,0:T(8,128)(2,1)S(1)}, u32[]{:S(2)}, u32[]{:S(2)}) %collective-permute-start.6) | collective-permute-done | bytes 262176 | tf_op jit(solution)/shard_map/ppermute | solution.py:126
  74.1 6.8 %collective-permute-done.7 = bf16[2,4,64,128]{3,2,1,0:T(8,128)(2,1)S(1)} collective-permute-done((bf16[2,4,64,128]{3,2,1,0:T(8,128)(2,1)S(1)}, bf16[2,4,64,128]{3,2,1,0:T(8,128)(2,1)S(1)}, u32[]{:S(2)}, u32[]{:S(2)}) %collective-permute-start.7) | collective-permute-done | bytes 131104 | tf_op jit(solution)/shard_map/ppermute | solution.py:126
  80.9 0.0 collective-permute-done.8
  81.0 0.0 collective-permute-done.9
  81.0 0.0 copy-start.2
  81.0 0.1 collective-permute-start.10
  81.2 1.4 collective-permute-start.11
  82.6 18.1 %collective-permute-done.10.refs_1_ = bf16[16,4,64,128]{3,2,1,0:T(8,128)(2,1)S(1)} collective-permute-done((bf16[16,4,64,128]{3,2,1,0:T(8,128)(2,1)S(1)}, bf16[16,4,64,128]{3,2,1,0:T(8,128)(2,1)S(1)}, u32[]{:S(2)}, u32[]{:S(2)}) %collective-permute-start.10) | collective-permute-done | bytes 1048608 | tf_op jit(solution)/shard_map/ppermute | solution.py:126
  100.7 0.8 collective-permute-start.12
  101.5 0.0 collective-permute-done.11.refs_2_
  101.6 0.9 collective-permute-start.13
  102.5 0.9 slice.63
  103.4 2.9 %collective-permute-start.19 = (bf16[32,2048]{1,0:T(8,128)(2,1)S(1)}, bf16[32,2048]{1,0:T(8,128)(2,1)S(1)}, u32[]{:S(2)}, u32[]{:S(2)}) collective-permute-start(bf16[32,2048]{1,0:T(8,128)(2,1)S(1)} %slice.63), channel_id=1, source_target_pairs={{0,1},{1,2},{2,3},{3,4},{4,5},{5,6},{6,7},{7,8},{8,9},{9,10},{10,1... | collective-permute-start | bytes 393224 | tf_op jit(solution)/shard_map/ppermute | solution.py:136
  106.3 8.9 %collective-permute-start.14 = (bf16[16,4,64,128]{3,2,1,0:T(8,128)(2,1)S(1)}, bf16[16,4,64,128]{3,2,1,0:T(8,128)(2,1)S(1)}, u32[]{:S(2)}, u32[]{:S(2)}) collective-permute-start(bf16[16,4,64,128]{3,2,1,0:T(8,128)(2,1)S(1)} %constant_dynamic-update-slice_fusion.refs_0_), channel_id=1, source_target_pairs={{4,0},{0,4},{12,8},{8,12},{20,16},{16,20},{28,24},{24,28},{36,32},... | collective-permute-start | bytes 3145736 | tf_op jit(solution)/shard_map/ppermute | solution.py:130
  115.2 0.1 collective-permute-start.15
  115.4 6.5 %collective-permute-done.19.refs_10_ = bf16[32,2048]{1,0:T(8,128)(2,1)S(1)} collective-permute-done((bf16[32,2048]{1,0:T(8,128)(2,1)S(1)}, bf16[32,2048]{1,0:T(8,128)(2,1)S(1)}, u32[]{:S(2)}, u32[]{:S(2)}) %collective-permute-start.19) | collective-permute-done | bytes 131104 | tf_op jit(solution)/shard_map/ppermute | solution.py:136
  121.8 0.0 collective-permute-start.16
  121.9 0.0 collective-permute-done.12.refs_3_
  121.9 0.6 collective-permute-start.17
  122.5 0.0 collective-permute-done.13.refs_4_
  122.5 0.2 collective-permute-start.18
  122.7 0.7 copy_bitcast_fusion
  123.3 0.6 fusion.5
  124.0 0.0 collective-permute-done.14.refs_5_
  124.0 0.0 collective-permute-done.15.refs_6_
  124.0 0.5 collective-permute-done.16.refs_7_
  124.5 0.7 collective-permute-done.17.refs_8_
  125.3 0.7 collective-permute-done.18.refs_9_
  126.0 0.8 copy-done.9
  126.8 0.0 copy-done.10
  126.8 0.0 copy-done.6
  126.8 0.0 copy-done.7
  126.8 0.0 copy-done.3
  126.8 0.0 copy-done.4
  126.9 0.0 copy-done.5
  126.9 0.0 copy-done.8
  126.9 15.5 %mixer_first.1.refs_1_ = bf16[800,2048]{1,0:T(8,128)(2,1)} custom-call(bf16[16,4,64,128]{3,2,1,0:T(8,128)(2,1)} %copy-done.2, bf16[16,4,64,128]{3,2,1,0:T(8,128)(2,1)} %copy-done, bf16[16,4,64,128]{3,2,1,0:T(8,128)(2,1)} %copy-done.1, bf16[8,4,64,128]{3,2,1,0:T(8,128)(2,1)} %copy-done.6, bf16[8,4,64,128]{3,2,1,0:T(8,128)(2,1)} %copy-done.7, ...), custom_call_target="tpu_custom_call" | custom-call | tf_op jit(solution)/shard_map/mixer_first/pallas_call | solution.py:100
  142.4 0.0 all-gather.3.cloned.1.call-done
  142.4 15.5 %mixer_last.1 = bf16[768,2048]{1,0:T(8,128)(2,1)} custom-call(bf16[32,4,4,64,128]{4,3,2,1,0:T(8,128)(2,1)} %bitcast.31, bf16[800,2048]{1,0:T(8,128)(2,1)} %mixer_first.1.refs_1_, f32[1,2048]{1,0:T(1,128)} %get-tuple-element.30.refs_2_, f32[3,512]{1,0:T(4,128)} %get-tuple-element.27.refs_3_, f32[1,2048]{1,0:T(1,128)} %get-tuple-element.19.refs_4_), custom_call_target="tpu_custom_call" | custom-call | tf_op jit(solution)/shard_map/mixer_last/pallas_call | solution.py:100
  (31 shorter events, 0.4 us)
Async XLA Ops:
  6.5 135.8 %all-gather.3.cloned.1.call-start = ((), (), s32[]{:S(2)}) async-start(), calls=%async_computation | async-start | bytes 8650752 | tf_op jit(solution)/shard_map/all_gather | solution.py:151
  8.8 113.0 %copy-start.13 = (f32[2,3,512]{2,0,1:T(2,128)S(1)}, f32[2,3,512]{2,0,1:T(2,128)}, u32[]{:S(2)}) copy-start(f32[2,3,512]{2,0,1:T(2,128)} %param.14) | copy-start | bytes 36868
  8.8 114.5 %copy-start.11 = (f32[2,2048]{1,0:T(2,128)S(1)}, f32[2,2048]{1,0:T(2,128)}, u32[]{:S(2)}) copy-start(f32[2,2048]{1,0:T(2,128)} %param.10) | copy-start | bytes 49156
  8.8 114.5 %copy-start.12 = (f32[2,2048]{1,0:T(2,128)S(1)}, f32[2,2048]{1,0:T(2,128)}, u32[]{:S(2)}) copy-start(f32[2,2048]{1,0:T(2,128)} %param.9) | copy-start | bytes 49156
  8.9 5.1 %collective-permute-start = (bf16[4,64,128]{2,1,0:T(8,128)(2,1)S(1)}, bf16[4,64,128]{2,1,0:T(8,128)(2,1)S(1)}, u32[]{:S(2)}, u32[]{:S(2)}) collective-permute-start(bf16[4,64,128]{2,1,0:T(8,128)(2,1)S(1)} %get-tuple-element.10), channel_id=1, source_target_pairs={{1,0},{2,1},{3,2},{0,3},{5,4},{6,5},{7,6},{4,7},{9,8},{10,9},{11,1... | collective-permute-start | bytes 196616 | tf_op jit(solution)/shard_map/ppermute | solution.py:126
  12.7 4.7 %collective-permute-start.1 = (bf16[4,64,128]{2,1,0:T(8,128)(2,1)S(1)}, bf16[4,64,128]{2,1,0:T(8,128)(2,1)S(1)}, u32[]{:S(2)}, u32[]{:S(2)}) collective-permute-start(bf16[4,64,128]{2,1,0:T(8,128)(2,1)S(1)} %get-tuple-element.10), channel_id=1, source_target_pairs={{2,0},{3,1},{0,2},{1,3},{6,4},{7,5},{4,6},{5,7},{10,8},{11,9},{8,1... | collective-permute-start | bytes 196616 | tf_op jit(solution)/shard_map/ppermute | solution.py:126
  12.9 5.0 %collective-permute-start.2 = (bf16[4,64,128]{2,1,0:T(8,128)(2,1)S(1)}, bf16[4,64,128]{2,1,0:T(8,128)(2,1)S(1)}, u32[]{:S(2)}, u32[]{:S(2)}) collective-permute-start(bf16[4,64,128]{2,1,0:T(8,128)(2,1)S(1)} %get-tuple-element.10), channel_id=1, source_target_pairs={{3,0},{0,1},{1,2},{2,3},{7,4},{4,5},{5,6},{6,7},{11,8},{8,9},{9,10... | collective-permute-start | bytes 196616 | tf_op jit(solution)/shard_map/ppermute | solution.py:126
  18.8 26.5 %collective-permute-start.3 = (bf16[4,64,128]{2,1,0:T(8,128)(2,1)S(1)}, bf16[4,64,128]{2,1,0:T(8,128)(2,1)S(1)}, u32[]{:S(2)}, u32[]{:S(2)}) collective-permute-start(bf16[4,64,128]{2,1,0:T(8,128)(2,1)S(1)} %get-tuple-element.8), channel_id=1, source_target_pairs={{32,0},{36,4},{40,8},{44,12},{48,16},{52,20},{56,24},{60,28},{64,3... | collective-permute-start | bytes 196616 | tf_op jit(solution)/shard_map/ppermute | solution.py:126
  40.1 11.6 %collective-permute-start.5 = (bf16[4,64,128]{2,1,0:T(8,128)(2,1)S(1)}, bf16[4,64,128]{2,1,0:T(8,128)(2,1)S(1)}, u32[]{:S(2)}, u32[]{:S(2)}) collective-permute-start(bf16[4,64,128]{2,1,0:T(8,128)(2,1)S(1)} %get-tuple-element.8), channel_id=1, source_target_pairs={{96,0},{100,4},{104,8},{108,12},{112,16},{116,20},{120,24},{124,28... | collective-permute-start | bytes 196616 | tf_op jit(solution)/shard_map/ppermute | solution.py:126
  40.1 12.7 %collective-permute-start.4 = (bf16[4,64,128]{2,1,0:T(8,128)(2,1)S(1)}, bf16[4,64,128]{2,1,0:T(8,128)(2,1)S(1)}, u32[]{:S(2)}, u32[]{:S(2)}) collective-permute-start(bf16[4,64,128]{2,1,0:T(8,128)(2,1)S(1)} %get-tuple-element.8), channel_id=1, source_target_pairs={{64,0},{68,4},{72,8},{76,12},{80,16},{84,20},{88,24},{92,28},{96,3... | collective-permute-start | bytes 196616 | tf_op jit(solution)/shard_map/ppermute | solution.py:126
  52.8 21.2 %collective-permute-start.6 = (bf16[4,4,64,128]{3,2,1,0:T(8,128)(2,1)S(1)}, bf16[4,4,64,128]{3,2,1,0:T(8,128)(2,1)S(1)}, u32[]{:S(2)}, u32[]{:S(2)}) collective-permute-start(bf16[4,4,64,128]{3,2,1,0:T(8,128)(2,1)S(1)} %pad_maximum_fusion.1), channel_id=1, source_target_pairs={{8,0},{12,4},{16,8},{20,12},{24,16},{28,20},{32,24},{36,28},{40,32... | collective-permute-start | bytes 786440 | tf_op jit(solution)/shard_map/ppermute | solution.py:126
  62.0 19.0 %collective-permute-start.9 = (bf16[4,4,64,128]{3,2,1,0:T(8,128)(2,1)S(1)}, bf16[4,4,64,128]{3,2,1,0:T(8,128)(2,1)S(1)}, u32[]{:S(2)}, u32[]{:S(2)}) collective-permute-start(bf16[4,4,64,128]{3,2,1,0:T(8,128)(2,1)S(1)} %pad_maximum_fusion.1), channel_id=1, source_target_pairs={{120,0},{124,4},{0,8},{4,12},{8,16},{12,20},{16,24},{20,28},{24,32... | collective-permute-start | bytes 786440 | tf_op jit(solution)/shard_map/ppermute | solution.py:126
  62.0 18.9 %collective-permute-start.7 = (bf16[2,4,64,128]{3,2,1,0:T(8,128)(2,1)S(1)}, bf16[2,4,64,128]{3,2,1,0:T(8,128)(2,1)S(1)}, u32[]{:S(2)}, u32[]{:S(2)}) collective-permute-start(bf16[2,4,64,128]{3,2,1,0:T(8,128)(2,1)S(1)} %get-tuple-element.6), channel_id=1, source_target_pairs={{16,0},{20,4},{24,8},{28,12},{32,16},{36,20},{40,24},{44,28},{48,3... | collective-permute-start | bytes 393224 | tf_op jit(solution)/shard_map/ppermute | solution.py:126
  64.3 16.7 %collective-permute-start.8 = (bf16[2,4,64,128]{3,2,1,0:T(8,128)(2,1)S(1)}, bf16[2,4,64,128]{3,2,1,0:T(8,128)(2,1)S(1)}, u32[]{:S(2)}, u32[]{:S(2)}) collective-permute-start(bf16[2,4,64,128]{3,2,1,0:T(8,128)(2,1)S(1)} %get-tuple-element.5), channel_id=1, source_target_pairs={{112,0},{116,4},{120,8},{124,12},{0,16},{4,20},{8,24},{12,28},{16,... | collective-permute-start | bytes 393224 | tf_op jit(solution)/shard_map/ppermute | solution.py:126
  81.0 45.8 %copy-start.2 = (bf16[16,4,64,128]{3,2,1,0:T(8,128)(2,1)}, bf16[16,4,64,128]{3,2,1,0:T(8,128)(2,1)S(1)}, u32[]{:S(2)}) copy-start(bf16[16,4,64,128]{3,2,1,0:T(8,128)(2,1)S(1)} %constant_dynamic-update-slice_fusion.refs_0_) | copy-start | bytes 3145732
  81.0 19.6 %collective-permute-start.10 = (bf16[16,4,64,128]{3,2,1,0:T(8,128)(2,1)S(1)}, bf16[16,4,64,128]{3,2,1,0:T(8,128)(2,1)S(1)}, u32[]{:S(2)}, u32[]{:S(2)}) collective-permute-start(bf16[16,4,64,128]{3,2,1,0:T(8,128)(2,1)S(1)} %constant_dynamic-update-slice_fusion.refs_0_), channel_id=1, source_target_pairs={{1,0},{2,1},{3,2},{0,3},{5,4},{6,5},{7,6},{4,7},{9,8},{10,9},{11,1... | collective-permute-start | bytes 3145736 | tf_op jit(solution)/shard_map/ppermute | solution.py:126
  81.2 20.3 %collective-permute-start.11 = (bf16[16,4,64,128]{3,2,1,0:T(8,128)(2,1)S(1)}, bf16[16,4,64,128]{3,2,1,0:T(8,128)(2,1)S(1)}, u32[]{:S(2)}, u32[]{:S(2)}) collective-permute-start(bf16[16,4,64,128]{3,2,1,0:T(8,128)(2,1)S(1)} %constant_dynamic-update-slice_fusion.refs_0_), channel_id=1, source_target_pairs={{3,0},{0,1},{1,2},{2,3},{7,4},{4,5},{5,6},{6,7},{11,8},{8,9},{9,10... | collective-permute-start | bytes 3145736 | tf_op jit(solution)/shard_map/ppermute | solution.py:126
  100.7 26.1 %copy-start = (bf16[16,4,64,128]{3,2,1,0:T(8,128)(2,1)}, bf16[16,4,64,128]{3,2,1,0:T(8,128)(2,1)S(1)}, u32[]{:S(2)}) copy-start(bf16[16,4,64,128]{3,2,1,0:T(8,128)(2,1)S(1)} %collective-permute-done.10.refs_1_) | copy-start | bytes 3145732
  100.7 21.1 %collective-permute-start.12 = (bf16[8,4,64,128]{3,2,1,0:T(8,128)(2,1)S(1)}, bf16[8,4,64,128]{3,2,1,0:T(8,128)(2,1)S(1)}, u32[]{:S(2)}, u32[]{:S(2)}) collective-permute-start(bf16[8,4,64,128]{3,2,1,0:T(8,128)(2,1)S(1)} %slice.70), channel_id=1, source_target_pairs={{1,0},{2,1},{3,2},{0,3},{5,4},{6,5},{7,6},{4,7},{9,8},{10,9},{11,1... | collective-permute-start | bytes 1572872 | tf_op jit(solution)/shard_map/ppermute | solution.py:126
  101.5 25.3 %copy-start.1 = (bf16[16,4,64,128]{3,2,1,0:T(8,128)(2,1)}, bf16[16,4,64,128]{3,2,1,0:T(8,128)(2,1)S(1)}, u32[]{:S(2)}) copy-start(bf16[16,4,64,128]{3,2,1,0:T(8,128)(2,1)S(1)} %collective-permute-done.11.refs_2_) | copy-start | bytes 3145732
  101.6 21.0 %collective-permute-start.13 = (bf16[8,4,64,128]{3,2,1,0:T(8,128)(2,1)S(1)}, bf16[8,4,64,128]{3,2,1,0:T(8,128)(2,1)S(1)}, u32[]{:S(2)}, u32[]{:S(2)}) collective-permute-start(bf16[8,4,64,128]{3,2,1,0:T(8,128)(2,1)S(1)} %slice.71), channel_id=1, source_target_pairs={{3,0},{0,1},{1,2},{2,3},{7,4},{4,5},{5,6},{6,7},{11,8},{8,9},{9,10... | collective-permute-start | bytes 1572872 | tf_op jit(solution)/shard_map/ppermute | solution.py:126
  103.4 18.4 %collective-permute-start.19 = (bf16[32,2048]{1,0:T(8,128)(2,1)S(1)}, bf16[32,2048]{1,0:T(8,128)(2,1)S(1)}, u32[]{:S(2)}, u32[]{:S(2)}) collective-permute-start(bf16[32,2048]{1,0:T(8,128)(2,1)S(1)} %slice.63), channel_id=1, source_target_pairs={{0,1},{1,2},{2,3},{3,4},{4,5},{5,6},{6,7},{7,8},{8,9},{9,10},{10,1... | collective-permute-start | bytes 393224 | tf_op jit(solution)/shard_map/ppermute | solution.py:136
  106.3 17.6 %collective-permute-start.14 = (bf16[16,4,64,128]{3,2,1,0:T(8,128)(2,1)S(1)}, bf16[16,4,64,128]{3,2,1,0:T(8,128)(2,1)S(1)}, u32[]{:S(2)}, u32[]{:S(2)}) collective-permute-start(bf16[16,4,64,128]{3,2,1,0:T(8,128)(2,1)S(1)} %constant_dynamic-update-slice_fusion.refs_0_), channel_id=1, source_target_pairs={{4,0},{0,4},{12,8},{8,12},{20,16},{16,20},{28,24},{24,28},{36,32},... | collective-permute-start | bytes 3145736 | tf_op jit(solution)/shard_map/ppermute | solution.py:130
  115.2 8.8 %collective-permute-start.15 = (bf16[16,4,64,128]{3,2,1,0:T(8,128)(2,1)S(1)}, bf16[16,4,64,128]{3,2,1,0:T(8,128)(2,1)S(1)}, u32[]{:S(2)}, u32[]{:S(2)}) collective-permute-start(bf16[16,4,64,128]{3,2,1,0:T(8,128)(2,1)S(1)} %collective-permute-done.10.refs_1_), channel_id=1, source_target_pairs={{4,0},{0,4},{12,8},{8,12},{20,16},{16,20},{28,24},{24,28},{36,32},... | collective-permute-start | bytes 3145736 | tf_op jit(solution)/shard_map/ppermute | solution.py:130
  121.8 5.0 %copy-start.10 = (bf16[32,2048]{1,0:T(8,128)(2,1)}, bf16[32,2048]{1,0:T(8,128)(2,1)S(1)}, u32[]{:S(2)}) copy-start(bf16[32,2048]{1,0:T(8,128)(2,1)S(1)} %collective-permute-done.19.refs_10_) | copy-start | bytes 393220
  121.8 2.7 %collective-permute-start.16 = (bf16[16,4,64,128]{3,2,1,0:T(8,128)(2,1)S(1)}, bf16[16,4,64,128]{3,2,1,0:T(8,128)(2,1)S(1)}, u32[]{:S(2)}, u32[]{:S(2)}) collective-permute-start(bf16[16,4,64,128]{3,2,1,0:T(8,128)(2,1)S(1)} %collective-permute-done.11.refs_2_), channel_id=1, source_target_pairs={{4,0},{0,4},{12,8},{8,12},{20,16},{16,20},{28,24},{24,28},{36,32},... | collective-permute-start | bytes 3145736 | tf_op jit(solution)/shard_map/ppermute | solution.py:130
  121.9 4.9 %copy-start.6 = (bf16[8,4,64,128]{3,2,1,0:T(8,128)(2,1)}, bf16[8,4,64,128]{3,2,1,0:T(8,128)(2,1)S(1)}, u32[]{:S(2)}) copy-start(bf16[8,4,64,128]{3,2,1,0:T(8,128)(2,1)S(1)} %collective-permute-done.12.refs_3_) | copy-start | bytes 1572868
  121.9 3.4 %collective-permute-start.17 = (bf16[8,4,64,128]{3,2,1,0:T(8,128)(2,1)S(1)}, bf16[8,4,64,128]{3,2,1,0:T(8,128)(2,1)S(1)}, u32[]{:S(2)}, u32[]{:S(2)}) collective-permute-start(bf16[8,4,64,128]{3,2,1,0:T(8,128)(2,1)S(1)} %collective-permute-done.12.refs_3_), channel_id=1, source_target_pairs={{4,0},{0,4},{12,8},{8,12},{20,16},{16,20},{28,24},{24,28},{36,32},... | collective-permute-start | bytes 1572872 | tf_op jit(solution)/shard_map/ppermute | solution.py:130
  122.5 4.3 %copy-start.7 = (bf16[8,4,64,128]{3,2,1,0:T(8,128)(2,1)}, bf16[8,4,64,128]{3,2,1,0:T(8,128)(2,1)S(1)}, u32[]{:S(2)}) copy-start(bf16[8,4,64,128]{3,2,1,0:T(8,128)(2,1)S(1)} %collective-permute-done.13.refs_4_) | copy-start | bytes 1572868
  122.5 3.5 %collective-permute-start.18 = (bf16[8,4,64,128]{3,2,1,0:T(8,128)(2,1)S(1)}, bf16[8,4,64,128]{3,2,1,0:T(8,128)(2,1)S(1)}, u32[]{:S(2)}, u32[]{:S(2)}) collective-permute-start(bf16[8,4,64,128]{3,2,1,0:T(8,128)(2,1)S(1)} %collective-permute-done.13.refs_4_), channel_id=1, source_target_pairs={{4,0},{0,4},{12,8},{8,12},{20,16},{16,20},{28,24},{24,28},{36,32},... | collective-permute-start | bytes 1572872 | tf_op jit(solution)/shard_map/ppermute | solution.py:130
  124.0 2.9 %copy-start.3 = (bf16[16,4,64,128]{3,2,1,0:T(8,128)(2,1)}, bf16[16,4,64,128]{3,2,1,0:T(8,128)(2,1)S(1)}, u32[]{:S(2)}) copy-start(bf16[16,4,64,128]{3,2,1,0:T(8,128)(2,1)S(1)} %collective-permute-done.14.refs_5_) | copy-start | bytes 3145732
  124.0 2.9 %copy-start.4 = (bf16[16,4,64,128]{3,2,1,0:T(8,128)(2,1)}, bf16[16,4,64,128]{3,2,1,0:T(8,128)(2,1)S(1)}, u32[]{:S(2)}) copy-start(bf16[16,4,64,128]{3,2,1,0:T(8,128)(2,1)S(1)} %collective-permute-done.15.refs_6_) | copy-start | bytes 3145732
  124.5 2.4 %copy-start.5 = (bf16[16,4,64,128]{3,2,1,0:T(8,128)(2,1)}, bf16[16,4,64,128]{3,2,1,0:T(8,128)(2,1)S(1)}, u32[]{:S(2)}) copy-start(bf16[16,4,64,128]{3,2,1,0:T(8,128)(2,1)S(1)} %collective-permute-done.16.refs_7_) | copy-start | bytes 3145732
  125.3 1.6 copy-start.8
  126.0 0.8 copy-start.9
Sparse Core Ops, SparseCore 0:
  18.9 103.1 all-gather.2

commit v2 on v1

v2 whole, which is shorter than its diff:
```python
import jax
import jax.numpy as jnp
from jax import lax
from jax.experimental import pallas as pl
from jax.experimental.pallas import tpu as pltpu
from jax.sharding import PartitionSpec as P


epsilon = 1e-06
HALO = 32
TILES = 2
MATS = 4
MAT_ORDER = (1, 2, 0, 3)


def rms(values_f):
    return lax.rsqrt(jnp.mean(values_f * values_f, axis=-1, keepdims=True) + epsilon)


def nt_dot(a, b):
    return lax.dot_general(a, b, (((1,), (1,)), ((), ())), preferred_element_type=jnp.float32)


def normed(values_f, gain):
    return values_f * rms(values_f) * gain


def layer_body(stream, hidden, weights, taps, gain_post, conv_ref, branch_ref):
    rows = stream.shape[0]
    kernel_size = taps.shape[0]
    project = lambda m: jnp.dot(hidden, weights(m), preferred_element_type=jnp.float32).astype(jnp.bfloat16)
    gate_c = project(1)
    values = project(2)
    product = (gate_c.astype(jnp.float32) * values.astype(jnp.float32)).astype(jnp.bfloat16)
    conv_ref[pl.ds(8, rows), :] = product.astype(jnp.float32)
    convolved = taps[0:1] * conv_ref[pl.ds(8 - kernel_size + 1, rows), :]
    for k in range(1, kernel_size):
        convolved = convolved + taps[k : k + 1] * conv_ref[pl.ds(8 - kernel_size + 1 + k, rows), :]
    gate_b = project(0)
    weighted = (gate_b.astype(jnp.float32) * convolved).astype(jnp.bfloat16)
    conv_ref[0:8, :] = conv_ref[pl.ds(rows, 8), :]
    branch_ref[...] = nt_dot(weighted, weights(3))
    return (stream.astype(jnp.float32) + normed(branch_ref[...], gain_post)).astype(jnp.bfloat16)


def mixer(copies, groups, sources, gain_pre, taps, gain_post, stream_parts, dims, out_rows):
    d, dc, sp, block_rows = dims
    total = sum(p.shape[0] for p in stream_parts)
    tile = total // TILES
    skip = total - out_rows
    n_src, n_parts = len(sources), len(stream_parts)

    def kernel(*refs):
        src = refs[:n_src]
        parts = refs[n_src : n_src + n_parts]
        pre_ref, taps_ref, post_ref, out_ref = refs[n_src + n_parts : n_src + n_parts + 4]
        w_ref, x_ref, h_ref, conv_ref, branch_ref, res_ref, w_sem, x_sem, o_sem = refs[n_src + n_parts + 4 :]

        def part_copies():
            start = 0
            for k, p in enumerate(parts):
                yield pltpu.make_async_copy(p, x_ref.at[pl.ds(start, p.shape[0])], x_sem.at[k])
                start += p.shape[0]

        for c in part_copies():
            c.start()
        copies(src, w_ref, w_sem)
        conv_ref[0:8, :] = jnp.zeros((8, dc), jnp.float32)
        for c in part_copies():
            c.wait()

        def rows_of(i):
            return pl.ds(pl.multiple_of(i * tile, 16), tile)

        def norm_step(i, carry):
            h_ref[rows_of(i), :] = normed(x_ref[rows_of(i), :].astype(jnp.float32), pre_ref[...]).astype(jnp.bfloat16)
            return carry

        lax.fori_loop(0, TILES, norm_step, 0)

        def arrive(i, m):
            if groups == 1 and m == MAT_ORDER[0]:
                pl.when(i == 0)(lambda: pltpu.make_async_copy(w_ref, w_ref, w_sem.at[0]).wait())
            if groups > 1:
                copy = pltpu.make_async_copy(w_ref.at[m], w_ref.at[m], w_sem.at[MAT_ORDER.index(m)])
                pl.when(i == 0)(lambda: copy.wait())

        def out_copy(i):
            first = skip if i == 0 else 0
            n = tile - first
            return pltpu.make_async_copy(
                res_ref.at[i, pl.ds(first, n)], out_ref.at[pl.ds(i * tile - skip + first, n)], o_sem.at[i]
            )

        def step(i, carry):
            def weights(m):
                arrive(i, m)
                return w_ref[m].reshape(d, dc)

            res_ref[i] = layer_body(
                x_ref[rows_of(i), :],
                h_ref[rows_of(i), :],
                weights,
                taps_ref[...],
                post_ref[...],
                conv_ref,
                branch_ref,
            )
            for k in range(TILES):
                pl.when(i == k)(lambda k=k: out_copy(k).start())
            return carry

        lax.fori_loop(0, TILES, step, 0)
        for i in range(TILES):
            out_copy(i).wait()

    hbm = pl.BlockSpec(memory_space=pltpu.MemorySpace.HBM)
    vmem = pl.BlockSpec(memory_space=pltpu.MemorySpace.VMEM)
    return pl.pallas_call(
        kernel,
        out_shape=jax.ShapeDtypeStruct((out_rows, d), jnp.bfloat16),
        in_specs=[hbm] * (n_src + n_parts) + [vmem] * 3,
        out_specs=hbm,
        scratch_shapes=[
            pltpu.VMEM((MATS, sp, block_rows, dc), jnp.bfloat16),
            pltpu.VMEM((total, d), jnp.bfloat16),
            pltpu.VMEM((total, d), jnp.bfloat16),
            pltpu.VMEM((tile + 8, dc), jnp.float32),
            pltpu.VMEM((tile, d), jnp.float32),
            pltpu.VMEM((TILES, tile, d), jnp.bfloat16),
            pltpu.SemaphoreType.DMA((groups,)),
            pltpu.SemaphoreType.DMA((n_parts,)),
            pltpu.SemaphoreType.DMA((TILES,)),
        ],
        cost_estimate=pl.CostEstimate(
            flops=2 * MATS * total * d * dc, transcendentals=0, bytes_accessed=2 * (MATS * d * dc + 2 * total * d)
        ),
        compiler_params=pltpu.CompilerParams(vmem_limit_bytes=56 * 2**20),
    )(*sources, *stream_parts, gain_pre, taps, gain_post)


def turned(size, stride, distance):
    n = size // stride
    return [(((i // stride + distance) % n) * stride + i % stride, i) for i in range(size)]


def receive(value, axis, distance, stride=1):
    return lax.ppermute(value, axis, turned(lax.axis_size(axis), stride, distance))


def other_core(value):
    return lax.ppermute(value, "sp", [(i ^ 1, i) for i in range(lax.axis_size("sp"))])


def early_halo(tokens):
    axes = ("sp", "tp")
    total = lax.axis_size(axes)
    return lax.ppermute(tokens[-HALO:], axes, [(i - 1, i) for i in range(1, total)])


def on_device(tokens, gain_pre, gain_post, w_b, w_c, w_x, taps, w_out):
    layer_total, block_rows, block_cols = w_b.shape
    sp, tp = lax.axis_size("sp"), lax.axis_size("tp")
    d, dc = sp * block_rows, tp * block_cols
    dims = (d, dc, sp, block_rows)
    chips = sp // 2
    half = chips // 2
    quarter = chips // 4
    z = lambda value, distance: receive(value, "sp", distance, 2)
    x = lambda value, distance: receive(value, "tp", distance)
    own = [jnp.stack([w_b[l], w_c[l], w_x[l], w_out[l].T]) for l in range(layer_total)]

    share = MATS // 2
    places = [(0, 0), (1, 0), (-1, 0), (2, 0), (2, half)]

    along = jnp.stack([own[1]] + [x(own[1], k) for k in range(1, tp)])
    gathered = lax.all_gather(along, "sp", axis=0)
    part = lax.dynamic_slice_in_dim(own[0], share * (lax.axis_index("grp") % 2), share)
    one = jnp.stack([part, z(part, quarter), z(part, 2 * quarter), z(part, -quarter)])
    wrap = jnp.stack([one[3], one[0]])
    kept = jnp.concatenate([one, z(one, 1), z(one[:2], 2), z(wrap, -2), z(one, -1)])

    def along_tp(two):
        ahead = x(two, 1)
        behind = x(two, -1)
        theirs = [other_core(two)]
        far_a = x(ahead[:half], 1)
        far_b = x(behind[half:], -1)
        mine = [two, ahead, behind, far_a, far_b]
        theirs += [other_core(value) for value in mine[1:]]
        return mine + theirs

    other = lax.ppermute(kept, "grp", [(i ^ 1, i) for i in range(lax.axis_size("grp"))])
    halo = early_halo(tokens)
    pieces = along_tp(kept) + along_tp(other)

    def first_copies(src, w_ref, w_sem):
        here_sp, here_tp, parity = lax.axis_index("sp"), lax.axis_index("tp"), lax.axis_index("grp") % 2
        chip, core = here_sp // 2, here_sp % 2
        for n, ref in enumerate(src):
            second, side, p = n // (2 * len(places)), n // len(places) % 2, n % len(places)
            column, begin = places[p]
            mats = pl.ds(share * (parity if second == 0 else 1 - parity), share)
            side_core = core if side == 0 else 1 - core
            lanes = pl.multiple_of(((here_tp + column + tp) % tp) * block_cols, block_cols)

            def start(k, carry):
                place = begin + k
                step = place // 4
                offset = quarter * (place % 4) + jnp.where(step == 3, -1, step)
                row = ((chip + offset + chips) % chips) * 2 + side_core
                target = w_ref.at[mats, row, :, pl.ds(lanes, block_cols)]
                pltpu.make_async_copy(ref.at[k], target, w_sem.at[0]).start()
                return carry

            lax.fori_loop(0, ref.shape[0], start, 0)

    def last_copies(src, w_ref, w_sem):
        here_tp = lax.axis_index("tp")
        for group, m in enumerate(MAT_ORDER):
            for k in range(tp):
                lanes = pl.multiple_of(((here_tp + k) % tp) * block_cols, block_cols)
                target = w_ref.at[m, :, :, pl.ds(lanes, block_cols)]
                pltpu.make_async_copy(src[0].at[:, k, m], target, w_sem.at[group]).start()

    row_of = lambda a, l: a[l][None, :]
    rows = tokens.shape[0]
    stream = mixer(
        first_copies, 1, pieces, row_of(gain_pre, 0), taps[0], row_of(gain_post, 0),
        [halo, tokens], dims, rows + HALO,
    )
    return mixer(
        last_copies, MATS, [gathered], row_of(gain_pre, 1), taps[1], row_of(gain_post, 1),
        [stream], dims, rows,
    )


def solution(mesh):
    placed = (
        P(("grp", "sp", "tp"), None),
        P(),
        P(),
        P(None, "sp", "tp"),
        P(None, "sp", "tp"),
        P(None, "sp", "tp"),
        P(),
        P(None, "tp", "sp"),
    )
    return jax.shard_map(
        on_device,
        mesh=mesh,
        in_specs=placed,
        out_specs=P(("grp", "sp", "tp"), None),
        check_vma=False,
    )
```

time: 167 us -> 161 us (0.964)
  waiting for transfers between devices: 54.7 us -> 37.9 us
  starting transfers between devices: 59 us -> 68.3 us
    ppermute x14 -> x19, waiting for transfers between devices: 46.1 us -> 32.8 us  [the longest x18 32.8 us: receive(): lax.ppermute(value, axis, turned(lax.axis_size(axis), stride, distance))]
    ppermute x5 -> x10, starting transfers between devices: 9.81 us -> 17.2 us  [other_core(): lax.ppermute(value, 'sp', [(i ^ 1, i) for i in range(lax.axis_size('sp'))])]
    ppermute x14 -> x19, starting transfers between devices: 46.3 us -> 48.9 us  [the longest x18 47.7 us: receive(): lax.ppermute(value, axis, turned(lax.axis_size(axis), stride, distance))]
    ppermute x1, waiting for transfers between devices: 6.47 us -> 4.48 us  [early_halo(): lax.ppermute(tokens[-HALO:], axes, [(i - 1, i) for i in range(1, total)])]
  transfers between devices with their start and end apart: 21 -> 31, of which waited for: 12 -> 13; matrix products, arithmetic and copies ran while one was open for 2% -> 2% of each run, Pallas kernels for 9% -> 11%
where the time goes in v2:
time: 161 us; the launch traced here: 159 us
  starting transfers between devices  68.3 us (42%)
  waiting for transfers between devices  37.9 us (24%)
  Pallas kernels  32.5 us (20%)
  between operations  13.8 us (9%)
  local copies, waits for them, and re-layouts  6.07 us (4%)
    ppermute x18, starting transfers between devices, receive(): lax.ppermute(value, axis, turned(lax.axis_size(axis), stride, distance))  47.7 us
    ppermute x18, waiting for transfers between devices, receive(): lax.ppermute(value, axis, turned(lax.axis_size(axis), stride, distance))  32.8 us
    pallas_call x2, Pallas kernels, mixer(): pl.pallas_call(kernel, out_shape=jax.ShapeDtypeStruct((out_rows, d), jnp....  32.5 us
    ppermute x10, starting transfers between devices, other_core(): lax.ppermute(value, 'sp', [(i ^ 1, i) for i in range(lax.axis_size('sp'))])  17.2 us
    ppermute x1, waiting for transfers between devices, early_halo(): lax.ppermute(tokens[-HALO:], axes, [(i - 1, i) for i in range(1, total)])  4.48 us
  transfers between devices with their start and end apart: 31, of which 13 were waited for; matrix products, arithmetic and copies ran while one was open for 2% of the time, Pallas kernels for 11%

profile of v2, /device:TPU:33, one launch (start us, length us, event | category | flops | bytes accessed | tf_op | source)
XLA Modules:
  0.0 159.4 jit_solution(13483460901339967232)
XLA Ops:
  6.6 0.8 fusion.7
  7.3 0.7 slice_bitcast_fusion
  8.1 0.8 fusion.5
  8.9 3.8 %collective-permute-start = (bf16[4,64,128]{2,1,0:T(8,128)(2,1)S(1)}, bf16[4,64,128]{2,1,0:T(8,128)(2,1)S(1)}, u32[]{:S(2)}, u32[]{:S(2)}) collective-permute-start(bf16[4,64,128]{2,1,0:T(8,128)(2,1)S(1)} %get-tuple-element.8), channel_id=1, source_target_pairs={{1,0},{2,1},{3,2},{0,3},{5,4},{6,5},{7,6},{4,7},{9,8},{10,9},{11,1... | collective-permute-start | bytes 196616 | tf_op jit(solution)/shard_map/ppermute | solution.py:148
  12.7 0.3 collective-permute-start.1
  13.0 0.7 collective-permute-start.2
  13.7 0.3 collective-permute-done
  14.0 3.4 %collective-permute-done.1 = bf16[4,64,128]{2,1,0:T(8,128)(2,1)S(1)} collective-permute-done((bf16[4,64,128]{2,1,0:T(8,128)(2,1)S(1)}, bf16[4,64,128]{2,1,0:T(8,128)(2,1)S(1)}, u32[]{:S(2)}, u32[]{:S(2)}) %collective-permute-start.1) | collective-permute-done | bytes 65568 | tf_op jit(solution)/shard_map/ppermute | solution.py:148
  17.4 0.6 collective-permute-done.2
  18.0 0.7 pad_maximum_fusion
  18.7 0.1 all-gather.3.cloned.1.call-update
  18.9 21.3 %collective-permute-start.3 = (bf16[2,64,128]{2,1,0:T(8,128)(2,1)S(1)}, bf16[2,64,128]{2,1,0:T(8,128)(2,1)S(1)}, u32[]{:S(2)}, u32[]{:S(2)}) collective-permute-start(bf16[2,64,128]{2,1,0:T(8,128)(2,1)S(1)} %get-tuple-element.6), channel_id=1, source_target_pairs={{32,0},{36,4},{40,8},{44,12},{48,16},{52,20},{56,24},{60,28},{64,3... | collective-permute-start | bytes 98312 | tf_op jit(solution)/shard_map/ppermute | solution.py:148
  40.2 5.2 %collective-permute-start.5 = (bf16[2,64,128]{2,1,0:T(8,128)(2,1)S(1)}, bf16[2,64,128]{2,1,0:T(8,128)(2,1)S(1)}, u32[]{:S(2)}, u32[]{:S(2)}) collective-permute-start(bf16[2,64,128]{2,1,0:T(8,128)(2,1)S(1)} %get-tuple-element.6), channel_id=1, source_target_pairs={{96,0},{100,4},{104,8},{108,12},{112,16},{116,20},{120,24},{124,28... | collective-permute-start | bytes 98312 | tf_op jit(solution)/shard_map/ppermute | solution.py:148
  45.4 6.3 %collective-permute-done.4 = bf16[2,64,128]{2,1,0:T(8,128)(2,1)S(1)} collective-permute-done((bf16[2,64,128]{2,1,0:T(8,128)(2,1)S(1)}, bf16[2,64,128]{2,1,0:T(8,128)(2,1)S(1)}, u32[]{:S(2)}, u32[]{:S(2)}) %collective-permute-start.4) | collective-permute-done | bytes 32800 | tf_op jit(solution)/shard_map/ppermute | solution.py:148
  51.7 0.0 collective-permute-done.5
  51.8 3.4 %collective-permute-start.6 = (bf16[4,2,64,128]{3,2,1,0:T(8,128)(2,1)S(1)}, bf16[4,2,64,128]{3,2,1,0:T(8,128)(2,1)S(1)}, u32[]{:S(2)}, u32[]{:S(2)}) collective-permute-start(bf16[4,2,64,128]{3,2,1,0:T(8,128)(2,1)S(1)} %pad_maximum_fusion.1), channel_id=1, source_target_pairs={{8,0},{12,4},{16,8},{20,12},{24,16},{28,20},{32,24},{36,28},{40,32... | collective-permute-start | bytes 393224 | tf_op jit(solution)/shard_map/ppermute | solution.py:148
  55.2 0.0 collective-permute-start.9
  55.2 1.4 collective-permute-start.7
  56.6 1.0 collective-permute-start.8
  57.7 1.7 %collective-permute-done.6 = bf16[4,2,64,128]{3,2,1,0:T(8,128)(2,1)S(1)} collective-permute-done((bf16[4,2,64,128]{3,2,1,0:T(8,128)(2,1)S(1)}, bf16[4,2,64,128]{3,2,1,0:T(8,128)(2,1)S(1)}, u32[]{:S(2)}, u32[]{:S(2)}) %collective-permute-start.6) | collective-permute-done | bytes 131104 | tf_op jit(solution)/shard_map/ppermute | solution.py:148
  59.5 3.0 %collective-permute-done.7 = bf16[2,2,64,128]{3,2,1,0:T(8,128)(2,1)S(1)} collective-permute-done((bf16[2,2,64,128]{3,2,1,0:T(8,128)(2,1)S(1)}, bf16[2,2,64,128]{3,2,1,0:T(8,128)(2,1)S(1)}, u32[]{:S(2)}, u32[]{:S(2)}) %collective-permute-start.7) | collective-permute-done | bytes 65568 | tf_op jit(solution)/shard_map/ppermute | solution.py:148
  62.4 1.9 %collective-permute-done.8 = bf16[2,2,64,128]{3,2,1,0:T(8,128)(2,1)S(1)} collective-permute-done((bf16[2,2,64,128]{3,2,1,0:T(8,128)(2,1)S(1)}, bf16[2,2,64,128]{3,2,1,0:T(8,128)(2,1)S(1)}, u32[]{:S(2)}, u32[]{:S(2)}) %collective-permute-start.8) | collective-permute-done | bytes 65568 | tf_op jit(solution)/shard_map/ppermute | solution.py:148
  64.4 0.0 collective-permute-done.9
  64.4 0.0 copy-start.7
  64.4 1.1 collective-permute-start.19
  65.6 0.9 collective-permute-start.10
  66.5 0.5 collective-permute-start.11
  67.0 7.0 %collective-permute-start.14 = (bf16[16,2,64,128]{3,2,1,0:T(8,128)(2,1)S(1)}, bf16[16,2,64,128]{3,2,1,0:T(8,128)(2,1)S(1)}, u32[]{:S(2)}, u32[]{:S(2)}) collective-permute-start(bf16[16,2,64,128]{3,2,1,0:T(8,128)(2,1)S(1)} %constant_dynamic-update-slice_fusion.refs_0_), channel_id=1, source_target_pairs={{4,0},{0,4},{12,8},{8,12},{20,16},{16,20},{28,24},{24,28},{36,32},... | collective-permute-start | bytes 1572872 | tf_op jit(solution)/shard_map/ppermute | solution.py:152
  74.0 0.9 slice.71
  75.0 2.2 %collective-permute-start.29 = (bf16[32,2048]{1,0:T(8,128)(2,1)S(1)}, bf16[32,2048]{1,0:T(8,128)(2,1)}, u32[]{:S(2)}, u32[]{:S(2)}) collective-permute-start(bf16[32,2048]{1,0:T(8,128)(2,1)S(1)} %slice.71), channel_id=1, source_target_pairs={{0,1},{1,2},{2,3},{3,4},{4,5},{5,6},{6,7},{7,8},{8,9},{9,10},{10,1... | collective-permute-start | bytes 393224 | tf_op jit(solution)/shard_map/ppermute | solution.py:158
  77.2 4.0 %collective-permute-start.20 = (bf16[16,2,64,128]{3,2,1,0:T(8,128)(2,1)S(1)}, bf16[16,2,64,128]{3,2,1,0:T(8,128)(2,1)S(1)}, u32[]{:S(2)}, u32[]{:S(2)}) collective-permute-start(bf16[16,2,64,128]{3,2,1,0:T(8,128)(2,1)S(1)} %collective-permute-done.19.refs_10_), channel_id=1, source_target_pairs={{1,0},{2,1},{3,2},{0,3},{5,4},{6,5},{7,6},{4,7},{9,8},{10,9},{11,1... | collective-permute-start | bytes 1572872 | tf_op jit(solution)/shard_map/ppermute | solution.py:148
  81.2 4.5 %collective-permute-done.29.refs_20_ = bf16[32,2048]{1,0:T(8,128)(2,1)} collective-permute-done((bf16[32,2048]{1,0:T(8,128)(2,1)S(1)}, bf16[32,2048]{1,0:T(8,128)(2,1)}, u32[]{:S(2)}, u32[]{:S(2)}) %collective-permute-start.29) | collective-permute-done | bytes 131104 | tf_op jit(solution)/shard_map/ppermute | solution.py:158
  85.7 0.0 collective-permute-start.21
  85.7 1.2 collective-permute-start.15
  86.9 0.1 collective-permute-start.16
  87.0 0.0 collective-permute-done.14.refs_5_
  87.0 0.4 collective-permute-start.24
  87.5 4.9 %collective-permute-done.20.refs_11_ = bf16[16,2,64,128]{3,2,1,0:T(8,128)(2,1)S(1)} collective-permute-done((bf16[16,2,64,128]{3,2,1,0:T(8,128)(2,1)S(1)}, bf16[16,2,64,128]{3,2,1,0:T(8,128)(2,1)S(1)}, u32[]{:S(2)}, u32[]{:S(2)}) %collective-permute-start.20) | collective-permute-done | bytes 524320 | tf_op jit(solution)/shard_map/ppermute | solution.py:148
  92.3 3.5 %collective-permute-start.12 = (bf16[8,2,64,128]{3,2,1,0:T(8,128)(2,1)S(1)}, bf16[8,2,64,128]{3,2,1,0:T(8,128)(2,1)S(1)}, u32[]{:S(2)}, u32[]{:S(2)}) collective-permute-start(bf16[8,2,64,128]{3,2,1,0:T(8,128)(2,1)S(1)} %slice.78), channel_id=1, source_target_pairs={{1,0},{2,1},{3,2},{0,3},{5,4},{6,5},{7,6},{4,7},{9,8},{10,9},{11,1... | collective-permute-start | bytes 786440 | tf_op jit(solution)/shard_map/ppermute | solution.py:148
  95.8 3.8 %collective-permute-done.21.refs_12_ = bf16[16,2,64,128]{3,2,1,0:T(8,128)(2,1)S(1)} collective-permute-done((bf16[16,2,64,128]{3,2,1,0:T(8,128)(2,1)S(1)}, bf16[16,2,64,128]{3,2,1,0:T(8,128)(2,1)S(1)}, u32[]{:S(2)}, u32[]{:S(2)}) %collective-permute-start.21) | collective-permute-done | bytes 524320 | tf_op jit(solution)/shard_map/ppermute | solution.py:148
  99.7 2.2 %collective-permute-done.12.refs_3_ = bf16[8,2,64,128]{3,2,1,0:T(8,128)(2,1)S(1)} collective-permute-done((bf16[8,2,64,128]{3,2,1,0:T(8,128)(2,1)S(1)}, bf16[8,2,64,128]{3,2,1,0:T(8,128)(2,1)S(1)}, u32[]{:S(2)}, u32[]{:S(2)}) %collective-permute-start.12) | collective-permute-done | bytes 262176 | tf_op jit(solution)/shard_map/ppermute | solution.py:148
  101.9 0.5 collective-permute-start.17
  102.4 4.7 %collective-permute-done.13.refs_4_ = bf16[8,2,64,128]{3,2,1,0:T(8,128)(2,1)S(1)} collective-permute-done((bf16[8,2,64,128]{3,2,1,0:T(8,128)(2,1)S(1)}, bf16[8,2,64,128]{3,2,1,0:T(8,128)(2,1)S(1)}, u32[]{:S(2)}, u32[]{:S(2)}) %collective-permute-start.13) | collective-permute-done | bytes 262176 | tf_op jit(solution)/shard_map/ppermute | solution.py:148
  107.1 0.0 collective-permute-start.22
  107.1 1.5 collective-permute-start.23
  108.6 3.0 %collective-permute-start.25 = (bf16[16,2,64,128]{3,2,1,0:T(8,128)(2,1)S(1)}, bf16[16,2,64,128]{3,2,1,0:T(8,128)(2,1)S(1)}, u32[]{:S(2)}, u32[]{:S(2)}) collective-permute-start(bf16[16,2,64,128]{3,2,1,0:T(8,128)(2,1)S(1)} %collective-permute-done.20.refs_11_), channel_id=1, source_target_pairs={{4,0},{0,4},{12,8},{8,12},{20,16},{16,20},{28,24},{24,28},{36,32},... | collective-permute-start | bytes 1572872 | tf_op jit(solution)/shard_map/ppermute | solution.py:152
  111.6 0.0 collective-permute-done.24.refs_15_
  111.6 0.1 collective-permute-start.26
  111.8 0.7 fusion.8
  112.4 0.4 collective-permute-start.18
  112.9 0.0 collective-permute-done.22.refs_13_
  112.9 3.1 %collective-permute-start.27 = (bf16[8,2,64,128]{3,2,1,0:T(8,128)(2,1)S(1)}, bf16[8,2,64,128]{3,2,1,0:T(8,128)(2,1)S(1)}, u32[]{:S(2)}, u32[]{:S(2)}) collective-permute-start(bf16[8,2,64,128]{3,2,1,0:T(8,128)(2,1)S(1)} %collective-permute-done.22.refs_13_), channel_id=1, source_target_pairs={{4,0},{0,4},{12,8},{8,12},{20,16},{16,20},{28,24},{24,28},{36,32},... | collective-permute-start | bytes 786440 | tf_op jit(solution)/shard_map/ppermute | solution.py:152
  115.9 0.0 collective-permute-done.23.refs_14_
  115.9 1.3 collective-permute-start.28
  117.3 0.6 copy_bitcast_fusion
  117.9 0.0 collective-permute-done.18.refs_9_
  117.9 0.0 collective-permute-done.27.refs_18_
  117.9 0.5 collective-permute-done.28.refs_19_
  118.5 0.7 copy-done.22
  119.3 0.1 copy-done.13
  119.3 0.6 copy-done.14
  119.9 17.0 %shard_map.82.refs_1_ = bf16[800,2048]{1,0:T(8,128)(2,1)} custom-call(bf16[16,2,64,128]{3,2,1,0:T(8,128)(2,1)} %copy-done.7, bf16[16,2,64,128]{3,2,1,0:T(8,128)(2,1)} %copy-done, bf16[16,2,64,128]{3,2,1,0:T(8,128)(2,1)} %copy-done.1, bf16[8,2,64,128]{3,2,1,0:T(8,128)(2,1)} %copy-done.15, bf16[8,2,64,128]{3,2,1,0:T(8,128)(2,1)} %copy-done.16, ...), custom_call_target="tpu_custom_call" | custom-call | flops 6710886400 | bytes 14942208 | tf_op jit(solution)/shard_map/pallas_call | solution.py:119
  136.9 0.0 all-gather.3.cloned.1.call-done
  137.0 15.5 %shard_map.83 = bf16[768,2048]{1,0:T(8,128)(2,1)} custom-call(bf16[32,4,4,64,128]{4,3,2,1,0:T(8,128)(2,1)} %bitcast.40, bf16[800,2048]{1,0:T(8,128)(2,1)} %shard_map.82.refs_1_, f32[1,2048]{1,0:T(1,128)} %get-tuple-element.30.refs_2_, f32[3,512]{1,0:T(4,128)} %get-tuple-element.27.refs_3_, f32[1,2048]{1,0:T(1,128)} %get-tuple-element.19.refs_4_), custom_call_target="tpu_custom_call" | custom-call | flops 6710886400 | bytes 14942208 | tf_op jit(solution)/shard_map/pallas_call | solution.py:119
  (70 shorter events, 0.4 us)
Async XLA Ops:
  6.5 105.2 %copy-start.4 = (f32[2,2048]{1,0:T(2,128)S(1)}, f32[2,2048]{1,0:T(2,128)}, u32[]{:S(2)}) copy-start(f32[2,2048]{1,0:T(2,128)} %param.10) | copy-start | bytes 49156
  6.5 105.2 %copy-start.5 = (f32[2,2048]{1,0:T(2,128)S(1)}, f32[2,2048]{1,0:T(2,128)}, u32[]{:S(2)}) copy-start(f32[2,2048]{1,0:T(2,128)} %param.9) | copy-start | bytes 49156
  6.6 110.7 %copy-start.6 = (f32[2,3,512]{2,0,1:T(2,128)S(1)}, f32[2,3,512]{2,0,1:T(2,128)}, u32[]{:S(2)}) copy-start(f32[2,3,512]{2,0,1:T(2,128)} %param.14) | copy-start | bytes 36868
  6.6 130.4 %all-gather.3.cloned.1.call-start = ((), (), s32[]{:S(2)}) async-start(), calls=%async_computation | async-start | bytes 8650752 | tf_op jit(solution)/shard_map/all_gather | solution.py:177
  8.9 5.1 %collective-permute-start = (bf16[4,64,128]{2,1,0:T(8,128)(2,1)S(1)}, bf16[4,64,128]{2,1,0:T(8,128)(2,1)S(1)}, u32[]{:S(2)}, u32[]{:S(2)}) collective-permute-start(bf16[4,64,128]{2,1,0:T(8,128)(2,1)S(1)} %get-tuple-element.8), channel_id=1, source_target_pairs={{1,0},{2,1},{3,2},{0,3},{5,4},{6,5},{7,6},{4,7},{9,8},{10,9},{11,1... | collective-permute-start | bytes 196616 | tf_op jit(solution)/shard_map/ppermute | solution.py:148
  12.7 4.7 %collective-permute-start.1 = (bf16[4,64,128]{2,1,0:T(8,128)(2,1)S(1)}, bf16[4,64,128]{2,1,0:T(8,128)(2,1)S(1)}, u32[]{:S(2)}, u32[]{:S(2)}) collective-permute-start(bf16[4,64,128]{2,1,0:T(8,128)(2,1)S(1)} %get-tuple-element.8), channel_id=1, source_target_pairs={{2,0},{3,1},{0,2},{1,3},{6,4},{7,5},{4,6},{5,7},{10,8},{11,9},{8,1... | collective-permute-start | bytes 196616 | tf_op jit(solution)/shard_map/ppermute | solution.py:148
  13.0 5.0 %collective-permute-start.2 = (bf16[4,64,128]{2,1,0:T(8,128)(2,1)S(1)}, bf16[4,64,128]{2,1,0:T(8,128)(2,1)S(1)}, u32[]{:S(2)}, u32[]{:S(2)}) collective-permute-start(bf16[4,64,128]{2,1,0:T(8,128)(2,1)S(1)} %get-tuple-element.8), channel_id=1, source_target_pairs={{3,0},{0,1},{1,2},{2,3},{7,4},{4,5},{5,6},{6,7},{11,8},{8,9},{9,10... | collective-permute-start | bytes 196616 | tf_op jit(solution)/shard_map/ppermute | solution.py:148
  18.9 26.5 %collective-permute-start.3 = (bf16[2,64,128]{2,1,0:T(8,128)(2,1)S(1)}, bf16[2,64,128]{2,1,0:T(8,128)(2,1)S(1)}, u32[]{:S(2)}, u32[]{:S(2)}) collective-permute-start(bf16[2,64,128]{2,1,0:T(8,128)(2,1)S(1)} %get-tuple-element.6), channel_id=1, source_target_pairs={{32,0},{36,4},{40,8},{44,12},{48,16},{52,20},{56,24},{60,28},{64,3... | collective-permute-start | bytes 98312 | tf_op jit(solution)/shard_map/ppermute | solution.py:148
  40.1 11.6 %collective-permute-start.4 = (bf16[2,64,128]{2,1,0:T(8,128)(2,1)S(1)}, bf16[2,64,128]{2,1,0:T(8,128)(2,1)S(1)}, u32[]{:S(2)}, u32[]{:S(2)}) collective-permute-start(bf16[2,64,128]{2,1,0:T(8,128)(2,1)S(1)} %get-tuple-element.6), channel_id=1, source_target_pairs={{64,0},{68,4},{72,8},{76,12},{80,16},{84,20},{88,24},{92,28},{96,3... | collective-permute-start | bytes 98312 | tf_op jit(solution)/shard_map/ppermute | solution.py:148
  40.2 11.6 %collective-permute-start.5 = (bf16[2,64,128]{2,1,0:T(8,128)(2,1)S(1)}, bf16[2,64,128]{2,1,0:T(8,128)(2,1)S(1)}, u32[]{:S(2)}, u32[]{:S(2)}) collective-permute-start(bf16[2,64,128]{2,1,0:T(8,128)(2,1)S(1)} %get-tuple-element.6), channel_id=1, source_target_pairs={{96,0},{100,4},{104,8},{108,12},{112,16},{116,20},{120,24},{124,28... | collective-permute-start | bytes 98312 | tf_op jit(solution)/shard_map/ppermute | solution.py:148
  51.8 7.7 %collective-permute-start.6 = (bf16[4,2,64,128]{3,2,1,0:T(8,128)(2,1)S(1)}, bf16[4,2,64,128]{3,2,1,0:T(8,128)(2,1)S(1)}, u32[]{:S(2)}, u32[]{:S(2)}) collective-permute-start(bf16[4,2,64,128]{3,2,1,0:T(8,128)(2,1)S(1)} %pad_maximum_fusion.1), channel_id=1, source_target_pairs={{8,0},{12,4},{16,8},{20,12},{24,16},{28,20},{32,24},{36,28},{40,32... | collective-permute-start | bytes 393224 | tf_op jit(solution)/shard_map/ppermute | solution.py:148
  55.2 9.2 %collective-permute-start.9 = (bf16[4,2,64,128]{3,2,1,0:T(8,128)(2,1)S(1)}, bf16[4,2,64,128]{3,2,1,0:T(8,128)(2,1)S(1)}, u32[]{:S(2)}, u32[]{:S(2)}) collective-permute-start(bf16[4,2,64,128]{3,2,1,0:T(8,128)(2,1)S(1)} %pad_maximum_fusion.1), channel_id=1, source_target_pairs={{120,0},{124,4},{0,8},{4,12},{8,16},{12,20},{16,24},{20,28},{24,32... | collective-permute-start | bytes 393224 | tf_op jit(solution)/shard_map/ppermute | solution.py:148
  55.2 7.2 %collective-permute-start.7 = (bf16[2,2,64,128]{3,2,1,0:T(8,128)(2,1)S(1)}, bf16[2,2,64,128]{3,2,1,0:T(8,128)(2,1)S(1)}, u32[]{:S(2)}, u32[]{:S(2)}) collective-permute-start(bf16[2,2,64,128]{3,2,1,0:T(8,128)(2,1)S(1)} %get-tuple-element.10), channel_id=1, source_target_pairs={{16,0},{20,4},{24,8},{28,12},{32,16},{36,20},{40,24},{44,28},{48,3... | collective-permute-start | bytes 196616 | tf_op jit(solution)/shard_map/ppermute | solution.py:148
  56.6 7.7 %collective-permute-start.8 = (bf16[2,2,64,128]{3,2,1,0:T(8,128)(2,1)S(1)}, bf16[2,2,64,128]{3,2,1,0:T(8,128)(2,1)S(1)}, u32[]{:S(2)}, u32[]{:S(2)}) collective-permute-start(bf16[2,2,64,128]{3,2,1,0:T(8,128)(2,1)S(1)} %get-tuple-element.9), channel_id=1, source_target_pairs={{112,0},{116,4},{120,8},{124,12},{0,16},{4,20},{8,24},{12,28},{16,... | collective-permute-start | bytes 196616 | tf_op jit(solution)/shard_map/ppermute | solution.py:148
  64.4 54.7 %copy-start.7 = (bf16[16,2,64,128]{3,2,1,0:T(8,128)(2,1)}, bf16[16,2,64,128]{3,2,1,0:T(8,128)(2,1)S(1)}, u32[]{:S(2)}) copy-start(bf16[16,2,64,128]{3,2,1,0:T(8,128)(2,1)S(1)} %constant_dynamic-update-slice_fusion.refs_0_) | copy-start | bytes 1572868
  64.4 12.7 %collective-permute-start.19 = (bf16[16,2,64,128]{3,2,1,0:T(8,128)(2,1)S(1)}, bf16[16,2,64,128]{3,2,1,0:T(8,128)(2,1)S(1)}, u32[]{:S(2)}, u32[]{:S(2)}) collective-permute-start(bf16[16,2,64,128]{3,2,1,0:T(8,128)(2,1)S(1)} %constant_dynamic-update-slice_fusion.refs_0_), channel_id=1, source_target_pairs={{128,0},{0,128},{129,1},{1,129},{130,2},{2,130},{131,3},{3,131},{1... | collective-permute-start | bytes 1572872 | tf_op jit(solution)/shard_map/ppermute | solution.py:193
  65.6 20.1 %collective-permute-start.10 = (bf16[16,2,64,128]{3,2,1,0:T(8,128)(2,1)S(1)}, bf16[16,2,64,128]{3,2,1,0:T(8,128)(2,1)S(1)}, u32[]{:S(2)}, u32[]{:S(2)}) collective-permute-start(bf16[16,2,64,128]{3,2,1,0:T(8,128)(2,1)S(1)} %constant_dynamic-update-slice_fusion.refs_0_), channel_id=1, source_target_pairs={{1,0},{2,1},{3,2},{0,3},{5,4},{6,5},{7,6},{4,7},{9,8},{10,9},{11,1... | collective-permute-start | bytes 1572872 | tf_op jit(solution)/shard_map/ppermute | solution.py:148
  66.5 20.4 %collective-permute-start.11 = (bf16[16,2,64,128]{3,2,1,0:T(8,128)(2,1)S(1)}, bf16[16,2,64,128]{3,2,1,0:T(8,128)(2,1)S(1)}, u32[]{:S(2)}, u32[]{:S(2)}) collective-permute-start(bf16[16,2,64,128]{3,2,1,0:T(8,128)(2,1)S(1)} %constant_dynamic-update-slice_fusion.refs_0_), channel_id=1, source_target_pairs={{3,0},{0,1},{1,2},{2,3},{7,4},{4,5},{5,6},{6,7},{11,8},{8,9},{9,10... | collective-permute-start | bytes 1572872 | tf_op jit(solution)/shard_map/ppermute | solution.py:148
  67.0 20.0 %collective-permute-start.14 = (bf16[16,2,64,128]{3,2,1,0:T(8,128)(2,1)S(1)}, bf16[16,2,64,128]{3,2,1,0:T(8,128)(2,1)S(1)}, u32[]{:S(2)}, u32[]{:S(2)}) collective-permute-start(bf16[16,2,64,128]{3,2,1,0:T(8,128)(2,1)S(1)} %constant_dynamic-update-slice_fusion.refs_0_), channel_id=1, source_target_pairs={{4,0},{0,4},{12,8},{8,12},{20,16},{16,20},{28,24},{24,28},{36,32},... | collective-permute-start | bytes 1572872 | tf_op jit(solution)/shard_map/ppermute | solution.py:152
  75.0 10.7 %collective-permute-start.29 = (bf16[32,2048]{1,0:T(8,128)(2,1)S(1)}, bf16[32,2048]{1,0:T(8,128)(2,1)}, u32[]{:S(2)}, u32[]{:S(2)}) collective-permute-start(bf16[32,2048]{1,0:T(8,128)(2,1)S(1)} %slice.71), channel_id=1, source_target_pairs={{0,1},{1,2},{2,3},{3,4},{4,5},{5,6},{6,7},{7,8},{8,9},{9,10},{10,1... | collective-permute-start | bytes 393224 | tf_op jit(solution)/shard_map/ppermute | solution.py:158
  77.2 42.0 %copy-start.8 = (bf16[16,2,64,128]{3,2,1,0:T(8,128)(2,1)}, bf16[16,2,64,128]{3,2,1,0:T(8,128)(2,1)S(1)}, u32[]{:S(2)}) copy-start(bf16[16,2,64,128]{3,2,1,0:T(8,128)(2,1)S(1)} %collective-permute-done.19.refs_10_) | copy-start | bytes 1572868
  77.2 15.1 %collective-permute-start.20 = (bf16[16,2,64,128]{3,2,1,0:T(8,128)(2,1)S(1)}, bf16[16,2,64,128]{3,2,1,0:T(8,128)(2,1)S(1)}, u32[]{:S(2)}, u32[]{:S(2)}) collective-permute-start(bf16[16,2,64,128]{3,2,1,0:T(8,128)(2,1)S(1)} %collective-permute-done.19.refs_10_), channel_id=1, source_target_pairs={{1,0},{2,1},{3,2},{0,3},{5,4},{6,5},{7,6},{4,7},{9,8},{10,9},{11,1... | collective-permute-start | bytes 1572872 | tf_op jit(solution)/shard_map/ppermute | solution.py:148
  85.7 13.9 %collective-permute-start.21 = (bf16[16,2,64,128]{3,2,1,0:T(8,128)(2,1)S(1)}, bf16[16,2,64,128]{3,2,1,0:T(8,128)(2,1)S(1)}, u32[]{:S(2)}, u32[]{:S(2)}) collective-permute-start(bf16[16,2,64,128]{3,2,1,0:T(8,128)(2,1)S(1)} %collective-permute-done.19.refs_10_), channel_id=1, source_target_pairs={{3,0},{0,1},{1,2},{2,3},{7,4},{4,5},{5,6},{6,7},{11,8},{8,9},{9,10... | collective-permute-start | bytes 1572872 | tf_op jit(solution)/shard_map/ppermute | solution.py:148
  85.7 33.4 %copy-start = (bf16[16,2,64,128]{3,2,1,0:T(8,128)(2,1)}, bf16[16,2,64,128]{3,2,1,0:T(8,128)(2,1)S(1)}, u32[]{:S(2)}) copy-start(bf16[16,2,64,128]{3,2,1,0:T(8,128)(2,1)S(1)} %collective-permute-done.10.refs_1_) | copy-start | bytes 1572868
  85.7 21.4 %collective-permute-start.15 = (bf16[16,2,64,128]{3,2,1,0:T(8,128)(2,1)S(1)}, bf16[16,2,64,128]{3,2,1,0:T(8,128)(2,1)S(1)}, u32[]{:S(2)}, u32[]{:S(2)}) collective-permute-start(bf16[16,2,64,128]{3,2,1,0:T(8,128)(2,1)S(1)} %collective-permute-done.10.refs_1_), channel_id=1, source_target_pairs={{4,0},{0,4},{12,8},{8,12},{20,16},{16,20},{28,24},{24,28},{36,32},... | collective-permute-start | bytes 1572872 | tf_op jit(solution)/shard_map/ppermute | solution.py:152
  86.9 32.2 %copy-start.1 = (bf16[16,2,64,128]{3,2,1,0:T(8,128)(2,1)}, bf16[16,2,64,128]{3,2,1,0:T(8,128)(2,1)S(1)}, u32[]{:S(2)}) copy-start(bf16[16,2,64,128]{3,2,1,0:T(8,128)(2,1)S(1)} %collective-permute-done.11.refs_2_) | copy-start | bytes 1572868
  86.9 21.7 %collective-permute-start.16 = (bf16[16,2,64,128]{3,2,1,0:T(8,128)(2,1)S(1)}, bf16[16,2,64,128]{3,2,1,0:T(8,128)(2,1)S(1)}, u32[]{:S(2)}, u32[]{:S(2)}) collective-permute-start(bf16[16,2,64,128]{3,2,1,0:T(8,128)(2,1)S(1)} %collective-permute-done.11.refs_2_), channel_id=1, source_target_pairs={{4,0},{0,4},{12,8},{8,12},{20,16},{16,20},{28,24},{24,28},{36,32},... | collective-permute-start | bytes 1572872 | tf_op jit(solution)/shard_map/ppermute | solution.py:152
  87.0 32.1 %copy-start.9 = (bf16[16,2,64,128]{3,2,1,0:T(8,128)(2,1)}, bf16[16,2,64,128]{3,2,1,0:T(8,128)(2,1)S(1)}, u32[]{:S(2)}) copy-start(bf16[16,2,64,128]{3,2,1,0:T(8,128)(2,1)S(1)} %collective-permute-done.14.refs_5_) | copy-start | bytes 1572868
  87.0 24.6 %collective-permute-start.24 = (bf16[16,2,64,128]{3,2,1,0:T(8,128)(2,1)S(1)}, bf16[16,2,64,128]{3,2,1,0:T(8,128)(2,1)S(1)}, u32[]{:S(2)}, u32[]{:S(2)}) collective-permute-start(bf16[16,2,64,128]{3,2,1,0:T(8,128)(2,1)S(1)} %collective-permute-done.19.refs_10_), channel_id=1, source_target_pairs={{4,0},{0,4},{12,8},{8,12},{20,16},{16,20},{28,24},{24,28},{36,32},... | collective-permute-start | bytes 1572872 | tf_op jit(solution)/shard_map/ppermute | solution.py:152
  92.3 26.8 %copy-start.2 = (bf16[16,2,64,128]{3,2,1,0:T(8,128)(2,1)}, bf16[16,2,64,128]{3,2,1,0:T(8,128)(2,1)S(1)}, u32[]{:S(2)}) copy-start(bf16[16,2,64,128]{3,2,1,0:T(8,128)(2,1)S(1)} %collective-permute-done.20.refs_11_) | copy-start | bytes 1572868
  92.3 9.5 %collective-permute-start.12 = (bf16[8,2,64,128]{3,2,1,0:T(8,128)(2,1)S(1)}, bf16[8,2,64,128]{3,2,1,0:T(8,128)(2,1)S(1)}, u32[]{:S(2)}, u32[]{:S(2)}) collective-permute-start(bf16[8,2,64,128]{3,2,1,0:T(8,128)(2,1)S(1)} %slice.78), channel_id=1, source_target_pairs={{1,0},{2,1},{3,2},{0,3},{5,4},{6,5},{7,6},{4,7},{9,8},{10,9},{11,1... | collective-permute-start | bytes 786440 | tf_op jit(solution)/shard_map/ppermute | solution.py:148
  99.6 19.5 %copy-start.3 = (bf16[16,2,64,128]{3,2,1,0:T(8,128)(2,1)}, bf16[16,2,64,128]{3,2,1,0:T(8,128)(2,1)S(1)}, u32[]{:S(2)}) copy-start(bf16[16,2,64,128]{3,2,1,0:T(8,128)(2,1)S(1)} %collective-permute-done.21.refs_12_) | copy-start | bytes 1572868
  99.6 7.5 %collective-permute-start.13 = (bf16[8,2,64,128]{3,2,1,0:T(8,128)(2,1)S(1)}, bf16[8,2,64,128]{3,2,1,0:T(8,128)(2,1)S(1)}, u32[]{:S(2)}, u32[]{:S(2)}) collective-permute-start(bf16[8,2,64,128]{3,2,1,0:T(8,128)(2,1)S(1)} %slice.79), channel_id=1, source_target_pairs={{3,0},{0,1},{1,2},{2,3},{7,4},{4,5},{5,6},{6,7},{11,8},{8,9},{9,10... | collective-permute-start | bytes 786440 | tf_op jit(solution)/shard_map/ppermute | solution.py:148
  101.9 17.3 %copy-start.15 = (bf16[8,2,64,128]{3,2,1,0:T(8,128)(2,1)}, bf16[8,2,64,128]{3,2,1,0:T(8,128)(2,1)S(1)}, u32[]{:S(2)}) copy-start(bf16[8,2,64,128]{3,2,1,0:T(8,128)(2,1)S(1)} %collective-permute-done.12.refs_3_) | copy-start | bytes 786436
  101.9 10.6 %collective-permute-start.17 = (bf16[8,2,64,128]{3,2,1,0:T(8,128)(2,1)S(1)}, bf16[8,2,64,128]{3,2,1,0:T(8,128)(2,1)S(1)}, u32[]{:S(2)}, u32[]{:S(2)}) collective-permute-start(bf16[8,2,64,128]{3,2,1,0:T(8,128)(2,1)S(1)} %collective-permute-done.12.refs_3_), channel_id=1, source_target_pairs={{4,0},{0,4},{12,8},{8,12},{20,16},{16,20},{28,24},{24,28},{36,32},... | collective-permute-start | bytes 786440 | tf_op jit(solution)/shard_map/ppermute | solution.py:152
  107.1 12.1 %copy-start.16 = (bf16[8,2,64,128]{3,2,1,0:T(8,128)(2,1)}, bf16[8,2,64,128]{3,2,1,0:T(8,128)(2,1)S(1)}, u32[]{:S(2)}) copy-start(bf16[8,2,64,128]{3,2,1,0:T(8,128)(2,1)S(1)} %collective-permute-done.13.refs_4_) | copy-start | bytes 786436
  107.1 5.8 %collective-permute-start.22 = (bf16[8,2,64,128]{3,2,1,0:T(8,128)(2,1)S(1)}, bf16[8,2,64,128]{3,2,1,0:T(8,128)(2,1)S(1)}, u32[]{:S(2)}, u32[]{:S(2)}) collective-permute-start(bf16[8,2,64,128]{3,2,1,0:T(8,128)(2,1)S(1)} %slice.80), channel_id=1, source_target_pairs={{1,0},{2,1},{3,2},{0,3},{5,4},{6,5},{7,6},{4,7},{9,8},{10,9},{11,1... | collective-permute-start | bytes 786440 | tf_op jit(solution)/shard_map/ppermute | solution.py:148
  107.1 12.1 %copy-start.10 = (bf16[16,2,64,128]{3,2,1,0:T(8,128)(2,1)}, bf16[16,2,64,128]{3,2,1,0:T(8,128)(2,1)S(1)}, u32[]{:S(2)}) copy-start(bf16[16,2,64,128]{3,2,1,0:T(8,128)(2,1)S(1)} %collective-permute-done.15.refs_6_) | copy-start | bytes 1572868
  107.1 8.8 %collective-permute-start.23 = (bf16[8,2,64,128]{3,2,1,0:T(8,128)(2,1)S(1)}, bf16[8,2,64,128]{3,2,1,0:T(8,128)(2,1)S(1)}, u32[]{:S(2)}, u32[]{:S(2)}) collective-permute-start(bf16[8,2,64,128]{3,2,1,0:T(8,128)(2,1)S(1)} %slice.81), channel_id=1, source_target_pairs={{3,0},{0,1},{1,2},{2,3},{7,4},{4,5},{5,6},{6,7},{11,8},{8,9},{9,10... | collective-permute-start | bytes 786440 | tf_op jit(solution)/shard_map/ppermute | solution.py:148
  108.6 10.6 %copy-start.11 = (bf16[16,2,64,128]{3,2,1,0:T(8,128)(2,1)}, bf16[16,2,64,128]{3,2,1,0:T(8,128)(2,1)S(1)}, u32[]{:S(2)}) copy-start(bf16[16,2,64,128]{3,2,1,0:T(8,128)(2,1)S(1)} %collective-permute-done.16.refs_7_) | copy-start | bytes 1572868
  108.6 9.9 %collective-permute-start.25 = (bf16[16,2,64,128]{3,2,1,0:T(8,128)(2,1)S(1)}, bf16[16,2,64,128]{3,2,1,0:T(8,128)(2,1)S(1)}, u32[]{:S(2)}, u32[]{:S(2)}) collective-permute-start(bf16[16,2,64,128]{3,2,1,0:T(8,128)(2,1)S(1)} %collective-permute-done.20.refs_11_), channel_id=1, source_target_pairs={{4,0},{0,4},{12,8},{8,12},{20,16},{16,20},{28,24},{24,28},{36,32},... | collective-permute-start | bytes 1572872 | tf_op jit(solution)/shard_map/ppermute | solution.py:152
  111.6 7.6 %copy-start.12 = (bf16[16,2,64,128]{3,2,1,0:T(8,128)(2,1)}, bf16[16,2,64,128]{3,2,1,0:T(8,128)(2,1)S(1)}, u32[]{:S(2)}) copy-start(bf16[16,2,64,128]{3,2,1,0:T(8,128)(2,1)S(1)} %collective-permute-done.24.refs_15_) | copy-start | bytes 1572868
  111.6 6.8 %collective-permute-start.26 = (bf16[16,2,64,128]{3,2,1,0:T(8,128)(2,1)S(1)}, bf16[16,2,64,128]{3,2,1,0:T(8,128)(2,1)S(1)}, u32[]{:S(2)}, u32[]{:S(2)}) collective-permute-start(bf16[16,2,64,128]{3,2,1,0:T(8,128)(2,1)S(1)} %collective-permute-done.21.refs_12_), channel_id=1, source_target_pairs={{4,0},{0,4},{12,8},{8,12},{20,16},{16,20},{28,24},{24,28},{36,32},... | collective-permute-start | bytes 1572872 | tf_op jit(solution)/shard_map/ppermute | solution.py:152
  112.4 6.8 %copy-start.17 = (bf16[8,2,64,128]{3,2,1,0:T(8,128)(2,1)}, bf16[8,2,64,128]{3,2,1,0:T(8,128)(2,1)S(1)}, u32[]{:S(2)}) copy-start(bf16[8,2,64,128]{3,2,1,0:T(8,128)(2,1)S(1)} %collective-permute-done.17.refs_8_) | copy-start | bytes 786436
  112.4 5.5 %collective-permute-start.18 = (bf16[8,2,64,128]{3,2,1,0:T(8,128)(2,1)S(1)}, bf16[8,2,64,128]{3,2,1,0:T(8,128)(2,1)S(1)}, u32[]{:S(2)}, u32[]{:S(2)}) collective-permute-start(bf16[8,2,64,128]{3,2,1,0:T(8,128)(2,1)S(1)} %collective-permute-done.13.refs_4_), channel_id=1, source_target_pairs={{4,0},{0,4},{12,8},{8,12},{20,16},{16,20},{28,24},{24,28},{36,32},... | collective-permute-start | bytes 786440 | tf_op jit(solution)/shard_map/ppermute | solution.py:152
  112.9 6.4 %copy-start.18 = (bf16[8,2,64,128]{3,2,1,0:T(8,128)(2,1)}, bf16[8,2,64,128]{3,2,1,0:T(8,128)(2,1)S(1)}, u32[]{:S(2)}) copy-start(bf16[8,2,64,128]{3,2,1,0:T(8,128)(2,1)S(1)} %collective-permute-done.22.refs_13_) | copy-start | bytes 786436
  112.9 5.0 %collective-permute-start.27 = (bf16[8,2,64,128]{3,2,1,0:T(8,128)(2,1)S(1)}, bf16[8,2,64,128]{3,2,1,0:T(8,128)(2,1)S(1)}, u32[]{:S(2)}, u32[]{:S(2)}) collective-permute-start(bf16[8,2,64,128]{3,2,1,0:T(8,128)(2,1)S(1)} %collective-permute-done.22.refs_13_), channel_id=1, source_target_pairs={{4,0},{0,4},{12,8},{8,12},{20,16},{16,20},{28,24},{24,28},{36,32},... | collective-permute-start | bytes 786440 | tf_op jit(solution)/shard_map/ppermute | solution.py:152
  115.9 3.3 %copy-start.19 = (bf16[8,2,64,128]{3,2,1,0:T(8,128)(2,1)}, bf16[8,2,64,128]{3,2,1,0:T(8,128)(2,1)S(1)}, u32[]{:S(2)}) copy-start(bf16[8,2,64,128]{3,2,1,0:T(8,128)(2,1)S(1)} %collective-permute-done.23.refs_14_) | copy-start | bytes 786436
  115.9 2.5 %collective-permute-start.28 = (bf16[8,2,64,128]{3,2,1,0:T(8,128)(2,1)S(1)}, bf16[8,2,64,128]{3,2,1,0:T(8,128)(2,1)S(1)}, u32[]{:S(2)}, u32[]{:S(2)}) collective-permute-start(bf16[8,2,64,128]{3,2,1,0:T(8,128)(2,1)S(1)} %collective-permute-done.23.refs_14_), channel_id=1, source_target_pairs={{4,0},{0,4},{12,8},{8,12},{20,16},{16,20},{28,24},{24,28},{36,32},... | collective-permute-start | bytes 786440 | tf_op jit(solution)/shard_map/ppermute | solution.py:152
  117.9 1.4 copy-start.20
  117.9 1.4 copy-start.21
  118.4 0.7 copy-start.22
  118.4 0.9 copy-start.13
  119.1 0.8 copy-start.14
Sparse Core Ops, SparseCore 0:
  18.9 95.0 all-gather.2

commit v3 on v2

v3 whole, which is shorter than its diff:
```python
import jax
import jax.numpy as jnp
from jax import lax
from jax.experimental import pallas as pl
from jax.experimental.pallas import tpu as pltpu
from jax.sharding import PartitionSpec as P


epsilon = 1e-06
HALO = 32
CHUNKS = 2
BANDS = 1
MATS = 4


def rms(values_f):
    return lax.rsqrt(jnp.mean(values_f * values_f, axis=-1, keepdims=True) + epsilon)


def nt_dot(a, b):
    return lax.dot_general(a, b, (((1,), (1,)), ((), ())), preferred_element_type=jnp.float32)


def normed(values_f, gain):
    return values_f * rms(values_f) * gain


def normed(values_f, gain):
    return values_f * rms(values_f) * gain


def chunks_of(total):
    size = total // CHUNKS
    return [slice(k * size, (k + 1) * size) for k in range(CHUNKS)]


HBM = pl.BlockSpec(memory_space=pltpu.MemorySpace.HBM)
VMEM = pl.BlockSpec(memory_space=pltpu.MemorySpace.VMEM)


def end_to_end(parts, target, sems):
    start = 0
    for k, p in enumerate(parts):
        yield pltpu.make_async_copy(p, target.at[pl.ds(start, p.shape[0])], sems.at[k])
        start += p.shape[0]


def normed_rows(parts, gain):
    total, d = sum(p.shape[0] for p in parts), parts[0].shape[1]
    n = len(parts)

    def kernel(*refs):
        gain_ref, out_ref, x_ref, h_ref, in_sem, out_sem = refs[n:]
        for c in end_to_end(refs[:n], x_ref, in_sem):
            c.start()
        for c in end_to_end(refs[:n], x_ref, in_sem):
            c.wait()
        stores = []
        for k, rows in enumerate(chunks_of(total)):
            h_ref[rows, :] = normed(x_ref[rows, :].astype(jnp.float32), gain_ref[...]).astype(jnp.bfloat16)
            span = pl.ds(rows.start, rows.stop - rows.start)
            stores.append(pltpu.make_async_copy(h_ref.at[span], out_ref.at[span], out_sem.at[k]))
            stores[-1].start()
        for c in stores:
            c.wait()

    return pl.pallas_call(
        kernel,
        out_shape=jax.ShapeDtypeStruct((total, d), jnp.bfloat16),
        in_specs=[HBM] * n + [VMEM],
        out_specs=HBM,
        scratch_shapes=[
            pltpu.VMEM((total, d), jnp.bfloat16),
            pltpu.VMEM((total, d), jnp.bfloat16),
            pltpu.SemaphoreType.DMA((n,)),
            pltpu.SemaphoreType.DMA((CHUNKS,)),
        ],
        cost_estimate=pl.CostEstimate(flops=8 * total * d, transcendentals=0, bytes_accessed=4 * total * d),
        compiler_params=pltpu.CompilerParams(vmem_limit_bytes=40 * 2**20),
    )(*parts, gain)


def two_mixers(copies, sources, hidden, parts, gain_pre, taps, gain_post, dims, out_rows):
    d, dc, sp, block_rows = dims
    total = hidden.shape[0]
    skip = total - out_rows
    pairs, wide = 2, dc // 2
    kernel_size = taps.shape[1]
    counts = [len(group) for group in sources]
    n_src, n_parts = sum(counts), len(parts)

    def kernel(*refs):
        src = [refs[: counts[0]], refs[counts[0] : n_src]]
        part_refs = refs[n_src : n_src + n_parts]
        hidden_ref, pre_ref, taps_ref, post_ref, out_ref = refs[n_src + n_parts : n_src + n_parts + 5]
        w_ref, x_ref, h_ref, c_ref, conv_ref, w_sem, x_sem, o_sem = refs[n_src + n_parts + 5 :]

        copies[0](src[0], w_ref.at[0], w_sem.at[0])
        for c in end_to_end(part_refs, x_ref, x_sem):
            c.start()
        copies[1](src[1], w_ref.at[1], w_sem.at[1])
        conv_ref[0:8, :] = jnp.zeros((8, dc), jnp.float32)
        chunks = chunks_of(total)
        chunk, band = total // CHUNKS, total // BANDS
        h_ref[...] = hidden_ref[...]

        def out_copy(r):
            first = max(chunks[r].start, skip)
            n = chunks[r].stop - first
            return pltpu.make_async_copy(x_ref.at[pl.ds(first, n)], out_ref.at[pl.ds(first - skip, n)], o_sem.at[r])

        def layer(l, carry):
            def pair_step(pair, carry):
                pltpu.make_async_copy(w_ref.at[l, pair], w_ref.at[l, pair], w_sem.at[l, pair]).wait()
                cols = pl.ds(pl.multiple_of(pair * wide, wide), wide)
                tap = lambda k: taps_ref[l, k : k + 1, cols]
                first = 8 - kernel_size + 1

                def band_step(i, carry):
                    start = pl.multiple_of(i * band, 16)

                    def project(m):
                        return jnp.dot(
                            h_ref[pl.ds(start, band), :], w_ref[l, pair, m].reshape(d, wide),
                            preferred_element_type=jnp.float32,
                        ).astype(jnp.bfloat16)

                    gate_c = project(1)
                    product = (gate_c.astype(jnp.float32) * project(2).astype(jnp.float32)).astype(jnp.bfloat16)
                    conv_ref[pl.ds(start + 8, band), cols] = product.astype(jnp.float32)
                    window = conv_ref[pl.ds(start, band + 8), cols]
                    convolved = tap(0) * window[first : first + band]
                    for k in range(1, kernel_size):
                        convolved = convolved + tap(k) * window[first + k : first + k + band]
                    c_ref[pl.ds(start, band), cols] = (project(0).astype(jnp.float32) * convolved).astype(jnp.bfloat16)
                    return carry

                return lax.fori_loop(0, BANDS, band_step, carry)

            lax.fori_loop(0, pairs, pair_step, 0)

            @pl.when(l == 0)
            def _():
                for c in end_to_end(part_refs, x_ref, x_sem):
                    c.wait()

            next_gain = pre_ref[pl.ds(jnp.minimum(l + 1, 1), 1), :]

            def chunk_step(r, carry):
                rows = pl.ds(pl.multiple_of(r * chunk, 16), chunk)
                back = jnp.concatenate([w_ref[l, p, 3].reshape(d, wide) for p in range(pairs)], axis=1)
                branch = nt_dot(c_ref[rows, :], back)
                stream = x_ref[rows, :].astype(jnp.float32) + normed(branch, post_ref[pl.ds(l, 1), :])
                rounded = stream.astype(jnp.bfloat16)
                x_ref[rows, :] = rounded
                h_ref[rows, :] = normed(rounded.astype(jnp.float32), next_gain).astype(jnp.bfloat16)
                for k in range(CHUNKS):
                    pl.when((l == 1) & (r == k))(lambda k=k: out_copy(k).start())
                return carry

            return lax.fori_loop(0, CHUNKS, chunk_step, carry)

        lax.fori_loop(0, 2, layer, 0)
        for r in range(CHUNKS):
            out_copy(r).wait()

    return pl.pallas_call(
        kernel,
        out_shape=jax.ShapeDtypeStruct((out_rows, d), jnp.bfloat16),
        in_specs=[HBM] * (n_src + n_parts) + [VMEM] * 4,
        out_specs=HBM,
        scratch_shapes=[
            pltpu.VMEM((2, pairs, MATS, sp, block_rows, wide), jnp.bfloat16),
            pltpu.VMEM((total, d), jnp.bfloat16),
            pltpu.VMEM((total, d), jnp.bfloat16),
            pltpu.VMEM((total, dc), jnp.bfloat16),
            pltpu.VMEM((total + 8, dc), jnp.float32),
            pltpu.SemaphoreType.DMA((2, pairs)),
            pltpu.SemaphoreType.DMA((n_parts,)),
            pltpu.SemaphoreType.DMA((CHUNKS,)),
        ],
        cost_estimate=pl.CostEstimate(
            flops=4 * MATS * total * d * dc, transcendentals=0, bytes_accessed=4 * MATS * d * dc + 6 * total * d
        ),
        compiler_params=pltpu.CompilerParams(vmem_limit_bytes=56 * 2**20),
    )(*sources[0], *sources[1], *parts, hidden, gain_pre, taps, gain_post)


def turned(size, stride, distance):
    n = size // stride
    return [(((i // stride + distance) % n) * stride + i % stride, i) for i in range(size)]


def receive(value, axis, distance, stride=1):
    return lax.ppermute(value, axis, turned(lax.axis_size(axis), stride, distance))


def other_core(value):
    return lax.ppermute(value, "sp", [(i ^ 1, i) for i in range(lax.axis_size("sp"))])


def early_halo(tokens):
    axes = ("sp", "tp")
    total = lax.axis_size(axes)
    return lax.ppermute(tokens[-HALO:], axes, [(i - 1, i) for i in range(1, total)])


def on_device(tokens, gain_pre, gain_post, w_b, w_c, w_x, taps, w_out):
    layer_total, block_rows, block_cols = w_b.shape
    sp, tp = lax.axis_size("sp"), lax.axis_size("tp")
    d, dc = sp * block_rows, tp * block_cols
    dims = (d, dc, sp, block_rows)
    chips = sp // 2
    half = chips // 2
    quarter = chips // 4
    z = lambda value, distance: receive(value, "sp", distance, 2)
    x = lambda value, distance: receive(value, "tp", distance)
    own = [jnp.stack([w_b[l], w_c[l], w_x[l], w_out[l].T]) for l in range(layer_total)]

    share = MATS // 2
    places = [(0, 0), (1, 0), (-1, 0), (2, 0), (2, half)]

    along = jnp.stack([own[1]] + [x(own[1], k) for k in range(1, tp)])
    gathered = lax.all_gather(along, "sp", axis=0)
    part = lax.dynamic_slice_in_dim(own[0], share * (lax.axis_index("grp") % 2), share)
    one = jnp.stack([part, z(part, quarter), z(part, 2 * quarter), z(part, -quarter)])
    wrap = jnp.stack([one[3], one[0]])
    kept = jnp.concatenate([one, z(one, 1), z(one[:2], 2), z(wrap, -2), z(one, -1)])

    def along_tp(two):
        ahead = x(two, 1)
        behind = x(two, -1)
        theirs = [other_core(two)]
        far_a = x(ahead[:half], 1)
        far_b = x(behind[half:], -1)
        mine = [two, ahead, behind, far_a, far_b]
        theirs += [other_core(value) for value in mine[1:]]
        return mine + theirs

    other = lax.ppermute(kept, "grp", [(i ^ 1, i) for i in range(lax.axis_size("grp"))])
    halo = early_halo(tokens)
    pieces = along_tp(kept) + along_tp(other)

    columns = ((0, 1, tp - 1, 2), tuple(range(tp)))

    def first_copies(src, w_ref, sems):
        here_sp, parity = lax.axis_index("sp"), lax.axis_index("grp") % 2
        chip, core = here_sp // 2, here_sp % 2

        def put(n):
            ref = src[n]
            second, side, p = n // (2 * len(places)), n // len(places) % 2, n % len(places)
            column, begin = places[p]
            place_of = columns[0].index(column % tp)
            pair, lanes = place_of // 2, pl.ds(place_of % 2 * block_cols, block_cols)
            mats = pl.ds(share * (parity if second == 0 else 1 - parity), share)
            side_core = core if side == 0 else 1 - core

            def start(k, carry):
                place = begin + k
                step = place // 4
                offset = quarter * (place % 4) + jnp.where(step == 3, -1, step)
                row = ((chip + offset + chips) % chips) * 2 + side_core
                target = w_ref.at[pair, mats, row, :, lanes]
                pltpu.make_async_copy(ref.at[k], target, sems.at[pair]).start()
                return carry

            lax.fori_loop(0, ref.shape[0], start, 0)

        for column in columns[0]:
            for n in range(len(src)):
                if places[n % len(places)][0] % tp == column:
                    put(n)

    def last_copies(src, w_ref, sems):
        for k in range(tp):
            for m in range(MATS):
                target = w_ref.at[k // 2, m, :, :, pl.ds(k % 2 * block_cols, block_cols)]
                pltpu.make_async_copy(src[0].at[:, k, m], target, sems.at[k // 2]).start()

    def own_order(rows, order):
        here = lax.axis_index("tp")
        return jnp.concatenate(
            [
                lax.dynamic_slice_in_dim(rows, (here + column) % tp * block_cols, block_cols, 1)
                for column in order
            ],
            axis=1,
        )

    own_taps = jnp.stack([own_order(taps[l], columns[l]) for l in range(layer_total)])
    parts = [halo, tokens]
    hidden = normed_rows(parts, gain_pre[0][None, :])
    return two_mixers(
        [first_copies, last_copies], [pieces, [gathered]], hidden, parts, gain_pre, own_taps, gain_post,
        dims, tokens.shape[0],
    )


def solution(mesh):
    placed = (
        P(("grp", "sp", "tp"), None),
        P(),
        P(),
        P(None, "sp", "tp"),
        P(None, "sp", "tp"),
        P(None, "sp", "tp"),
        P(),
        P(None, "tp", "sp"),
    )
    return jax.shard_map(
        on_device,
        mesh=mesh,
        in_specs=placed,
        out_specs=P(("grp", "sp", "tp"), None),
        check_vma=False,
    )
```

time: 161 us -> 165 us (1.025)
  local copies, waits for them, and re-layouts: 6.07 us -> 11.4 us
  Pallas kernels: 32.5 us -> 30.8 us
    ppermute x1, waiting for transfers between devices: 4.48 us -> 12.8 us  [early_halo(): lax.ppermute(tokens[-HALO:], axes, [(i - 1, i) for i in range(1, total)])]
    ppermute x18, waiting for transfers between devices: 32.8 us -> 24.6 us  [receive(): lax.ppermute(value, axis, turned(lax.axis_size(axis), stride, distance))]
    ppermute x18, starting transfers between devices: 47.7 us -> 53.9 us  [receive(): lax.ppermute(value, axis, turned(lax.axis_size(axis), stride, distance))]
    ppermute x10, starting transfers between devices: 17.2 us -> 11 us  [other_core(): lax.ppermute(value, 'sp', [(i ^ 1, i) for i in range(lax.axis_size('sp'))])]
    unnamed x52 -> x46, local copies, waits for them, and re-layouts: 1.48 us -> 4.53 us
    pallas_call x2, Pallas kernels: 32.5 us -> 30.8 us  [the longest x1 28.7 us: two_mixers(): pl.pallas_call(kernel, out_shape=jax.ShapeDtypeStruct((out_rows, d), jnp....]
  transfers between devices with their start and end apart: 31 -> 31, of which waited for: 13 -> 13; matrix products, arithmetic and copies ran while one was open for 2% -> 3% of each run, Pallas kernels for 11% -> 1%
where the time goes in v3:
time: 165 us; the launch traced here: 164 us
  starting transfers between devices  69.4 us (42%)
  waiting for transfers between devices  37.5 us (23%)
  Pallas kernels  30.8 us (19%)
  between operations  13.9 us (8%)
  local copies, waits for them, and re-layouts  11.4 us (7%)
    ppermute x18, starting transfers between devices, receive(): lax.ppermute(value, axis, turned(lax.axis_size(axis), stride, distance))  53.9 us
    pallas_call x1, Pallas kernels, two_mixers(): pl.pallas_call(kernel, out_shape=jax.ShapeDtypeStruct((out_rows, d), jnp....  28.7 us
    ppermute x18, waiting for transfers between devices, receive(): lax.ppermute(value, axis, turned(lax.axis_size(axis), stride, distance))  24.6 us
    ppermute x1, waiting for transfers between devices, early_halo(): lax.ppermute(tokens[-HALO:], axes, [(i - 1, i) for i in range(1, total)])  12.8 us
    ppermute x10, starting transfers between devices, other_core(): lax.ppermute(value, 'sp', [(i ^ 1, i) for i in range(lax.axis_size('sp'))])  11 us
    unnamed x46, local copies, waits for them, and re-layouts  4.53 us
  transfers between devices with their start and end apart: 31, of which 13 were waited for; matrix products, arithmetic and copies ran while one was open for 3% of the time, Pallas kernels for 1%

profile of v3, /device:TPU:33, one launch (start us, length us, event | category | flops | bytes accessed | tf_op | source)
XLA Modules:
  0.0 164.4 jit_solution(2448064482746613007)
XLA Ops:
  6.6 0.9 fusion.7
  7.4 0.8 slice_bitcast_fusion
  8.3 0.8 fusion.5
  9.1 4.0 %collective-permute-start.27 = (bf16[4,64,128]{2,1,0:T(8,128)(2,1)S(1)}, bf16[4,64,128]{2,1,0:T(8,128)(2,1)S(1)}, u32[]{:S(2)}, u32[]{:S(2)}) collective-permute-start(bf16[4,64,128]{2,1,0:T(8,128)(2,1)S(1)} %get-tuple-element.8), channel_id=1, source_target_pairs={{2,0},{3,1},{0,2},{1,3},{6,4},{7,5},{4,6},{5,7},{10,8},{11,9},{8,1... | collective-permute-start | bytes 196616 | tf_op jit(solution)/shard_map/ppermute | solution.py:195
  13.0 0.7 collective-permute-start.26
  13.7 0.7 collective-permute-start.28
  14.5 0.2 collective-permute-done.27
  14.7 2.1 %collective-permute-done.26 = bf16[4,64,128]{2,1,0:T(8,128)(2,1)S(1)} collective-permute-done((bf16[4,64,128]{2,1,0:T(8,128)(2,1)S(1)}, bf16[4,64,128]{2,1,0:T(8,128)(2,1)S(1)}, u32[]{:S(2)}, u32[]{:S(2)}) %collective-permute-start.26) | collective-permute-done | bytes 65568 | tf_op jit(solution)/shard_map/ppermute | solution.py:195
  16.8 1.3 collective-permute-done.28
  18.1 0.7 pad_maximum_fusion
  18.8 0.1 all-gather.3.cloned.1.call-update
  18.9 0.0 copy-start.5
  18.9 20.5 %collective-permute-start.1 = (bf16[2,64,128]{2,1,0:T(8,128)(2,1)S(1)}, bf16[2,64,128]{2,1,0:T(8,128)(2,1)S(1)}, u32[]{:S(2)}, u32[]{:S(2)}) collective-permute-start(bf16[2,64,128]{2,1,0:T(8,128)(2,1)S(1)} %get-tuple-element.6), channel_id=1, source_target_pairs={{64,0},{68,4},{72,8},{76,12},{80,16},{84,20},{88,24},{92,28},{96,3... | collective-permute-start | bytes 98312 | tf_op jit(solution)/shard_map/ppermute | solution.py:195
  39.5 0.6 collective-permute-start
  40.0 5.0 %collective-permute-start.2 = (bf16[2,64,128]{2,1,0:T(8,128)(2,1)S(1)}, bf16[2,64,128]{2,1,0:T(8,128)(2,1)S(1)}, u32[]{:S(2)}, u32[]{:S(2)}) collective-permute-start(bf16[2,64,128]{2,1,0:T(8,128)(2,1)S(1)} %get-tuple-element.6), channel_id=1, source_target_pairs={{96,0},{100,4},{104,8},{108,12},{112,16},{116,20},{120,24},{124,28... | collective-permute-start | bytes 98312 | tf_op jit(solution)/shard_map/ppermute | solution.py:195
  45.0 0.0 collective-permute-done.1
  45.0 1.3 collective-permute-done
  46.3 0.7 collective-permute-done.2
  47.0 1.5 collective-permute-start.6
  48.5 5.5 %collective-permute-start.3 = (bf16[4,2,64,128]{3,2,1,0:T(8,128)(2,1)S(1)}, bf16[4,2,64,128]{3,2,1,0:T(8,128)(2,1)S(1)}, u32[]{:S(2)}, u32[]{:S(2)}) collective-permute-start(bf16[4,2,64,128]{3,2,1,0:T(8,128)(2,1)S(1)} %pad_maximum_fusion.1), channel_id=1, source_target_pairs={{8,0},{12,4},{16,8},{20,12},{24,16},{28,20},{32,24},{36,28},{40,32... | collective-permute-start | bytes 393224 | tf_op jit(solution)/shard_map/ppermute | solution.py:195
  54.0 0.1 collective-permute-start.5
  54.1 3.5 %collective-permute-start.4 = (bf16[2,2,64,128]{3,2,1,0:T(8,128)(2,1)S(1)}, bf16[2,2,64,128]{3,2,1,0:T(8,128)(2,1)S(1)}, u32[]{:S(2)}, u32[]{:S(2)}) collective-permute-start(bf16[2,2,64,128]{3,2,1,0:T(8,128)(2,1)S(1)} %get-tuple-element.18), channel_id=1, source_target_pairs={{16,0},{20,4},{24,8},{28,12},{32,16},{36,20},{40,24},{44,28},{48,3... | collective-permute-start | bytes 196616 | tf_op jit(solution)/shard_map/ppermute | solution.py:195
  57.7 0.6 collective-permute-done.3
  58.3 2.9 %collective-permute-done.4 = bf16[2,2,64,128]{3,2,1,0:T(8,128)(2,1)S(1)} collective-permute-done((bf16[2,2,64,128]{3,2,1,0:T(8,128)(2,1)S(1)}, bf16[2,2,64,128]{3,2,1,0:T(8,128)(2,1)S(1)}, u32[]{:S(2)}, u32[]{:S(2)}) %collective-permute-start.4) | collective-permute-done | bytes 65568 | tf_op jit(solution)/shard_map/ppermute | solution.py:195
  61.2 2.0 %collective-permute-done.5 = bf16[2,2,64,128]{3,2,1,0:T(8,128)(2,1)S(1)} collective-permute-done((bf16[2,2,64,128]{3,2,1,0:T(8,128)(2,1)S(1)}, bf16[2,2,64,128]{3,2,1,0:T(8,128)(2,1)S(1)}, u32[]{:S(2)}, u32[]{:S(2)}) %collective-permute-start.5) | collective-permute-done | bytes 65568 | tf_op jit(solution)/shard_map/ppermute | solution.py:195
  63.3 2.5 %collective-permute-start.16 = (bf16[16,2,64,128]{3,2,1,0:T(8,128)(2,1)S(1)}, bf16[16,2,64,128]{3,2,1,0:T(8,128)(2,1)S(1)}, u32[]{:S(2)}, u32[]{:S(2)}) collective-permute-start(bf16[16,2,64,128]{3,2,1,0:T(8,128)(2,1)S(1)} %constant_dynamic-update-slice_fusion.refs_0_), channel_id=1, source_target_pairs={{128,0},{0,128},{129,1},{1,129},{130,2},{2,130},{131,3},{3,131},{1... | collective-permute-start | bytes 1572872 | tf_op jit(solution)/shard_map/ppermute | solution.py:240
  65.8 5.6 %collective-permute-start.11 = (bf16[16,2,64,128]{3,2,1,0:T(8,128)(2,1)S(1)}, bf16[16,2,64,128]{3,2,1,0:T(8,128)(2,1)S(1)}, u32[]{:S(2)}, u32[]{:S(2)}) collective-permute-start(bf16[16,2,64,128]{3,2,1,0:T(8,128)(2,1)S(1)} %constant_dynamic-update-slice_fusion.refs_0_), channel_id=1, source_target_pairs={{4,0},{0,4},{12,8},{8,12},{20,16},{16,20},{28,24},{24,28},{36,32},... | collective-permute-start | bytes 1572872 | tf_op jit(solution)/shard_map/ppermute | solution.py:199
  71.4 2.7 %collective-permute-start.7 = (bf16[16,2,64,128]{3,2,1,0:T(8,128)(2,1)S(1)}, bf16[16,2,64,128]{3,2,1,0:T(8,128)(2,1)S(1)}, u32[]{:S(2)}, u32[]{:S(2)}) collective-permute-start(bf16[16,2,64,128]{3,2,1,0:T(8,128)(2,1)S(1)} %constant_dynamic-update-slice_fusion.refs_0_), channel_id=1, source_target_pairs={{1,0},{2,1},{3,2},{0,3},{5,4},{6,5},{7,6},{4,7},{9,8},{10,9},{11,1... | collective-permute-start | bytes 1572872 | tf_op jit(solution)/shard_map/ppermute | solution.py:195
  74.0 0.9 slice.62
  75.0 2.0 %collective-permute-start.29 = (bf16[32,2048]{1,0:T(8,128)(2,1)S(1)}, bf16[32,2048]{1,0:T(8,128)(2,1)S(1)}, u32[]{:S(2)}, u32[]{:S(2)}) collective-permute-start(bf16[32,2048]{1,0:T(8,128)(2,1)S(1)} %slice.62), channel_id=1, source_target_pairs={{0,1},{1,2},{2,3},{3,4},{4,5},{5,6},{6,7},{7,8},{8,9},{9,10},{10,1... | collective-permute-start | bytes 393224 | tf_op jit(solution)/shard_map/ppermute | solution.py:205
  76.9 0.1 collective-permute-start.18
  77.1 12.8 %collective-permute-done.29.refs_0_.refs_21_ = bf16[32,2048]{1,0:T(8,128)(2,1)S(1)} collective-permute-done((bf16[32,2048]{1,0:T(8,128)(2,1)S(1)}, bf16[32,2048]{1,0:T(8,128)(2,1)S(1)}, u32[]{:S(2)}, u32[]{:S(2)}) %collective-permute-start.29) | collective-permute-done | bytes 131104 | tf_op jit(solution)/shard_map/ppermute | solution.py:205
  89.9 0.0 collective-permute-start.17
  89.9 0.0 collective-permute-done.11.refs_5_
  89.9 0.1 collective-permute-start.21
  90.1 0.5 collective-permute-start.13
  90.6 0.0 collective-permute-done.7.refs_1_
  90.6 0.3 collective-permute-start.12
  90.9 6.5 %collective-permute-done.18.refs_12_ = bf16[16,2,64,128]{3,2,1,0:T(8,128)(2,1)} collective-permute-done((bf16[16,2,64,128]{3,2,1,0:T(8,128)(2,1)S(1)}, bf16[16,2,64,128]{3,2,1,0:T(8,128)(2,1)}, u32[]{:S(2)}, u32[]{:S(2)}) %collective-permute-start.18) | collective-permute-done | bytes 524320 | tf_op jit(solution)/shard_map/ppermute | solution.py:195
  97.4 1.9 %collective-permute-start.10 = (bf16[8,2,64,128]{3,2,1,0:T(8,128)(2,1)S(1)}, bf16[8,2,64,128]{3,2,1,0:T(8,128)(2,1)}, u32[]{:S(2)}, u32[]{:S(2)}) collective-permute-start(bf16[8,2,64,128]{3,2,1,0:T(8,128)(2,1)S(1)} %slice.67), channel_id=1, source_target_pairs={{3,0},{0,1},{1,2},{2,3},{7,4},{4,5},{5,6},{6,7},{11,8},{8,9},{9,10... | collective-permute-start | bytes 786440 | tf_op jit(solution)/shard_map/ppermute | solution.py:195
  99.3 2.4 %collective-permute-done.17.refs_11_ = bf16[16,2,64,128]{3,2,1,0:T(8,128)(2,1)} collective-permute-done((bf16[16,2,64,128]{3,2,1,0:T(8,128)(2,1)S(1)}, bf16[16,2,64,128]{3,2,1,0:T(8,128)(2,1)}, u32[]{:S(2)}, u32[]{:S(2)}) %collective-permute-start.17) | collective-permute-done | bytes 524320 | tf_op jit(solution)/shard_map/ppermute | solution.py:195
  101.6 3.5 %collective-permute-start.9 = (bf16[8,2,64,128]{3,2,1,0:T(8,128)(2,1)S(1)}, bf16[8,2,64,128]{3,2,1,0:T(8,128)(2,1)S(1)}, u32[]{:S(2)}, u32[]{:S(2)}) collective-permute-start(bf16[8,2,64,128]{3,2,1,0:T(8,128)(2,1)S(1)} %slice.66), channel_id=1, source_target_pairs={{1,0},{2,1},{3,2},{0,3},{5,4},{6,5},{7,6},{4,7},{9,8},{10,9},{11,1... | collective-permute-start | bytes 786440 | tf_op jit(solution)/shard_map/ppermute | solution.py:195
  105.1 1.7 %slice.69 = bf16[8,2,64,128]{3,2,1,0:T(8,128)(2,1)} slice(bf16[16,2,64,128]{3,2,1,0:T(8,128)(2,1)} %collective-permute-done.18.refs_12_), slice={[8:16], [0:2], [0:64], [0:128]} | slice | bytes 524288 | tf_op jit(solution)/shard_map/slice | solution.py:235
  106.8 1.0 slice.68
  107.8 0.0 collective-permute-done.10.refs_4_
  107.8 0.9 collective-permute-start.15
  108.7 1.7 %collective-permute-done.9.refs_3_ = bf16[8,2,64,128]{3,2,1,0:T(8,128)(2,1)S(1)} collective-permute-done((bf16[8,2,64,128]{3,2,1,0:T(8,128)(2,1)S(1)}, bf16[8,2,64,128]{3,2,1,0:T(8,128)(2,1)S(1)}, u32[]{:S(2)}, u32[]{:S(2)}) %collective-permute-start.9) | collective-permute-done | bytes 262176 | tf_op jit(solution)/shard_map/ppermute | solution.py:195
  110.4 3.6 %collective-permute-start.19 = (bf16[8,2,64,128]{3,2,1,0:T(8,128)(2,1)S(1)}, bf16[8,2,64,128]{3,2,1,0:T(8,128)(2,1)}, u32[]{:S(2)}, u32[]{:S(2)}) collective-permute-start(bf16[8,2,64,128]{3,2,1,0:T(8,128)(2,1)S(1)} %slice.68), channel_id=1, source_target_pairs={{1,0},{2,1},{3,2},{0,3},{5,4},{6,5},{7,6},{4,7},{9,8},{10,9},{11,1... | collective-permute-start | bytes 786440 | tf_op jit(solution)/shard_map/ppermute | solution.py:195
  114.1 1.6 collective-permute-start.23
  115.6 0.2 collective-permute-start.22
  115.8 0.6 copy-done.11
  116.6 0.2 collective-permute-start.14
  116.8 3.0 %collective-permute-done.20.refs_14_ = bf16[8,2,64,128]{3,2,1,0:T(8,128)(2,1)} collective-permute-done((bf16[8,2,64,128]{3,2,1,0:T(8,128)(2,1)}, bf16[8,2,64,128]{3,2,1,0:T(8,128)(2,1)}, u32[]{:S(2)}, u32[]{:S(2)}) %collective-permute-start.20) | collective-permute-done | bytes 262176 | tf_op jit(solution)/shard_map/ppermute | solution.py:195
  119.8 1.7 %collective-permute-start.25 = (bf16[8,2,64,128]{3,2,1,0:T(8,128)(2,1)}, bf16[8,2,64,128]{3,2,1,0:T(8,128)(2,1)S(1)}, u32[]{:S(2)}, u32[]{:S(2)}) collective-permute-start(bf16[8,2,64,128]{3,2,1,0:T(8,128)(2,1)} %collective-permute-done.20.refs_14_), channel_id=1, source_target_pairs={{4,0},{0,4},{12,8},{8,12},{20,16},{16,20},{28,24},{24,28},{36,32},... | collective-permute-start | bytes 786440 | tf_op jit(solution)/shard_map/ppermute | solution.py:199
  121.5 0.0 collective-permute-start.24
  121.5 0.7 slice.63.refs_2_
  122.3 0.6 pad_maximum_fusion.5.refs_25_
  122.9 2.1 %shard_map.82.refs_23_ = bf16[800,2048]{1,0:T(8,128)(2,1)S(1)} custom-call(bf16[32,2048]{1,0:T(8,128)(2,1)S(1)} %collective-permute-done.29.refs_0_.refs_21_, bf16[768,2048]{1,0:T(8,128)(2,1)S(1)} %copy-done, f32[1,2048]{1,0:T(1,128)S(1)} %slice.63.refs_2_), custom_call_target="tpu_custom_call" | custom-call | flops 13107200 | bytes 6553600 | tf_op jit(solution)/shard_map/pallas_call | solution.py:67
  125.0 1.7 %copy-done.1 = bf16[800,2048]{1,0:T(8,128)(2,1)} copy-done((bf16[800,2048]{1,0:T(8,128)(2,1)}, bf16[800,2048]{1,0:T(8,128)(2,1)S(1)}, u32[]{:S(2)}) %copy-start.1) | copy-done | bytes 3276824
  126.7 0.7 copy-done.13
  127.4 0.7 copy-done.14
  128.1 0.0 all-gather.3.cloned.1.call-done
  128.1 0.6 copy-done.15
  128.8 28.7 %shard_map.83 = bf16[768,2048]{1,0:T(8,128)(2,1)} custom-call(bf16[16,2,64,128]{3,2,1,0:T(8,128)(2,1)} %copy-done.6, bf16[16,2,64,128]{3,2,1,0:T(8,128)(2,1)} %copy-done.4, bf16[16,2,64,128]{3,2,1,0:T(8,128)(2,1)} %copy-done.3, bf16[8,2,64,128]{3,2,1,0:T(8,128)(2,1)} %copy-done.12, bf16[8,2,64,128]{3,2,1,0:T(8,128)(2,1)} %collective-permute-done.10.refs_4_, ...), custom_call_target="tpu_custom_call" | custom-call | flops 13421772800 | bytes 26607616 | tf_op jit(solution)/shard_map/pallas_call | solution.py:167
  (67 shorter events, 0.4 us)
Async XLA Ops:
  6.5 116.3 %copy-start = (bf16[768,2048]{1,0:T(8,128)(2,1)S(1)}, bf16[768,2048]{1,0:T(8,128)(2,1)}, u32[]{:S(2)}) copy-start(bf16[768,2048]{1,0:T(8,128)(2,1)} %refs_22_.1) | copy-start | bytes 9437188
  6.5 121.6 %all-gather.3.cloned.1.call-start = ((), (), s32[]{:S(2)}) async-start(), calls=%async_computation | async-start | bytes 8650752 | tf_op jit(solution)/shard_map/all_gather | solution.py:224
  9.1 5.6 %collective-permute-start.27 = (bf16[4,64,128]{2,1,0:T(8,128)(2,1)S(1)}, bf16[4,64,128]{2,1,0:T(8,128)(2,1)S(1)}, u32[]{:S(2)}, u32[]{:S(2)}) collective-permute-start(bf16[4,64,128]{2,1,0:T(8,128)(2,1)S(1)} %get-tuple-element.8), channel_id=1, source_target_pairs={{2,0},{3,1},{0,2},{1,3},{6,4},{7,5},{4,6},{5,7},{10,8},{11,9},{8,1... | collective-permute-start | bytes 196616 | tf_op jit(solution)/shard_map/ppermute | solution.py:195
  13.0 3.8 %collective-permute-start.26 = (bf16[4,64,128]{2,1,0:T(8,128)(2,1)S(1)}, bf16[4,64,128]{2,1,0:T(8,128)(2,1)S(1)}, u32[]{:S(2)}, u32[]{:S(2)}) collective-permute-start(bf16[4,64,128]{2,1,0:T(8,128)(2,1)S(1)} %get-tuple-element.8), channel_id=1, source_target_pairs={{1,0},{2,1},{3,2},{0,3},{5,4},{6,5},{7,6},{4,7},{9,8},{10,9},{11,1... | collective-permute-start | bytes 196616 | tf_op jit(solution)/shard_map/ppermute | solution.py:195
  13.7 4.3 %collective-permute-start.28 = (bf16[4,64,128]{2,1,0:T(8,128)(2,1)S(1)}, bf16[4,64,128]{2,1,0:T(8,128)(2,1)S(1)}, u32[]{:S(2)}, u32[]{:S(2)}) collective-permute-start(bf16[4,64,128]{2,1,0:T(8,128)(2,1)S(1)} %get-tuple-element.8), channel_id=1, source_target_pairs={{3,0},{0,1},{1,2},{2,3},{7,4},{4,5},{5,6},{6,7},{11,8},{8,9},{9,10... | collective-permute-start | bytes 196616 | tf_op jit(solution)/shard_map/ppermute | solution.py:195
  18.9 97.6 %copy-start.5 = (f32[2,3,512]{2,0,1:T(2,128)S(1)}, f32[2,3,512]{2,0,1:T(2,128)}, u32[]{:S(2)}) copy-start(f32[2,3,512]{2,0,1:T(2,128)} %param.14) | copy-start | bytes 36868
  18.9 26.1 %collective-permute-start.1 = (bf16[2,64,128]{2,1,0:T(8,128)(2,1)S(1)}, bf16[2,64,128]{2,1,0:T(8,128)(2,1)S(1)}, u32[]{:S(2)}, u32[]{:S(2)}) collective-permute-start(bf16[2,64,128]{2,1,0:T(8,128)(2,1)S(1)} %get-tuple-element.6), channel_id=1, source_target_pairs={{64,0},{68,4},{72,8},{76,12},{80,16},{84,20},{88,24},{92,28},{96,3... | collective-permute-start | bytes 98312 | tf_op jit(solution)/shard_map/ppermute | solution.py:195
  39.5 6.8 %collective-permute-start = (bf16[2,64,128]{2,1,0:T(8,128)(2,1)S(1)}, bf16[2,64,128]{2,1,0:T(8,128)(2,1)S(1)}, u32[]{:S(2)}, u32[]{:S(2)}) collective-permute-start(bf16[2,64,128]{2,1,0:T(8,128)(2,1)S(1)} %get-tuple-element.6), channel_id=1, source_target_pairs={{32,0},{36,4},{40,8},{44,12},{48,16},{52,20},{56,24},{60,28},{64,3... | collective-permute-start | bytes 98312 | tf_op jit(solution)/shard_map/ppermute | solution.py:195
  40.0 7.0 %collective-permute-start.2 = (bf16[2,64,128]{2,1,0:T(8,128)(2,1)S(1)}, bf16[2,64,128]{2,1,0:T(8,128)(2,1)S(1)}, u32[]{:S(2)}, u32[]{:S(2)}) collective-permute-start(bf16[2,64,128]{2,1,0:T(8,128)(2,1)S(1)} %get-tuple-element.6), channel_id=1, source_target_pairs={{96,0},{100,4},{104,8},{108,12},{112,16},{116,20},{120,24},{124,28... | collective-permute-start | bytes 98312 | tf_op jit(solution)/shard_map/ppermute | solution.py:195
  47.0 16.2 %collective-permute-start.6 = (bf16[4,2,64,128]{3,2,1,0:T(8,128)(2,1)S(1)}, bf16[4,2,64,128]{3,2,1,0:T(8,128)(2,1)S(1)}, u32[]{:S(2)}, u32[]{:S(2)}) collective-permute-start(bf16[4,2,64,128]{3,2,1,0:T(8,128)(2,1)S(1)} %pad_maximum_fusion.1), channel_id=1, source_target_pairs={{120,0},{124,4},{0,8},{4,12},{8,16},{12,20},{16,24},{20,28},{24,32... | collective-permute-start | bytes 393224 | tf_op jit(solution)/shard_map/ppermute | solution.py:195
  48.5 9.8 %collective-permute-start.3 = (bf16[4,2,64,128]{3,2,1,0:T(8,128)(2,1)S(1)}, bf16[4,2,64,128]{3,2,1,0:T(8,128)(2,1)S(1)}, u32[]{:S(2)}, u32[]{:S(2)}) collective-permute-start(bf16[4,2,64,128]{3,2,1,0:T(8,128)(2,1)S(1)} %pad_maximum_fusion.1), channel_id=1, source_target_pairs={{8,0},{12,4},{16,8},{20,12},{24,16},{28,20},{32,24},{36,28},{40,32... | collective-permute-start | bytes 393224 | tf_op jit(solution)/shard_map/ppermute | solution.py:195
  54.0 9.2 %collective-permute-start.5 = (bf16[2,2,64,128]{3,2,1,0:T(8,128)(2,1)S(1)}, bf16[2,2,64,128]{3,2,1,0:T(8,128)(2,1)S(1)}, u32[]{:S(2)}, u32[]{:S(2)}) collective-permute-start(bf16[2,2,64,128]{3,2,1,0:T(8,128)(2,1)S(1)} %get-tuple-element.17), channel_id=1, source_target_pairs={{112,0},{116,4},{120,8},{124,12},{0,16},{4,20},{8,24},{12,28},{16,... | collective-permute-start | bytes 196616 | tf_op jit(solution)/shard_map/ppermute | solution.py:195
  54.1 7.1 %collective-permute-start.4 = (bf16[2,2,64,128]{3,2,1,0:T(8,128)(2,1)S(1)}, bf16[2,2,64,128]{3,2,1,0:T(8,128)(2,1)S(1)}, u32[]{:S(2)}, u32[]{:S(2)}) collective-permute-start(bf16[2,2,64,128]{3,2,1,0:T(8,128)(2,1)S(1)} %get-tuple-element.18), channel_id=1, source_target_pairs={{16,0},{20,4},{24,8},{28,12},{32,16},{36,20},{40,24},{44,28},{48,3... | collective-permute-start | bytes 196616 | tf_op jit(solution)/shard_map/ppermute | solution.py:195
  63.3 27.3 %copy-start.6 = (bf16[16,2,64,128]{3,2,1,0:T(8,128)(2,1)}, bf16[16,2,64,128]{3,2,1,0:T(8,128)(2,1)S(1)}, u32[]{:S(2)}) copy-start(bf16[16,2,64,128]{3,2,1,0:T(8,128)(2,1)S(1)} %constant_dynamic-update-slice_fusion.refs_0_) | copy-start | bytes 1572868
  63.3 13.7 %collective-permute-start.16 = (bf16[16,2,64,128]{3,2,1,0:T(8,128)(2,1)S(1)}, bf16[16,2,64,128]{3,2,1,0:T(8,128)(2,1)S(1)}, u32[]{:S(2)}, u32[]{:S(2)}) collective-permute-start(bf16[16,2,64,128]{3,2,1,0:T(8,128)(2,1)S(1)} %constant_dynamic-update-slice_fusion.refs_0_), channel_id=1, source_target_pairs={{128,0},{0,128},{129,1},{1,129},{130,2},{2,130},{131,3},{3,131},{1... | collective-permute-start | bytes 1572872 | tf_op jit(solution)/shard_map/ppermute | solution.py:240
  65.8 24.1 %collective-permute-start.11 = (bf16[16,2,64,128]{3,2,1,0:T(8,128)(2,1)S(1)}, bf16[16,2,64,128]{3,2,1,0:T(8,128)(2,1)S(1)}, u32[]{:S(2)}, u32[]{:S(2)}) collective-permute-start(bf16[16,2,64,128]{3,2,1,0:T(8,128)(2,1)S(1)} %constant_dynamic-update-slice_fusion.refs_0_), channel_id=1, source_target_pairs={{4,0},{0,4},{12,8},{8,12},{20,16},{16,20},{28,24},{24,28},{36,32},... | collective-permute-start | bytes 1572872 | tf_op jit(solution)/shard_map/ppermute | solution.py:199
  71.4 18.7 %collective-permute-start.8 = (bf16[16,2,64,128]{3,2,1,0:T(8,128)(2,1)S(1)}, bf16[16,2,64,128]{3,2,1,0:T(8,128)(2,1)S(1)}, u32[]{:S(2)}, u32[]{:S(2)}) collective-permute-start(bf16[16,2,64,128]{3,2,1,0:T(8,128)(2,1)S(1)} %constant_dynamic-update-slice_fusion.refs_0_), channel_id=1, source_target_pairs={{3,0},{0,1},{1,2},{2,3},{7,4},{4,5},{5,6},{6,7},{11,8},{8,9},{9,10... | collective-permute-start | bytes 1572872 | tf_op jit(solution)/shard_map/ppermute | solution.py:195
  71.4 19.2 %collective-permute-start.7 = (bf16[16,2,64,128]{3,2,1,0:T(8,128)(2,1)S(1)}, bf16[16,2,64,128]{3,2,1,0:T(8,128)(2,1)S(1)}, u32[]{:S(2)}, u32[]{:S(2)}) collective-permute-start(bf16[16,2,64,128]{3,2,1,0:T(8,128)(2,1)S(1)} %constant_dynamic-update-slice_fusion.refs_0_), channel_id=1, source_target_pairs={{1,0},{2,1},{3,2},{0,3},{5,4},{6,5},{7,6},{4,7},{9,8},{10,9},{11,1... | collective-permute-start | bytes 1572872 | tf_op jit(solution)/shard_map/ppermute | solution.py:195
  75.0 14.9 %collective-permute-start.29 = (bf16[32,2048]{1,0:T(8,128)(2,1)S(1)}, bf16[32,2048]{1,0:T(8,128)(2,1)S(1)}, u32[]{:S(2)}, u32[]{:S(2)}) collective-permute-start(bf16[32,2048]{1,0:T(8,128)(2,1)S(1)} %slice.62), channel_id=1, source_target_pairs={{0,1},{1,2},{2,3},{3,4},{4,5},{5,6},{6,7},{7,8},{8,9},{9,10},{10,1... | collective-permute-start | bytes 393224 | tf_op jit(solution)/shard_map/ppermute | solution.py:205
  76.9 38.7 %copy-start.7 = (bf16[16,2,64,128]{3,2,1,0:T(8,128)(2,1)}, bf16[16,2,64,128]{3,2,1,0:T(8,128)(2,1)S(1)}, u32[]{:S(2)}) copy-start(bf16[16,2,64,128]{3,2,1,0:T(8,128)(2,1)S(1)} %collective-permute-done.16.refs_10_) | copy-start | bytes 1572868
  76.9 20.5 %collective-permute-start.18 = (bf16[16,2,64,128]{3,2,1,0:T(8,128)(2,1)S(1)}, bf16[16,2,64,128]{3,2,1,0:T(8,128)(2,1)}, u32[]{:S(2)}, u32[]{:S(2)}) collective-permute-start(bf16[16,2,64,128]{3,2,1,0:T(8,128)(2,1)S(1)} %collective-permute-done.16.refs_10_), channel_id=1, source_target_pairs={{3,0},{0,1},{1,2},{2,3},{7,4},{4,5},{5,6},{6,7},{11,8},{8,9},{9,10... | collective-permute-start | bytes 1572872 | tf_op jit(solution)/shard_map/ppermute | solution.py:195
  89.9 35.1 %copy-start.2 = (bf16[32,2048]{1,0:T(8,128)(2,1)}, bf16[32,2048]{1,0:T(8,128)(2,1)S(1)}, u32[]{:S(2)}) copy-start(bf16[32,2048]{1,0:T(8,128)(2,1)S(1)} %collective-permute-done.29.refs_0_.refs_21_) | copy-start | bytes 393220
  89.9 11.7 %collective-permute-start.17 = (bf16[16,2,64,128]{3,2,1,0:T(8,128)(2,1)S(1)}, bf16[16,2,64,128]{3,2,1,0:T(8,128)(2,1)}, u32[]{:S(2)}, u32[]{:S(2)}) collective-permute-start(bf16[16,2,64,128]{3,2,1,0:T(8,128)(2,1)S(1)} %collective-permute-done.16.refs_10_), channel_id=1, source_target_pairs={{1,0},{2,1},{3,2},{0,3},{5,4},{6,5},{7,6},{4,7},{9,8},{10,9},{11,1... | collective-permute-start | bytes 1572872 | tf_op jit(solution)/shard_map/ppermute | solution.py:195
  89.9 25.9 %copy-start.8 = (bf16[16,2,64,128]{3,2,1,0:T(8,128)(2,1)}, bf16[16,2,64,128]{3,2,1,0:T(8,128)(2,1)S(1)}, u32[]{:S(2)}) copy-start(bf16[16,2,64,128]{3,2,1,0:T(8,128)(2,1)S(1)} %collective-permute-done.11.refs_5_) | copy-start | bytes 1572868
  89.9 20.5 %collective-permute-start.21 = (bf16[16,2,64,128]{3,2,1,0:T(8,128)(2,1)S(1)}, bf16[16,2,64,128]{3,2,1,0:T(8,128)(2,1)S(1)}, u32[]{:S(2)}, u32[]{:S(2)}) collective-permute-start(bf16[16,2,64,128]{3,2,1,0:T(8,128)(2,1)S(1)} %collective-permute-done.16.refs_10_), channel_id=1, source_target_pairs={{4,0},{0,4},{12,8},{8,12},{20,16},{16,20},{28,24},{24,28},{36,32},... | collective-permute-start | bytes 1572872 | tf_op jit(solution)/shard_map/ppermute | solution.py:199
  90.1 24.0 %copy-start.3 = (bf16[16,2,64,128]{3,2,1,0:T(8,128)(2,1)}, bf16[16,2,64,128]{3,2,1,0:T(8,128)(2,1)S(1)}, u32[]{:S(2)}) copy-start(bf16[16,2,64,128]{3,2,1,0:T(8,128)(2,1)S(1)} %collective-permute-done.8.refs_2_) | copy-start | bytes 1572868
  90.1 24.0 %collective-permute-start.13 = (bf16[16,2,64,128]{3,2,1,0:T(8,128)(2,1)S(1)}, bf16[16,2,64,128]{3,2,1,0:T(8,128)(2,1)S(1)}, u32[]{:S(2)}, u32[]{:S(2)}) collective-permute-start(bf16[16,2,64,128]{3,2,1,0:T(8,128)(2,1)S(1)} %collective-permute-done.8.refs_2_), channel_id=1, source_target_pairs={{4,0},{0,4},{12,8},{8,12},{20,16},{16,20},{28,24},{24,28},{36,32},... | collective-permute-start | bytes 1572872 | tf_op jit(solution)/shard_map/ppermute | solution.py:199
  90.6 23.5 %copy-start.4 = (bf16[16,2,64,128]{3,2,1,0:T(8,128)(2,1)}, bf16[16,2,64,128]{3,2,1,0:T(8,128)(2,1)S(1)}, u32[]{:S(2)}) copy-start(bf16[16,2,64,128]{3,2,1,0:T(8,128)(2,1)S(1)} %collective-permute-done.7.refs_1_) | copy-start | bytes 1572868
  90.6 25.1 %collective-permute-start.12 = (bf16[16,2,64,128]{3,2,1,0:T(8,128)(2,1)S(1)}, bf16[16,2,64,128]{3,2,1,0:T(8,128)(2,1)S(1)}, u32[]{:S(2)}, u32[]{:S(2)}) collective-permute-start(bf16[16,2,64,128]{3,2,1,0:T(8,128)(2,1)S(1)} %collective-permute-done.7.refs_1_), channel_id=1, source_target_pairs={{4,0},{0,4},{12,8},{8,12},{20,16},{16,20},{28,24},{24,28},{36,32},... | collective-permute-start | bytes 1572872 | tf_op jit(solution)/shard_map/ppermute | solution.py:199
  97.4 10.4 %collective-permute-start.10 = (bf16[8,2,64,128]{3,2,1,0:T(8,128)(2,1)S(1)}, bf16[8,2,64,128]{3,2,1,0:T(8,128)(2,1)}, u32[]{:S(2)}, u32[]{:S(2)}) collective-permute-start(bf16[8,2,64,128]{3,2,1,0:T(8,128)(2,1)S(1)} %slice.67), channel_id=1, source_target_pairs={{3,0},{0,1},{1,2},{2,3},{7,4},{4,5},{5,6},{6,7},{11,8},{8,9},{9,10... | collective-permute-start | bytes 786440 | tf_op jit(solution)/shard_map/ppermute | solution.py:195
  101.6 8.8 %collective-permute-start.9 = (bf16[8,2,64,128]{3,2,1,0:T(8,128)(2,1)S(1)}, bf16[8,2,64,128]{3,2,1,0:T(8,128)(2,1)S(1)}, u32[]{:S(2)}, u32[]{:S(2)}) collective-permute-start(bf16[8,2,64,128]{3,2,1,0:T(8,128)(2,1)S(1)} %slice.66), channel_id=1, source_target_pairs={{1,0},{2,1},{3,2},{0,3},{5,4},{6,5},{7,6},{4,7},{9,8},{10,9},{11,1... | collective-permute-start | bytes 786440 | tf_op jit(solution)/shard_map/ppermute | solution.py:195
  107.8 8.8 %collective-permute-start.15 = (bf16[8,2,64,128]{3,2,1,0:T(8,128)(2,1)}, bf16[8,2,64,128]{3,2,1,0:T(8,128)(2,1)}, u32[]{:S(2)}, u32[]{:S(2)}) collective-permute-start(bf16[8,2,64,128]{3,2,1,0:T(8,128)(2,1)} %collective-permute-done.10.refs_4_), channel_id=1, source_target_pairs={{4,0},{0,4},{12,8},{8,12},{20,16},{16,20},{28,24},{24,28},{36,32},... | collective-permute-start | bytes 786440 | tf_op jit(solution)/shard_map/ppermute | solution.py:199
  110.4 5.4 %copy-start.12 = (bf16[8,2,64,128]{3,2,1,0:T(8,128)(2,1)}, bf16[8,2,64,128]{3,2,1,0:T(8,128)(2,1)S(1)}, u32[]{:S(2)}) copy-start(bf16[8,2,64,128]{3,2,1,0:T(8,128)(2,1)S(1)} %collective-permute-done.9.refs_3_) | copy-start | bytes 786436
  110.4 9.4 %collective-permute-start.20 = (bf16[8,2,64,128]{3,2,1,0:T(8,128)(2,1)}, bf16[8,2,64,128]{3,2,1,0:T(8,128)(2,1)}, u32[]{:S(2)}, u32[]{:S(2)}) collective-permute-start(bf16[8,2,64,128]{3,2,1,0:T(8,128)(2,1)} %slice.69), channel_id=1, source_target_pairs={{3,0},{0,1},{1,2},{2,3},{7,4},{4,5},{5,6},{6,7},{11,8},{8,9},{9,10... | collective-permute-start | bytes 786440 | tf_op jit(solution)/shard_map/ppermute | solution.py:195
  110.4 5.4 %copy-start.9 = (bf16[16,2,64,128]{3,2,1,0:T(8,128)(2,1)}, bf16[16,2,64,128]{3,2,1,0:T(8,128)(2,1)S(1)}, u32[]{:S(2)}) copy-start(bf16[16,2,64,128]{3,2,1,0:T(8,128)(2,1)S(1)} %collective-permute-done.21.refs_15_) | copy-start | bytes 1572868
  110.4 11.1 %collective-permute-start.19 = (bf16[8,2,64,128]{3,2,1,0:T(8,128)(2,1)S(1)}, bf16[8,2,64,128]{3,2,1,0:T(8,128)(2,1)}, u32[]{:S(2)}, u32[]{:S(2)}) collective-permute-start(bf16[8,2,64,128]{3,2,1,0:T(8,128)(2,1)S(1)} %slice.68), channel_id=1, source_target_pairs={{1,0},{2,1},{3,2},{0,3},{5,4},{6,5},{7,6},{4,7},{9,8},{10,9},{11,1... | collective-permute-start | bytes 786440 | tf_op jit(solution)/shard_map/ppermute | solution.py:195
  114.1 1.8 %copy-start.10 = (bf16[16,2,64,128]{3,2,1,0:T(8,128)(2,1)}, bf16[16,2,64,128]{3,2,1,0:T(8,128)(2,1)S(1)}, u32[]{:S(2)}) copy-start(bf16[16,2,64,128]{3,2,1,0:T(8,128)(2,1)S(1)} %collective-permute-done.13.refs_7_) | copy-start | bytes 1572868
  114.1 14.0 %collective-permute-start.23 = (bf16[16,2,64,128]{3,2,1,0:T(8,128)(2,1)}, bf16[16,2,64,128]{3,2,1,0:T(8,128)(2,1)}, u32[]{:S(2)}, u32[]{:S(2)}) collective-permute-start(bf16[16,2,64,128]{3,2,1,0:T(8,128)(2,1)} %collective-permute-done.18.refs_12_), channel_id=1, source_target_pairs={{4,0},{0,4},{12,8},{8,12},{20,16},{16,20},{28,24},{24,28},{36,32},... | collective-permute-start | bytes 1572872 | tf_op jit(solution)/shard_map/ppermute | solution.py:199
  115.6 0.8 copy-start.11
  115.6 12.5 %collective-permute-start.22 = (bf16[16,2,64,128]{3,2,1,0:T(8,128)(2,1)}, bf16[16,2,64,128]{3,2,1,0:T(8,128)(2,1)}, u32[]{:S(2)}, u32[]{:S(2)}) collective-permute-start(bf16[16,2,64,128]{3,2,1,0:T(8,128)(2,1)} %collective-permute-done.17.refs_11_), channel_id=1, source_target_pairs={{4,0},{0,4},{12,8},{8,12},{20,16},{16,20},{28,24},{24,28},{36,32},... | collective-permute-start | bytes 1572872 | tf_op jit(solution)/shard_map/ppermute | solution.py:199
  116.6 10.0 %collective-permute-start.14 = (bf16[8,2,64,128]{3,2,1,0:T(8,128)(2,1)}, bf16[8,2,64,128]{3,2,1,0:T(8,128)(2,1)S(1)}, u32[]{:S(2)}, u32[]{:S(2)}) collective-permute-start(bf16[8,2,64,128]{3,2,1,0:T(8,128)(2,1)} %copy-done.12), channel_id=1, source_target_pairs={{4,0},{0,4},{12,8},{8,12},{20,16},{16,20},{28,24},{24,28},{36,32},... | collective-permute-start | bytes 786440 | tf_op jit(solution)/shard_map/ppermute | solution.py:199
  119.8 7.6 %collective-permute-start.25 = (bf16[8,2,64,128]{3,2,1,0:T(8,128)(2,1)}, bf16[8,2,64,128]{3,2,1,0:T(8,128)(2,1)S(1)}, u32[]{:S(2)}, u32[]{:S(2)}) collective-permute-start(bf16[8,2,64,128]{3,2,1,0:T(8,128)(2,1)} %collective-permute-done.20.refs_14_), channel_id=1, source_target_pairs={{4,0},{0,4},{12,8},{8,12},{20,16},{16,20},{28,24},{24,28},{36,32},... | collective-permute-start | bytes 786440 | tf_op jit(solution)/shard_map/ppermute | solution.py:199
  121.5 6.6 %collective-permute-start.24 = (bf16[8,2,64,128]{3,2,1,0:T(8,128)(2,1)}, bf16[8,2,64,128]{3,2,1,0:T(8,128)(2,1)S(1)}, u32[]{:S(2)}, u32[]{:S(2)}) collective-permute-start(bf16[8,2,64,128]{3,2,1,0:T(8,128)(2,1)} %collective-permute-done.19.refs_13_), channel_id=1, source_target_pairs={{4,0},{0,4},{12,8},{8,12},{20,16},{16,20},{28,24},{24,28},{36,32},... | collective-permute-start | bytes 786440 | tf_op jit(solution)/shard_map/ppermute | solution.py:199
  125.0 1.7 %copy-start.1 = (bf16[800,2048]{1,0:T(8,128)(2,1)}, bf16[800,2048]{1,0:T(8,128)(2,1)S(1)}, u32[]{:S(2)}) copy-start(bf16[800,2048]{1,0:T(8,128)(2,1)S(1)} %shard_map.82.refs_23_) | copy-start | bytes 9830404
  126.7 0.7 copy-start.13
  127.4 0.7 copy-start.14
  128.1 0.7 copy-start.15
Sparse Core Ops, SparseCore 0:
  19.0 94.8 all-gather.2

commit v4 on v3

--- a/solution.py
+++ b/solution.py
@@ -153,7 +153,11 @@
                 stream = x_ref[rows, :].astype(jnp.float32) + normed(branch, post_ref[pl.ds(l, 1), :])
                 rounded = stream.astype(jnp.bfloat16)
                 x_ref[rows, :] = rounded
-                h_ref[rows, :] = normed(rounded.astype(jnp.float32), next_gain).astype(jnp.bfloat16)
+
+                @pl.when(l == 0)
+                def _():
+                    h_ref[rows, :] = normed(rounded.astype(jnp.float32), next_gain).astype(jnp.bfloat16)
+
                 for k in range(CHUNKS):
                     pl.when((l == 1) & (r == k))(lambda k=k: out_copy(k).start())
                 return carry
@@ -247,25 +251,18 @@
         here_sp, parity = lax.axis_index("sp"), lax.axis_index("grp") % 2
         chip, core = here_sp // 2, here_sp % 2
 
+        places_along = [(quarter * (place % 4) + (0, 1, 2, -1)[place // 4]) % chips for place in range(chips)]
+        row_of = [[(chip + away) % chips * 2 + c for away in places_along] for c in (core, 1 - core)]
+        mats_of = [pl.ds(share * parity, share), pl.ds(share * (1 - parity), share)]
+
         def put(n):
-            ref = src[n]
             second, side, p = n // (2 * len(places)), n // len(places) % 2, n % len(places)
             column, begin = places[p]
             place_of = columns[0].index(column % tp)
             pair, lanes = place_of // 2, pl.ds(place_of % 2 * block_cols, block_cols)
-            mats = pl.ds(share * (parity if second == 0 else 1 - parity), share)
-            side_core = core if side == 0 else 1 - core
-
-            def start(k, carry):
-                place = begin + k
-                step = place // 4
-                offset = quarter * (place % 4) + jnp.where(step == 3, -1, step)
-                row = ((chip + offset + chips) % chips) * 2 + side_core
-                target = w_ref.at[pair, mats, row, :, lanes]
-                pltpu.make_async_copy(ref.at[k], target, sems.at[pair]).start()
-                return carry
-
-            lax.fori_loop(0, ref.shape[0], start, 0)
+            for k in range(src[n].shape[0]):
+                target = w_ref.at[pair, mats_of[second], row_of[side][begin + k], :, lanes]
+                pltpu.make_async_copy(src[n].at[k], target, sems.at[pair]).start()
 
         for column in columns[0]:
             for n in range(len(src)):

time: 165 us -> 162 us (0.982)
  Pallas kernels: 30.8 us -> 27.4 us
    pallas_call x1, Pallas kernels: 28.7 us -> 25.4 us  [two_mixers(): pl.pallas_call(kernel, out_shape=jax.ShapeDtypeStruct((out_rows, d), jnp....]
where the time goes in v4:
time: 162 us; the launch traced here: 161 us
  starting transfers between devices  69.4 us (43%)
  waiting for transfers between devices  37.5 us (23%)
  Pallas kernels  27.4 us (17%)
  between operations  13.9 us (9%)
  local copies, waits for them, and re-layouts  11.4 us (7%)
    ppermute x18, starting transfers between devices, receive(): lax.ppermute(value, axis, turned(lax.axis_size(axis), stride, distance))  53.9 us
    pallas_call x1, Pallas kernels, two_mixers(): pl.pallas_call(kernel, out_shape=jax.ShapeDtypeStruct((out_rows, d), jnp....  25.4 us
    ppermute x18, waiting for transfers between devices, receive(): lax.ppermute(value, axis, turned(lax.axis_size(axis), stride, distance))  24.6 us
    ppermute x1, waiting for transfers between devices, early_halo(): lax.ppermute(tokens[-HALO:], axes, [(i - 1, i) for i in range(1, total)])  12.8 us
    ppermute x10, starting transfers between devices, other_core(): lax.ppermute(value, 'sp', [(i ^ 1, i) for i in range(lax.axis_size('sp'))])  11 us
    unnamed x46, local copies, waits for them, and re-layouts  4.53 us
  transfers between devices with their start and end apart: 31, of which 13 were waited for; matrix products, arithmetic and copies ran while one was open for 3% of the time, Pallas kernels for 1%

profile of v4, /device:TPU:33, one launch (start us, length us, event | category | flops | bytes accessed | tf_op | source)
XLA Modules:
  0.0 161.1 jit_solution(13011892598962313130)
XLA Ops:
  6.6 0.9 fusion.7
  7.4 0.8 slice_bitcast_fusion
  8.3 0.8 fusion.5
  9.1 4.0 %collective-permute-start.27 = (bf16[4,64,128]{2,1,0:T(8,128)(2,1)S(1)}, bf16[4,64,128]{2,1,0:T(8,128)(2,1)S(1)}, u32[]{:S(2)}, u32[]{:S(2)}) collective-permute-start(bf16[4,64,128]{2,1,0:T(8,128)(2,1)S(1)} %get-tuple-element.8), channel_id=1, source_target_pairs={{2,0},{3,1},{0,2},{1,3},{6,4},{7,5},{4,6},{5,7},{10,8},{11,9},{8,1... | collective-permute-start | bytes 196616 | tf_op jit(solution)/shard_map/ppermute | solution.py:199
  13.0 0.7 collective-permute-start.26
  13.7 0.7 collective-permute-start.28
  14.5 0.2 collective-permute-done.27
  14.7 2.1 %collective-permute-done.26 = bf16[4,64,128]{2,1,0:T(8,128)(2,1)S(1)} collective-permute-done((bf16[4,64,128]{2,1,0:T(8,128)(2,1)S(1)}, bf16[4,64,128]{2,1,0:T(8,128)(2,1)S(1)}, u32[]{:S(2)}, u32[]{:S(2)}) %collective-permute-start.26) | collective-permute-done | bytes 65568 | tf_op jit(solution)/shard_map/ppermute | solution.py:199
  16.8 1.3 collective-permute-done.28
  18.1 0.7 pad_maximum_fusion
  18.8 0.1 all-gather.3.cloned.1.call-update
  18.9 0.0 copy-start.5
  18.9 20.5 %collective-permute-start.1 = (bf16[2,64,128]{2,1,0:T(8,128)(2,1)S(1)}, bf16[2,64,128]{2,1,0:T(8,128)(2,1)S(1)}, u32[]{:S(2)}, u32[]{:S(2)}) collective-permute-start(bf16[2,64,128]{2,1,0:T(8,128)(2,1)S(1)} %get-tuple-element.6), channel_id=1, source_target_pairs={{64,0},{68,4},{72,8},{76,12},{80,16},{84,20},{88,24},{92,28},{96,3... | collective-permute-start | bytes 98312 | tf_op jit(solution)/shard_map/ppermute | solution.py:199
  39.5 0.6 collective-permute-start
  40.0 5.0 %collective-permute-start.2 = (bf16[2,64,128]{2,1,0:T(8,128)(2,1)S(1)}, bf16[2,64,128]{2,1,0:T(8,128)(2,1)S(1)}, u32[]{:S(2)}, u32[]{:S(2)}) collective-permute-start(bf16[2,64,128]{2,1,0:T(8,128)(2,1)S(1)} %get-tuple-element.6), channel_id=1, source_target_pairs={{96,0},{100,4},{104,8},{108,12},{112,16},{116,20},{120,24},{124,28... | collective-permute-start | bytes 98312 | tf_op jit(solution)/shard_map/ppermute | solution.py:199
  45.0 0.0 collective-permute-done.1
  45.0 1.3 collective-permute-done
  46.3 0.7 collective-permute-done.2
  47.0 1.5 collective-permute-start.6
  48.5 5.5 %collective-permute-start.3 = (bf16[4,2,64,128]{3,2,1,0:T(8,128)(2,1)S(1)}, bf16[4,2,64,128]{3,2,1,0:T(8,128)(2,1)S(1)}, u32[]{:S(2)}, u32[]{:S(2)}) collective-permute-start(bf16[4,2,64,128]{3,2,1,0:T(8,128)(2,1)S(1)} %pad_maximum_fusion.1), channel_id=1, source_target_pairs={{8,0},{12,4},{16,8},{20,12},{24,16},{28,20},{32,24},{36,28},{40,32... | collective-permute-start | bytes 393224 | tf_op jit(solution)/shard_map/ppermute | solution.py:199
  54.0 0.1 collective-permute-start.5
  54.1 3.5 %collective-permute-start.4 = (bf16[2,2,64,128]{3,2,1,0:T(8,128)(2,1)S(1)}, bf16[2,2,64,128]{3,2,1,0:T(8,128)(2,1)S(1)}, u32[]{:S(2)}, u32[]{:S(2)}) collective-permute-start(bf16[2,2,64,128]{3,2,1,0:T(8,128)(2,1)S(1)} %get-tuple-element.18), channel_id=1, source_target_pairs={{16,0},{20,4},{24,8},{28,12},{32,16},{36,20},{40,24},{44,28},{48,3... | collective-permute-start | bytes 196616 | tf_op jit(solution)/shard_map/ppermute | solution.py:199
  57.7 0.6 collective-permute-done.3
  58.3 2.9 %collective-permute-done.4 = bf16[2,2,64,128]{3,2,1,0:T(8,128)(2,1)S(1)} collective-permute-done((bf16[2,2,64,128]{3,2,1,0:T(8,128)(2,1)S(1)}, bf16[2,2,64,128]{3,2,1,0:T(8,128)(2,1)S(1)}, u32[]{:S(2)}, u32[]{:S(2)}) %collective-permute-start.4) | collective-permute-done | bytes 65568 | tf_op jit(solution)/shard_map/ppermute | solution.py:199
  61.2 2.0 %collective-permute-done.5 = bf16[2,2,64,128]{3,2,1,0:T(8,128)(2,1)S(1)} collective-permute-done((bf16[2,2,64,128]{3,2,1,0:T(8,128)(2,1)S(1)}, bf16[2,2,64,128]{3,2,1,0:T(8,128)(2,1)S(1)}, u32[]{:S(2)}, u32[]{:S(2)}) %collective-permute-start.5) | collective-permute-done | bytes 65568 | tf_op jit(solution)/shard_map/ppermute | solution.py:199
  63.3 2.5 %collective-permute-start.16 = (bf16[16,2,64,128]{3,2,1,0:T(8,128)(2,1)S(1)}, bf16[16,2,64,128]{3,2,1,0:T(8,128)(2,1)S(1)}, u32[]{:S(2)}, u32[]{:S(2)}) collective-permute-start(bf16[16,2,64,128]{3,2,1,0:T(8,128)(2,1)S(1)} %constant_dynamic-update-slice_fusion.refs_0_), channel_id=1, source_target_pairs={{128,0},{0,128},{129,1},{1,129},{130,2},{2,130},{131,3},{3,131},{1... | collective-permute-start | bytes 1572872 | tf_op jit(solution)/shard_map/ppermute | solution.py:244
  65.8 5.6 %collective-permute-start.11 = (bf16[16,2,64,128]{3,2,1,0:T(8,128)(2,1)S(1)}, bf16[16,2,64,128]{3,2,1,0:T(8,128)(2,1)S(1)}, u32[]{:S(2)}, u32[]{:S(2)}) collective-permute-start(bf16[16,2,64,128]{3,2,1,0:T(8,128)(2,1)S(1)} %constant_dynamic-update-slice_fusion.refs_0_), channel_id=1, source_target_pairs={{4,0},{0,4},{12,8},{8,12},{20,16},{16,20},{28,24},{24,28},{36,32},... | collective-permute-start | bytes 1572872 | tf_op jit(solution)/shard_map/ppermute | solution.py:203
  71.4 2.7 %collective-permute-start.7 = (bf16[16,2,64,128]{3,2,1,0:T(8,128)(2,1)S(1)}, bf16[16,2,64,128]{3,2,1,0:T(8,128)(2,1)S(1)}, u32[]{:S(2)}, u32[]{:S(2)}) collective-permute-start(bf16[16,2,64,128]{3,2,1,0:T(8,128)(2,1)S(1)} %constant_dynamic-update-slice_fusion.refs_0_), channel_id=1, source_target_pairs={{1,0},{2,1},{3,2},{0,3},{5,4},{6,5},{7,6},{4,7},{9,8},{10,9},{11,1... | collective-permute-start | bytes 1572872 | tf_op jit(solution)/shard_map/ppermute | solution.py:199
  74.0 0.9 slice.62
  75.0 2.0 %collective-permute-start.29 = (bf16[32,2048]{1,0:T(8,128)(2,1)S(1)}, bf16[32,2048]{1,0:T(8,128)(2,1)S(1)}, u32[]{:S(2)}, u32[]{:S(2)}) collective-permute-start(bf16[32,2048]{1,0:T(8,128)(2,1)S(1)} %slice.62), channel_id=1, source_target_pairs={{0,1},{1,2},{2,3},{3,4},{4,5},{5,6},{6,7},{7,8},{8,9},{9,10},{10,1... | collective-permute-start | bytes 393224 | tf_op jit(solution)/shard_map/ppermute | solution.py:209
  76.9 0.1 collective-permute-start.18
  77.1 12.8 %collective-permute-done.29.refs_0_.refs_21_ = bf16[32,2048]{1,0:T(8,128)(2,1)S(1)} collective-permute-done((bf16[32,2048]{1,0:T(8,128)(2,1)S(1)}, bf16[32,2048]{1,0:T(8,128)(2,1)S(1)}, u32[]{:S(2)}, u32[]{:S(2)}) %collective-permute-start.29) | collective-permute-done | bytes 131104 | tf_op jit(solution)/shard_map/ppermute | solution.py:209
  89.9 0.0 collective-permute-start.17
  89.9 0.0 collective-permute-done.11.refs_5_
  89.9 0.1 collective-permute-start.21
  90.1 0.5 collective-permute-start.13
  90.6 0.0 collective-permute-done.7.refs_1_
  90.6 0.3 collective-permute-start.12
  90.9 6.5 %collective-permute-done.18.refs_12_ = bf16[16,2,64,128]{3,2,1,0:T(8,128)(2,1)} collective-permute-done((bf16[16,2,64,128]{3,2,1,0:T(8,128)(2,1)S(1)}, bf16[16,2,64,128]{3,2,1,0:T(8,128)(2,1)}, u32[]{:S(2)}, u32[]{:S(2)}) %collective-permute-start.18) | collective-permute-done | bytes 524320 | tf_op jit(solution)/shard_map/ppermute | solution.py:199
  97.4 1.9 %collective-permute-start.10 = (bf16[8,2,64,128]{3,2,1,0:T(8,128)(2,1)S(1)}, bf16[8,2,64,128]{3,2,1,0:T(8,128)(2,1)}, u32[]{:S(2)}, u32[]{:S(2)}) collective-permute-start(bf16[8,2,64,128]{3,2,1,0:T(8,128)(2,1)S(1)} %slice.67), channel_id=1, source_target_pairs={{3,0},{0,1},{1,2},{2,3},{7,4},{4,5},{5,6},{6,7},{11,8},{8,9},{9,10... | collective-permute-start | bytes 786440 | tf_op jit(solution)/shard_map/ppermute | solution.py:199
  99.3 2.4 %collective-permute-done.17.refs_11_ = bf16[16,2,64,128]{3,2,1,0:T(8,128)(2,1)} collective-permute-done((bf16[16,2,64,128]{3,2,1,0:T(8,128)(2,1)S(1)}, bf16[16,2,64,128]{3,2,1,0:T(8,128)(2,1)}, u32[]{:S(2)}, u32[]{:S(2)}) %collective-permute-start.17) | collective-permute-done | bytes 524320 | tf_op jit(solution)/shard_map/ppermute | solution.py:199
  101.6 3.5 %collective-permute-start.9 = (bf16[8,2,64,128]{3,2,1,0:T(8,128)(2,1)S(1)}, bf16[8,2,64,128]{3,2,1,0:T(8,128)(2,1)S(1)}, u32[]{:S(2)}, u32[]{:S(2)}) collective-permute-start(bf16[8,2,64,128]{3,2,1,0:T(8,128)(2,1)S(1)} %slice.66), channel_id=1, source_target_pairs={{1,0},{2,1},{3,2},{0,3},{5,4},{6,5},{7,6},{4,7},{9,8},{10,9},{11,1... | collective-permute-start | bytes 786440 | tf_op jit(solution)/shard_map/ppermute | solution.py:199
  105.1 1.7 %slice.69 = bf16[8,2,64,128]{3,2,1,0:T(8,128)(2,1)} slice(bf16[16,2,64,128]{3,2,1,0:T(8,128)(2,1)} %collective-permute-done.18.refs_12_), slice={[8:16], [0:2], [0:64], [0:128]} | slice | bytes 524288 | tf_op jit(solution)/shard_map/slice | solution.py:239
  106.8 1.0 slice.68
  107.8 0.0 collective-permute-done.10.refs_4_
  107.8 0.9 collective-permute-start.15
  108.7 1.7 %collective-permute-done.9.refs_3_ = bf16[8,2,64,128]{3,2,1,0:T(8,128)(2,1)S(1)} collective-permute-done((bf16[8,2,64,128]{3,2,1,0:T(8,128)(2,1)S(1)}, bf16[8,2,64,128]{3,2,1,0:T(8,128)(2,1)S(1)}, u32[]{:S(2)}, u32[]{:S(2)}) %collective-permute-start.9) | collective-permute-done | bytes 262176 | tf_op jit(solution)/shard_map/ppermute | solution.py:199
  110.4 3.6 %collective-permute-start.19 = (bf16[8,2,64,128]{3,2,1,0:T(8,128)(2,1)S(1)}, bf16[8,2,64,128]{3,2,1,0:T(8,128)(2,1)}, u32[]{:S(2)}, u32[]{:S(2)}) collective-permute-start(bf16[8,2,64,128]{3,2,1,0:T(8,128)(2,1)S(1)} %slice.68), channel_id=1, source_target_pairs={{1,0},{2,1},{3,2},{0,3},{5,4},{6,5},{7,6},{4,7},{9,8},{10,9},{11,1... | collective-permute-start | bytes 786440 | tf_op jit(solution)/shard_map/ppermute | solution.py:199
  114.1 1.6 collective-permute-start.23
  115.6 0.2 collective-permute-start.22
  115.8 0.6 copy-done.11
  116.6 0.2 collective-permute-start.14
  116.8 3.0 %collective-permute-done.20.refs_14_ = bf16[8,2,64,128]{3,2,1,0:T(8,128)(2,1)} collective-permute-done((bf16[8,2,64,128]{3,2,1,0:T(8,128)(2,1)}, bf16[8,2,64,128]{3,2,1,0:T(8,128)(2,1)}, u32[]{:S(2)}, u32[]{:S(2)}) %collective-permute-start.20) | collective-permute-done | bytes 262176 | tf_op jit(solution)/shard_map/ppermute | solution.py:199
  119.8 1.7 %collective-permute-start.25 = (bf16[8,2,64,128]{3,2,1,0:T(8,128)(2,1)}, bf16[8,2,64,128]{3,2,1,0:T(8,128)(2,1)S(1)}, u32[]{:S(2)}, u32[]{:S(2)}) collective-permute-start(bf16[8,2,64,128]{3,2,1,0:T(8,128)(2,1)} %collective-permute-done.20.refs_14_), channel_id=1, source_target_pairs={{4,0},{0,4},{12,8},{8,12},{20,16},{16,20},{28,24},{24,28},{36,32},... | collective-permute-start | bytes 786440 | tf_op jit(solution)/shard_map/ppermute | solution.py:203
  121.5 0.0 collective-permute-start.24
  121.5 0.7 slice.63.refs_2_
  122.3 0.6 pad_maximum_fusion.5.refs_25_
  122.9 2.1 %shard_map.82.refs_23_ = bf16[800,2048]{1,0:T(8,128)(2,1)S(1)} custom-call(bf16[32,2048]{1,0:T(8,128)(2,1)S(1)} %collective-permute-done.29.refs_0_.refs_21_, bf16[768,2048]{1,0:T(8,128)(2,1)S(1)} %copy-done, f32[1,2048]{1,0:T(1,128)S(1)} %slice.63.refs_2_), custom_call_target="tpu_custom_call" | custom-call | flops 13107200 | bytes 6553600 | tf_op jit(solution)/shard_map/pallas_call | solution.py:67
  125.0 1.7 %copy-done.1 = bf16[800,2048]{1,0:T(8,128)(2,1)} copy-done((bf16[800,2048]{1,0:T(8,128)(2,1)}, bf16[800,2048]{1,0:T(8,128)(2,1)S(1)}, u32[]{:S(2)}) %copy-start.1) | copy-done | bytes 3276824
  126.7 0.7 copy-done.13
  127.4 0.7 copy-done.14
  128.1 0.0 all-gather.3.cloned.1.call-done
  128.1 0.6 copy-done.15
  128.8 25.4 %shard_map.83 = bf16[768,2048]{1,0:T(8,128)(2,1)} custom-call(bf16[16,2,64,128]{3,2,1,0:T(8,128)(2,1)} %copy-done.6, bf16[16,2,64,128]{3,2,1,0:T(8,128)(2,1)} %copy-done.4, bf16[16,2,64,128]{3,2,1,0:T(8,128)(2,1)} %copy-done.3, bf16[8,2,64,128]{3,2,1,0:T(8,128)(2,1)} %copy-done.12, bf16[8,2,64,128]{3,2,1,0:T(8,128)(2,1)} %collective-permute-done.10.refs_4_, ...), custom_call_target="tpu_custom_call" | custom-call | flops 13421772800 | bytes 26607616 | tf_op jit(solution)/shard_map/pallas_call | solution.py:171
  (67 shorter events, 0.4 us)
Async XLA Ops:
  6.5 116.3 %copy-start = (bf16[768,2048]{1,0:T(8,128)(2,1)S(1)}, bf16[768,2048]{1,0:T(8,128)(2,1)}, u32[]{:S(2)}) copy-start(bf16[768,2048]{1,0:T(8,128)(2,1)} %refs_22_.1) | copy-start | bytes 9437188
  6.5 121.6 %all-gather.3.cloned.1.call-start = ((), (), s32[]{:S(2)}) async-start(), calls=%async_computation | async-start | bytes 8650752 | tf_op jit(solution)/shard_map/all_gather | solution.py:228
  9.1 5.6 %collective-permute-start.27 = (bf16[4,64,128]{2,1,0:T(8,128)(2,1)S(1)}, bf16[4,64,128]{2,1,0:T(8,128)(2,1)S(1)}, u32[]{:S(2)}, u32[]{:S(2)}) collective-permute-start(bf16[4,64,128]{2,1,0:T(8,128)(2,1)S(1)} %get-tuple-element.8), channel_id=1, source_target_pairs={{2,0},{3,1},{0,2},{1,3},{6,4},{7,5},{4,6},{5,7},{10,8},{11,9},{8,1... | collective-permute-start | bytes 196616 | tf_op jit(solution)/shard_map/ppermute | solution.py:199
  13.0 3.8 %collective-permute-start.26 = (bf16[4,64,128]{2,1,0:T(8,128)(2,1)S(1)}, bf16[4,64,128]{2,1,0:T(8,128)(2,1)S(1)}, u32[]{:S(2)}, u32[]{:S(2)}) collective-permute-start(bf16[4,64,128]{2,1,0:T(8,128)(2,1)S(1)} %get-tuple-element.8), channel_id=1, source_target_pairs={{1,0},{2,1},{3,2},{0,3},{5,4},{6,5},{7,6},{4,7},{9,8},{10,9},{11,1... | collective-permute-start | bytes 196616 | tf_op jit(solution)/shard_map/ppermute | solution.py:199
  13.7 4.3 %collective-permute-start.28 = (bf16[4,64,128]{2,1,0:T(8,128)(2,1)S(1)}, bf16[4,64,128]{2,1,0:T(8,128)(2,1)S(1)}, u32[]{:S(2)}, u32[]{:S(2)}) collective-permute-start(bf16[4,64,128]{2,1,0:T(8,128)(2,1)S(1)} %get-tuple-element.8), channel_id=1, source_target_pairs={{3,0},{0,1},{1,2},{2,3},{7,4},{4,5},{5,6},{6,7},{11,8},{8,9},{9,10... | collective-permute-start | bytes 196616 | tf_op jit(solution)/shard_map/ppermute | solution.py:199
  18.9 97.6 %copy-start.5 = (f32[2,3,512]{2,0,1:T(2,128)S(1)}, f32[2,3,512]{2,0,1:T(2,128)}, u32[]{:S(2)}) copy-start(f32[2,3,512]{2,0,1:T(2,128)} %param.14) | copy-start | bytes 36868
  18.9 26.1 %collective-permute-start.1 = (bf16[2,64,128]{2,1,0:T(8,128)(2,1)S(1)}, bf16[2,64,128]{2,1,0:T(8,128)(2,1)S(1)}, u32[]{:S(2)}, u32[]{:S(2)}) collective-permute-start(bf16[2,64,128]{2,1,0:T(8,128)(2,1)S(1)} %get-tuple-element.6), channel_id=1, source_target_pairs={{64,0},{68,4},{72,8},{76,12},{80,16},{84,20},{88,24},{92,28},{96,3... | collective-permute-start | bytes 98312 | tf_op jit(solution)/shard_map/ppermute | solution.py:199
  39.5 6.8 %collective-permute-start = (bf16[2,64,128]{2,1,0:T(8,128)(2,1)S(1)}, bf16[2,64,128]{2,1,0:T(8,128)(2,1)S(1)}, u32[]{:S(2)}, u32[]{:S(2)}) collective-permute-start(bf16[2,64,128]{2,1,0:T(8,128)(2,1)S(1)} %get-tuple-element.6), channel_id=1, source_target_pairs={{32,0},{36,4},{40,8},{44,12},{48,16},{52,20},{56,24},{60,28},{64,3... | collective-permute-start | bytes 98312 | tf_op jit(solution)/shard_map/ppermute | solution.py:199
  40.0 7.0 %collective-permute-start.2 = (bf16[2,64,128]{2,1,0:T(8,128)(2,1)S(1)}, bf16[2,64,128]{2,1,0:T(8,128)(2,1)S(1)}, u32[]{:S(2)}, u32[]{:S(2)}) collective-permute-start(bf16[2,64,128]{2,1,0:T(8,128)(2,1)S(1)} %get-tuple-element.6), channel_id=1, source_target_pairs={{96,0},{100,4},{104,8},{108,12},{112,16},{116,20},{120,24},{124,28... | collective-permute-start | bytes 98312 | tf_op jit(solution)/shard_map/ppermute | solution.py:199
  47.0 16.2 %collective-permute-start.6 = (bf16[4,2,64,128]{3,2,1,0:T(8,128)(2,1)S(1)}, bf16[4,2,64,128]{3,2,1,0:T(8,128)(2,1)S(1)}, u32[]{:S(2)}, u32[]{:S(2)}) collective-permute-start(bf16[4,2,64,128]{3,2,1,0:T(8,128)(2,1)S(1)} %pad_maximum_fusion.1), channel_id=1, source_target_pairs={{120,0},{124,4},{0,8},{4,12},{8,16},{12,20},{16,24},{20,28},{24,32... | collective-permute-start | bytes 393224 | tf_op jit(solution)/shard_map/ppermute | solution.py:199
  48.5 9.8 %collective-permute-start.3 = (bf16[4,2,64,128]{3,2,1,0:T(8,128)(2,1)S(1)}, bf16[4,2,64,128]{3,2,1,0:T(8,128)(2,1)S(1)}, u32[]{:S(2)}, u32[]{:S(2)}) collective-permute-start(bf16[4,2,64,128]{3,2,1,0:T(8,128)(2,1)S(1)} %pad_maximum_fusion.1), channel_id=1, source_target_pairs={{8,0},{12,4},{16,8},{20,12},{24,16},{28,20},{32,24},{36,28},{40,32... | collective-permute-start | bytes 393224 | tf_op jit(solution)/shard_map/ppermute | solution.py:199
  54.0 9.2 %collective-permute-start.5 = (bf16[2,2,64,128]{3,2,1,0:T(8,128)(2,1)S(1)}, bf16[2,2,64,128]{3,2,1,0:T(8,128)(2,1)S(1)}, u32[]{:S(2)}, u32[]{:S(2)}) collective-permute-start(bf16[2,2,64,128]{3,2,1,0:T(8,128)(2,1)S(1)} %get-tuple-element.17), channel_id=1, source_target_pairs={{112,0},{116,4},{120,8},{124,12},{0,16},{4,20},{8,24},{12,28},{16,... | collective-permute-start | bytes 196616 | tf_op jit(solution)/shard_map/ppermute | solution.py:199
  54.1 7.1 %collective-permute-start.4 = (bf16[2,2,64,128]{3,2,1,0:T(8,128)(2,1)S(1)}, bf16[2,2,64,128]{3,2,1,0:T(8,128)(2,1)S(1)}, u32[]{:S(2)}, u32[]{:S(2)}) collective-permute-start(bf16[2,2,64,128]{3,2,1,0:T(8,128)(2,1)S(1)} %get-tuple-element.18), channel_id=1, source_target_pairs={{16,0},{20,4},{24,8},{28,12},{32,16},{36,20},{40,24},{44,28},{48,3... | collective-permute-start | bytes 196616 | tf_op jit(solution)/shard_map/ppermute | solution.py:199
  63.3 27.3 %copy-start.6 = (bf16[16,2,64,128]{3,2,1,0:T(8,128)(2,1)}, bf16[16,2,64,128]{3,2,1,0:T(8,128)(2,1)S(1)}, u32[]{:S(2)}) copy-start(bf16[16,2,64,128]{3,2,1,0:T(8,128)(2,1)S(1)} %constant_dynamic-update-slice_fusion.refs_0_) | copy-start | bytes 1572868
  63.3 13.7 %collective-permute-start.16 = (bf16[16,2,64,128]{3,2,1,0:T(8,128)(2,1)S(1)}, bf16[16,2,64,128]{3,2,1,0:T(8,128)(2,1)S(1)}, u32[]{:S(2)}, u32[]{:S(2)}) collective-permute-start(bf16[16,2,64,128]{3,2,1,0:T(8,128)(2,1)S(1)} %constant_dynamic-update-slice_fusion.refs_0_), channel_id=1, source_target_pairs={{128,0},{0,128},{129,1},{1,129},{130,2},{2,130},{131,3},{3,131},{1... | collective-permute-start | bytes 1572872 | tf_op jit(solution)/shard_map/ppermute | solution.py:244
  65.8 24.1 %collective-permute-start.11 = (bf16[16,2,64,128]{3,2,1,0:T(8,128)(2,1)S(1)}, bf16[16,2,64,128]{3,2,1,0:T(8,128)(2,1)S(1)}, u32[]{:S(2)}, u32[]{:S(2)}) collective-permute-start(bf16[16,2,64,128]{3,2,1,0:T(8,128)(2,1)S(1)} %constant_dynamic-update-slice_fusion.refs_0_), channel_id=1, source_target_pairs={{4,0},{0,4},{12,8},{8,12},{20,16},{16,20},{28,24},{24,28},{36,32},... | collective-permute-start | bytes 1572872 | tf_op jit(solution)/shard_map/ppermute | solution.py:203
  71.4 18.7 %collective-permute-start.8 = (bf16[16,2,64,128]{3,2,1,0:T(8,128)(2,1)S(1)}, bf16[16,2,64,128]{3,2,1,0:T(8,128)(2,1)S(1)}, u32[]{:S(2)}, u32[]{:S(2)}) collective-permute-start(bf16[16,2,64,128]{3,2,1,0:T(8,128)(2,1)S(1)} %constant_dynamic-update-slice_fusion.refs_0_), channel_id=1, source_target_pairs={{3,0},{0,1},{1,2},{2,3},{7,4},{4,5},{5,6},{6,7},{11,8},{8,9},{9,10... | collective-permute-start | bytes 1572872 | tf_op jit(solution)/shard_map/ppermute | solution.py:199
  71.4 19.2 %collective-permute-start.7 = (bf16[16,2,64,128]{3,2,1,0:T(8,128)(2,1)S(1)}, bf16[16,2,64,128]{3,2,1,0:T(8,128)(2,1)S(1)}, u32[]{:S(2)}, u32[]{:S(2)}) collective-permute-start(bf16[16,2,64,128]{3,2,1,0:T(8,128)(2,1)S(1)} %constant_dynamic-update-slice_fusion.refs_0_), channel_id=1, source_target_pairs={{1,0},{2,1},{3,2},{0,3},{5,4},{6,5},{7,6},{4,7},{9,8},{10,9},{11,1... | collective-permute-start | bytes 1572872 | tf_op jit(solution)/shard_map/ppermute | solution.py:199
  75.0 14.9 %collective-permute-start.29 = (bf16[32,2048]{1,0:T(8,128)(2,1)S(1)}, bf16[32,2048]{1,0:T(8,128)(2,1)S(1)}, u32[]{:S(2)}, u32[]{:S(2)}) collective-permute-start(bf16[32,2048]{1,0:T(8,128)(2,1)S(1)} %slice.62), channel_id=1, source_target_pairs={{0,1},{1,2},{2,3},{3,4},{4,5},{5,6},{6,7},{7,8},{8,9},{9,10},{10,1... | collective-permute-start | bytes 393224 | tf_op jit(solution)/shard_map/ppermute | solution.py:209
  76.9 38.7 %copy-start.7 = (bf16[16,2,64,128]{3,2,1,0:T(8,128)(2,1)}, bf16[16,2,64,128]{3,2,1,0:T(8,128)(2,1)S(1)}, u32[]{:S(2)}) copy-start(bf16[16,2,64,128]{3,2,1,0:T(8,128)(2,1)S(1)} %collective-permute-done.16.refs_10_) | copy-start | bytes 1572868
  76.9 20.5 %collective-permute-start.18 = (bf16[16,2,64,128]{3,2,1,0:T(8,128)(2,1)S(1)}, bf16[16,2,64,128]{3,2,1,0:T(8,128)(2,1)}, u32[]{:S(2)}, u32[]{:S(2)}) collective-permute-start(bf16[16,2,64,128]{3,2,1,0:T(8,128)(2,1)S(1)} %collective-permute-done.16.refs_10_), channel_id=1, source_target_pairs={{3,0},{0,1},{1,2},{2,3},{7,4},{4,5},{5,6},{6,7},{11,8},{8,9},{9,10... | collective-permute-start | bytes 1572872 | tf_op jit(solution)/shard_map/ppermute | solution.py:199
  89.9 35.1 %copy-start.2 = (bf16[32,2048]{1,0:T(8,128)(2,1)}, bf16[32,2048]{1,0:T(8,128)(2,1)S(1)}, u32[]{:S(2)}) copy-start(bf16[32,2048]{1,0:T(8,128)(2,1)S(1)} %collective-permute-done.29.refs_0_.refs_21_) | copy-start | bytes 393220
  89.9 11.7 %collective-permute-start.17 = (bf16[16,2,64,128]{3,2,1,0:T(8,128)(2,1)S(1)}, bf16[16,2,64,128]{3,2,1,0:T(8,128)(2,1)}, u32[]{:S(2)}, u32[]{:S(2)}) collective-permute-start(bf16[16,2,64,128]{3,2,1,0:T(8,128)(2,1)S(1)} %collective-permute-done.16.refs_10_), channel_id=1, source_target_pairs={{1,0},{2,1},{3,2},{0,3},{5,4},{6,5},{7,6},{4,7},{9,8},{10,9},{11,1... | collective-permute-start | bytes 1572872 | tf_op jit(solution)/shard_map/ppermute | solution.py:199
  89.9 25.9 %copy-start.8 = (bf16[16,2,64,128]{3,2,1,0:T(8,128)(2,1)}, bf16[16,2,64,128]{3,2,1,0:T(8,128)(2,1)S(1)}, u32[]{:S(2)}) copy-start(bf16[16,2,64,128]{3,2,1,0:T(8,128)(2,1)S(1)} %collective-permute-done.11.refs_5_) | copy-start | bytes 1572868
  89.9 20.5 %collective-permute-start.21 = (bf16[16,2,64,128]{3,2,1,0:T(8,128)(2,1)S(1)}, bf16[16,2,64,128]{3,2,1,0:T(8,128)(2,1)S(1)}, u32[]{:S(2)}, u32[]{:S(2)}) collective-permute-start(bf16[16,2,64,128]{3,2,1,0:T(8,128)(2,1)S(1)} %collective-permute-done.16.refs_10_), channel_id=1, source_target_pairs={{4,0},{0,4},{12,8},{8,12},{20,16},{16,20},{28,24},{24,28},{36,32},... | collective-permute-start | bytes 1572872 | tf_op jit(solution)/shard_map/ppermute | solution.py:203
  90.1 24.0 %copy-start.3 = (bf16[16,2,64,128]{3,2,1,0:T(8,128)(2,1)}, bf16[16,2,64,128]{3,2,1,0:T(8,128)(2,1)S(1)}, u32[]{:S(2)}) copy-start(bf16[16,2,64,128]{3,2,1,0:T(8,128)(2,1)S(1)} %collective-permute-done.8.refs_2_) | copy-start | bytes 1572868
  90.1 24.0 %collective-permute-start.13 = (bf16[16,2,64,128]{3,2,1,0:T(8,128)(2,1)S(1)}, bf16[16,2,64,128]{3,2,1,0:T(8,128)(2,1)S(1)}, u32[]{:S(2)}, u32[]{:S(2)}) collective-permute-start(bf16[16,2,64,128]{3,2,1,0:T(8,128)(2,1)S(1)} %collective-permute-done.8.refs_2_), channel_id=1, source_target_pairs={{4,0},{0,4},{12,8},{8,12},{20,16},{16,20},{28,24},{24,28},{36,32},... | collective-permute-start | bytes 1572872 | tf_op jit(solution)/shard_map/ppermute | solution.py:203
  90.6 23.5 %copy-start.4 = (bf16[16,2,64,128]{3,2,1,0:T(8,128)(2,1)}, bf16[16,2,64,128]{3,2,1,0:T(8,128)(2,1)S(1)}, u32[]{:S(2)}) copy-start(bf16[16,2,64,128]{3,2,1,0:T(8,128)(2,1)S(1)} %collective-permute-done.7.refs_1_) | copy-start | bytes 1572868
  90.6 25.1 %collective-permute-start.12 = (bf16[16,2,64,128]{3,2,1,0:T(8,128)(2,1)S(1)}, bf16[16,2,64,128]{3,2,1,0:T(8,128)(2,1)S(1)}, u32[]{:S(2)}, u32[]{:S(2)}) collective-permute-start(bf16[16,2,64,128]{3,2,1,0:T(8,128)(2,1)S(1)} %collective-permute-done.7.refs_1_), channel_id=1, source_target_pairs={{4,0},{0,4},{12,8},{8,12},{20,16},{16,20},{28,24},{24,28},{36,32},... | collective-permute-start | bytes 1572872 | tf_op jit(solution)/shard_map/ppermute | solution.py:203
  97.4 10.4 %collective-permute-start.10 = (bf16[8,2,64,128]{3,2,1,0:T(8,128)(2,1)S(1)}, bf16[8,2,64,128]{3,2,1,0:T(8,128)(2,1)}, u32[]{:S(2)}, u32[]{:S(2)}) collective-permute-start(bf16[8,2,64,128]{3,2,1,0:T(8,128)(2,1)S(1)} %slice.67), channel_id=1, source_target_pairs={{3,0},{0,1},{1,2},{2,3},{7,4},{4,5},{5,6},{6,7},{11,8},{8,9},{9,10... | collective-permute-start | bytes 786440 | tf_op jit(solution)/shard_map/ppermute | solution.py:199
  101.6 8.8 %collective-permute-start.9 = (bf16[8,2,64,128]{3,2,1,0:T(8,128)(2,1)S(1)}, bf16[8,2,64,128]{3,2,1,0:T(8,128)(2,1)S(1)}, u32[]{:S(2)}, u32[]{:S(2)}) collective-permute-start(bf16[8,2,64,128]{3,2,1,0:T(8,128)(2,1)S(1)} %slice.66), channel_id=1, source_target_pairs={{1,0},{2,1},{3,2},{0,3},{5,4},{6,5},{7,6},{4,7},{9,8},{10,9},{11,1... | collective-permute-start | bytes 786440 | tf_op jit(solution)/shard_map/ppermute | solution.py:199
  107.8 8.8 %collective-permute-start.15 = (bf16[8,2,64,128]{3,2,1,0:T(8,128)(2,1)}, bf16[8,2,64,128]{3,2,1,0:T(8,128)(2,1)}, u32[]{:S(2)}, u32[]{:S(2)}) collective-permute-start(bf16[8,2,64,128]{3,2,1,0:T(8,128)(2,1)} %collective-permute-done.10.refs_4_), channel_id=1, source_target_pairs={{4,0},{0,4},{12,8},{8,12},{20,16},{16,20},{28,24},{24,28},{36,32},... | collective-permute-start | bytes 786440 | tf_op jit(solution)/shard_map/ppermute | solution.py:203
  110.4 5.4 %copy-start.12 = (bf16[8,2,64,128]{3,2,1,0:T(8,128)(2,1)}, bf16[8,2,64,128]{3,2,1,0:T(8,128)(2,1)S(1)}, u32[]{:S(2)}) copy-start(bf16[8,2,64,128]{3,2,1,0:T(8,128)(2,1)S(1)} %collective-permute-done.9.refs_3_) | copy-start | bytes 786436
  110.4 9.4 %collective-permute-start.20 = (bf16[8,2,64,128]{3,2,1,0:T(8,128)(2,1)}, bf16[8,2,64,128]{3,2,1,0:T(8,128)(2,1)}, u32[]{:S(2)}, u32[]{:S(2)}) collective-permute-start(bf16[8,2,64,128]{3,2,1,0:T(8,128)(2,1)} %slice.69), channel_id=1, source_target_pairs={{3,0},{0,1},{1,2},{2,3},{7,4},{4,5},{5,6},{6,7},{11,8},{8,9},{9,10... | collective-permute-start | bytes 786440 | tf_op jit(solution)/shard_map/ppermute | solution.py:199
  110.4 5.4 %copy-start.9 = (bf16[16,2,64,128]{3,2,1,0:T(8,128)(2,1)}, bf16[16,2,64,128]{3,2,1,0:T(8,128)(2,1)S(1)}, u32[]{:S(2)}) copy-start(bf16[16,2,64,128]{3,2,1,0:T(8,128)(2,1)S(1)} %collective-permute-done.21.refs_15_) | copy-start | bytes 1572868
  110.4 11.1 %collective-permute-start.19 = (bf16[8,2,64,128]{3,2,1,0:T(8,128)(2,1)S(1)}, bf16[8,2,64,128]{3,2,1,0:T(8,128)(2,1)}, u32[]{:S(2)}, u32[]{:S(2)}) collective-permute-start(bf16[8,2,64,128]{3,2,1,0:T(8,128)(2,1)S(1)} %slice.68), channel_id=1, source_target_pairs={{1,0},{2,1},{3,2},{0,3},{5,4},{6,5},{7,6},{4,7},{9,8},{10,9},{11,1... | collective-permute-start | bytes 786440 | tf_op jit(solution)/shard_map/ppermute | solution.py:199
  114.1 1.8 %copy-start.10 = (bf16[16,2,64,128]{3,2,1,0:T(8,128)(2,1)}, bf16[16,2,64,128]{3,2,1,0:T(8,128)(2,1)S(1)}, u32[]{:S(2)}) copy-start(bf16[16,2,64,128]{3,2,1,0:T(8,128)(2,1)S(1)} %collective-permute-done.13.refs_7_) | copy-start | bytes 1572868
  114.1 14.0 %collective-permute-start.23 = (bf16[16,2,64,128]{3,2,1,0:T(8,128)(2,1)}, bf16[16,2,64,128]{3,2,1,0:T(8,128)(2,1)}, u32[]{:S(2)}, u32[]{:S(2)}) collective-permute-start(bf16[16,2,64,128]{3,2,1,0:T(8,128)(2,1)} %collective-permute-done.18.refs_12_), channel_id=1, source_target_pairs={{4,0},{0,4},{12,8},{8,12},{20,16},{16,20},{28,24},{24,28},{36,32},... | collective-permute-start | bytes 1572872 | tf_op jit(solution)/shard_map/ppermute | solution.py:203
  115.6 0.8 copy-start.11
  115.6 12.5 %collective-permute-start.22 = (bf16[16,2,64,128]{3,2,1,0:T(8,128)(2,1)}, bf16[16,2,64,128]{3,2,1,0:T(8,128)(2,1)}, u32[]{:S(2)}, u32[]{:S(2)}) collective-permute-start(bf16[16,2,64,128]{3,2,1,0:T(8,128)(2,1)} %collective-permute-done.17.refs_11_), channel_id=1, source_target_pairs={{4,0},{0,4},{12,8},{8,12},{20,16},{16,20},{28,24},{24,28},{36,32},... | collective-permute-start | bytes 1572872 | tf_op jit(solution)/shard_map/ppermute | solution.py:203
  116.6 10.0 %collective-permute-start.14 = (bf16[8,2,64,128]{3,2,1,0:T(8,128)(2,1)}, bf16[8,2,64,128]{3,2,1,0:T(8,128)(2,1)S(1)}, u32[]{:S(2)}, u32[]{:S(2)}) collective-permute-start(bf16[8,2,64,128]{3,2,1,0:T(8,128)(2,1)} %copy-done.12), channel_id=1, source_target_pairs={{4,0},{0,4},{12,8},{8,12},{20,16},{16,20},{28,24},{24,28},{36,32},... | collective-permute-start | bytes 786440 | tf_op jit(solution)/shard_map/ppermute | solution.py:203
  119.8 7.6 %collective-permute-start.25 = (bf16[8,2,64,128]{3,2,1,0:T(8,128)(2,1)}, bf16[8,2,64,128]{3,2,1,0:T(8,128)(2,1)S(1)}, u32[]{:S(2)}, u32[]{:S(2)}) collective-permute-start(bf16[8,2,64,128]{3,2,1,0:T(8,128)(2,1)} %collective-permute-done.20.refs_14_), channel_id=1, source_target_pairs={{4,0},{0,4},{12,8},{8,12},{20,16},{16,20},{28,24},{24,28},{36,32},... | collective-permute-start | bytes 786440 | tf_op jit(solution)/shard_map/ppermute | solution.py:203
  121.5 6.6 %collective-permute-start.24 = (bf16[8,2,64,128]{3,2,1,0:T(8,128)(2,1)}, bf16[8,2,64,128]{3,2,1,0:T(8,128)(2,1)S(1)}, u32[]{:S(2)}, u32[]{:S(2)}) collective-permute-start(bf16[8,2,64,128]{3,2,1,0:T(8,128)(2,1)} %collective-permute-done.19.refs_13_), channel_id=1, source_target_pairs={{4,0},{0,4},{12,8},{8,12},{20,16},{16,20},{28,24},{24,28},{36,32},... | collective-permute-start | bytes 786440 | tf_op jit(solution)/shard_map/ppermute | solution.py:203
  125.0 1.7 %copy-start.1 = (bf16[800,2048]{1,0:T(8,128)(2,1)}, bf16[800,2048]{1,0:T(8,128)(2,1)S(1)}, u32[]{:S(2)}) copy-start(bf16[800,2048]{1,0:T(8,128)(2,1)S(1)} %shard_map.82.refs_23_) | copy-start | bytes 9830404
  126.7 0.7 copy-start.13
  127.4 0.7 copy-start.14
  128.1 0.7 copy-start.15
Sparse Core Ops, SparseCore 0:
  19.0 94.8 all-gather.2
